TPU v7x, 32 devices: a whole 2x2x4 slice. The times are simulated.
32 devices in a mesh: sp: 16 (over z, y, x), tp: 2 (over core).
Axes of the slice: x: 2, y: 2, z: 4, core: 2. Of those that a mesh axis runs over, the one named last changes fastest.
Arguments:
- mid_rows: bfloat16 [4096, 2048], P(('sp', 'tp')), may hold values from -6 to 6
- cotangent: bfloat16 [4096, 2048], P(('sp', 'tp')), may hold values from -6 to 6
- routes: int32 [4096, 2], P(('sp', 'tp')), may hold values from 0 to 15, all different within a row; in each aligned block of 128 rows (0 to 127, 128 to 255, ...) at most 32 rows name the same one
- route_weight: float32 [4096, 2], P(('sp', 'tp')), may hold values from 0.3 to 2
- filtered: bfloat16 [4096, 2048], P('sp', 'tp'), may hold values from -30 to 30
- conv_taps: float32 [31, 2048], P(None, 'tp'), may hold values from -1 to 1
- norm_gain: float32 [2048], P('tp'), may hold values from 0.1 to 1.9
- out_weight: bfloat16 [2048, 2048], P('tp'), may hold values from -0.125 to 0.125
- gate_weight: bfloat16 [16, 2048, 1024], P('sp', None, 'tp'), may hold values from -0.125 to 0.125
- up_weight: bfloat16 [16, 2048, 1024], P('sp', None, 'tp'), may hold values from -0.125 to 0.125
- down_weight: bfloat16 [16, 1024, 2048], P('sp', 'tp'), may hold values from -0.1875 to 0.1875
Outputs:
- gate_grad: float32 [16, 2048, 1024], P('sp', None, 'tp')
- up_grad: float32 [16, 2048, 1024], P('sp', None, 'tp')
- down_grad: float32 [16, 1024, 2048], P('sp', 'tp')
- proj_grad: float32 [2048, 2048], P('sp', 'tp')
- input_grad: bfloat16 [4096, 2048], P('sp', 'tp')
Inputs may be any that keep to these rules, and one draw needn't show every extreme that they name: `routes`: each row names 2 different experts. In each aligned block of 128 rows no expert is named by more than 32 rows.
All inputs are finite; a program needn't handle non-finite values.
Results may differ from a plain program's by a relative error of at most 0.0075.
Values may be sent and summed in bfloat16 or wider, within the bound.
A program may use at most 128 MiB of HBM per device.

v0:
```python
import jax
import jax.numpy as jnp
from jax import lax
from jax.sharding import PartitionSpec as P

NORM_EPS = 1e-05


def extended(block, sides, width):
    for axis, dim in sides:
        count = lax.axis_size(axis)
        forward = [(i, i + 1) for i in range(count - 1)]
        backward = [(target, source) for source, target in forward]
        low = lax.ppermute(
            lax.slice_in_dim(block, block.shape[dim] - width, None, axis=dim), axis, forward
        )
        high = lax.ppermute(lax.slice_in_dim(block, 0, width, axis=dim), axis, backward)
        block = jnp.concatenate([low, block, high], axis=dim)
    return block


def silu_grad(pre_act):
    logistic = jax.nn.sigmoid(pre_act)
    return logistic * (1.0 + pre_act * (1.0 - logistic))


def assign_slots(routes, experts, capacity):
    token_count, per_token = routes.shape
    flattened = routes.reshape(token_count * per_token)
    one_hot = (flattened[:, None] == jnp.arange(experts, dtype=jnp.int32)[None, :]).astype(
        jnp.int32
    )
    earlier = jnp.cumsum(one_hot, axis=0) - one_hot
    positions = jnp.sum(earlier * one_hot, axis=1)
    target = flattened * capacity + positions
    route_ids = jnp.arange(token_count * per_token, dtype=jnp.int32)
    slot_owner = (
        jnp.full((experts * capacity,), token_count * per_token, jnp.int32)
        .at[target]
        .set(route_ids)
    )
    return (slot_owner, target)


def expert_backward(inputs, routed, gate_mat, up_mat, down_mat):
    pre_gate = jnp.einsum("secd,edf->secf", inputs, gate_mat, preferred_element_type=jnp.float32)
    pre_up = jnp.einsum("secd,edf->secf", inputs, up_mat, preferred_element_type=jnp.float32)
    gate_act = jax.nn.silu(pre_gate)
    hidden = (gate_act * pre_up).astype(jnp.bfloat16)
    down_part = jnp.einsum("secf,secd->efd", hidden, routed, preferred_element_type=jnp.float32)
    hidden_grad = jnp.einsum("secd,efd->secf", routed, down_mat, preferred_element_type=jnp.float32)
    gate_pre = (hidden_grad * pre_up * silu_grad(pre_gate)).astype(jnp.bfloat16)
    up_pre = (hidden_grad * gate_act).astype(jnp.bfloat16)
    gate_part = jnp.einsum("secd,secf->edf", inputs, gate_pre, preferred_element_type=jnp.float32)
    up_part = jnp.einsum("secd,secf->edf", inputs, up_pre, preferred_element_type=jnp.float32)
    return (gate_pre, up_pre, gate_part, up_part, down_part)


def input_part(gate_pre, up_pre, gate_mat, up_mat):
    first_term = jnp.einsum(
        "secf,edf->secd", gate_pre, gate_mat, preferred_element_type=jnp.float32
    )
    return first_term + jnp.einsum(
        "secf,edf->secd", up_pre, up_mat, preferred_element_type=jnp.float32
    )


def per_device(
    mid_rows,
    cotangent,
    routes,
    route_weight,
    filtered,
    conv_taps,
    norm_gain,
    out_weight,
    gate_weight,
    up_weight,
    down_weight,
):
    sp_count = lax.axis_size("sp")
    token_count, model_width = mid_rows.shape
    per_token = routes.shape[1]
    local_experts = gate_weight.shape[0]
    experts = local_experts * sp_count
    capacity = 2 * token_count * per_token // sp_count
    values = filtered.astype(jnp.float32)
    channel_sum, squares = lax.psum(
        (jnp.sum(values, axis=1), jnp.sum(values * values, axis=1)), "tp"
    )
    slot_owner, target = assign_slots(routes, experts, capacity)
    token_of = slot_owner // per_token
    inputs = jnp.take(mid_rows, token_of, axis=0, mode="fill", fill_value=0)
    route_scale = jnp.take(
        route_weight.reshape(token_count * per_token), slot_owner, mode="fill", fill_value=0.0
    )
    cot_rows = jnp.take(cotangent, token_of, axis=0, mode="fill", fill_value=0)
    routed = (route_scale[:, None] * cot_rows.astype(jnp.float32)).astype(jnp.bfloat16)
    inputs = inputs.reshape(sp_count, local_experts, capacity, model_width)
    routed = routed.reshape(sp_count, local_experts, capacity, model_width)
    got_in = lax.all_to_all(inputs, "sp", split_axis=0, concat_axis=0, tiled=True)
    got_cot = lax.all_to_all(routed, "sp", split_axis=0, concat_axis=0, tiled=True)
    all_in = lax.all_gather(got_in, "tp", axis=0, tiled=True)
    all_cot = lax.all_gather(got_cot, "tp", axis=0, tiled=True)
    gate_pre, up_pre, gate_part, up_part, down_part = expert_backward(
        all_in, all_cot, gate_weight, up_weight, down_weight
    )
    partial_rows = input_part(gate_pre, up_pre, gate_weight, up_weight).astype(jnp.bfloat16)
    back_rows = (
        lax.psum_scatter(partial_rows, "tp", scatter_dimension=0, tiled=True)
        .astype(jnp.float32)
        .astype(jnp.bfloat16)
    )
    returned = lax.all_to_all(back_rows, "sp", split_axis=0, concat_axis=0, tiled=True)
    gate_grad, up_grad, down_grad = (gate_part, up_part, down_part)
    back_all = returned.reshape(experts * capacity, model_width)
    route_rows = jnp.take(back_all, target, axis=0)
    route_sum = jnp.sum(
        route_rows.astype(jnp.float32).reshape(token_count, per_token, model_width), axis=1
    )
    mid_grad = (cotangent.astype(jnp.float32) + route_sum).astype(jnp.bfloat16)
    average = channel_sum / model_width
    variance = squares / model_width - average * average
    inv_scale = lax.rsqrt(variance + NORM_EPS)[:, None]
    normed = (values - average[:, None]) * inv_scale
    scaled = normed * norm_gain
    activated = jax.nn.silu(scaled).astype(jnp.bfloat16)
    grad_tokens = lax.all_gather(mid_grad, "tp", axis=0, tiled=True)
    proj_grad = lax.psum_scatter(
        lax.dot_general(
            grad_tokens, activated, (((0,), (0,)), ((), ())), preferred_element_type=jnp.float32
        ),
        "sp",
        scatter_dimension=0,
        tiled=True,
    )
    act_grad = lax.dot_general(
        grad_tokens, out_weight, (((1,), (1,)), ((), ())), preferred_element_type=jnp.float32
    )
    scaled_grad = act_grad * silu_grad(scaled) * norm_gain
    grad_total, corr_total = lax.psum(
        (jnp.sum(scaled_grad, axis=1), jnp.sum(scaled_grad * normed, axis=1)), "tp"
    )
    grad_mean = (grad_total / model_width)[:, None]
    grad_corr = (corr_total / model_width)[:, None]
    conv_grad = (inv_scale * (scaled_grad - grad_mean - normed * grad_corr)).astype(jnp.bfloat16)
    halo_width = conv_taps.shape[0] // 2
    padded = extended(conv_grad, (("sp", 0),), halo_width)
    seq_rows = conv_grad.shape[0]
    accumulated = jnp.zeros(conv_grad.shape, jnp.float32)
    for offset in range(conv_taps.shape[0]):
        lead = 2 * halo_width - offset
        accumulated = accumulated + conv_taps[offset] * padded[lead : lead + seq_rows]
    input_grad = accumulated.astype(jnp.bfloat16)
    return (gate_grad, up_grad, down_grad, proj_grad, input_grad)


def solution(mesh):
    in_specs = (
        P(("sp", "tp"), None),
        P(("sp", "tp"), None),
        P(("sp", "tp"), None),
        P(("sp", "tp"), None),
        P("sp", "tp"),
        P(None, "tp"),
        P("tp"),
        P("tp", None),
        P("sp", None, "tp"),
        P("sp", None, "tp"),
        P("sp", "tp", None),
    )
    out_specs = (
        P("sp", None, "tp"),
        P("sp", None, "tp"),
        P("sp", "tp", None),
        P("sp", "tp"),
        P("sp", "tp"),
    )
    return jax.shard_map(
        per_device, mesh=mesh, in_specs=in_specs, out_specs=out_specs, check_vma=False
    )
```

profile of v0, /device:TPU:0, one launch (start us, length us, event | category | flops | bytes accessed | tf_op | source)
XLA Modules:
  0.0 438.8 jit_solution(12679315250991110465)
XLA Ops:
  7.2 0.8 broadcast_multiply_fusion.3
  8.0 0.8 copy.43
  8.9 0.1 eq.29
  9.2 0.1 mul.422
  9.4 0.6 reduce-window.6
  9.9 0.2 slice_reduce_fusion
  10.3 1.4 scatter_custom_fusion
  11.7 6.3 %gather_fusion.2 = bf16[512,2048]{1,0:T(8,128)(2,1)} fusion(bf16[128,2048]{1,0:T(8,128)(2,1)} %param.13, s32[1024]{0:T(1024)S(1)} %pad_clamp_fusion.2), kind=kCustom, calls=%fused_computation.clone | custom fusion | bytes 4196352 | tf_op jit(solution)/shard_map/jit(_take)/gather | solution.py:93
  18.1 3.1 broadcast_select_fusion
  21.2 8.5 %all-to-all-start = ((bf16[16,1,32,2048]{3,2,1,0:T(8,128)(2,1)}), bf16[16,1,32,2048]{3,2,1,0:T(8,128)(2,1)}, u32[]{:S(2)}, u32[]{:S(2)}) async-start(bf16[16,1,32,2048]{3,2,1,0:T(8,128)(2,1)} %bitcast.187), calls=%async_computation | async-start | bytes 4194304 | tf_op jit(solution)/shard_map/all_to_all | solution.py:101
  29.8 3.3 gather_fusion.3
  33.2 0.1 reshape.144
  33.3 3.5 gather_fusion
  36.9 35.9 %all-to-all-done = bf16[16,1,32,2048]{3,2,1,0:T(8,128)(2,1)} async-done(((bf16[16,1,32,2048]{3,2,1,0:T(8,128)(2,1)}), bf16[16,1,32,2048]{3,2,1,0:T(8,128)(2,1)}, u32[]{:S(2)}, u32[]{:S(2)}) %all-to-all-start) | async-done | bytes 2097184 | tf_op jit(solution)/shard_map/all_to_all | solution.py:101
  72.9 2.1 multiply_convert_fusion
  75.0 58.1 %all_to_all.15 = bf16[16,1,32,2048]{3,2,1,0:T(8,128)(2,1)} all-to-all(bf16[16,1,32,2048]{3,2,1,0:T(8,128)(2,1)S(1)} %bitcast.188), channel_id=1, replica_groups=mesh['sp'=16,'tp'=2] {'sp'}, dimensions={0} | all-to-all | bytes 4194304 | tf_op jit(solution)/shard_map/all_to_all | solution.py:102
  133.1 0.2 reduce-scatter.3.cloned.1.call-start
  133.4 6.0 %fusion.9 = f32[32,32,512]{2,1,0:T(8,128)} fusion(bf16[32,1,32,2048]{3,2,1,0:T(8,128)(2,1)} %all-gather.4.cloned.1.call-done, bf16[1,2048,512]{2,1,0:T(8,128)(2,1)S(1)} %copy-done), kind=kOutput, calls=%fused_computation.15 | convolution fusion | flops 2147483648 | bytes 8388608 | tf_op jit(solution)/shard_map/secd,edf->secf/dot_general | solution.py:46
  139.4 3.7 fusion.11
  143.1 2.2 all-gather.6.cloned.1.call-done
  145.3 7.1 %fusion.56 = (bf16[32,32,512]{2,1,0:T(8,128)(2,1)S(1)}, bf16[32,1,32,512]{3,2,0,1:T(8,128)(2,1)S(1)}) fusion(f32[32,32,512]{2,1,0:T(8,128)} %fusion.9, f32[32,32,512]{2,1,0:T(8,128)} %fusion.11, bf16[1,512,2048]{2,1,0:T(8,128)(2,1)} %param.23, bf16[32,1,32,2048]{3,2,1,0:T(8,128)(2,1)} %all-gather.6.cloned.1.call-done), kind=kOutput, calls=%fused_computation.98 | convolution fusion | flops 2154299392 | bytes 12582912 | tf_op jit(solution)/shard_map/secd,efd->secf/dot_general | solution.py:51
  152.4 2.4 fusion.31
  154.8 4.4 fusion
  159.2 13.4 %reduce-scatter.3.cloned.1.call-done = bf16[16,1,32,2048]{3,2,0,1:T(8,128)(2,1)} async-done(((bf16[32,1,32,2048]{3,2,0,1:T(8,128)(2,1)}), bf16[16,1,32,2048]{3,2,0,1:T(8,128)(2,1)}) %reduce-scatter.3.cloned.1.call-update) | async-done | bytes 2097168 | tf_op jit(solution)/shard_map/reduce_scatter | solution.py:110
  172.6 7.0 %all-to-all-start.2 = ((bf16[16,1,32,2048]{3,2,1,0:T(8,128)(2,1)}), bf16[16,1,32,2048]{3,2,1,0:T(8,128)(2,1)S(1)}, u32[]{:S(2)}, u32[]{:S(2)}) async-start(bf16[16,1,32,2048]{3,2,1,0:T(8,128)(2,1)} %bitcast.189), calls=%async_computation.3 | async-start | bytes 4194304 | tf_op jit(solution)/shard_map/all_to_all | solution.py:114
  179.6 0.3 all-gather.8.cloned.1.call-start
  180.1 0.1 copy.50
  180.3 42.6 %all-to-all-done.2 = bf16[16,1,32,2048]{3,2,1,0:T(8,128)(2,1)S(1)} async-done(((bf16[16,1,32,2048]{3,2,1,0:T(8,128)(2,1)}), bf16[16,1,32,2048]{3,2,1,0:T(8,128)(2,1)S(1)}, u32[]{:S(2)}, u32[]{:S(2)}) %all-to-all-start.2) | async-done | bytes 2097184 | tf_op jit(solution)/shard_map/all_to_all | solution.py:114
  222.9 2.3 gather_fusion.1
  225.2 1.7 gather.15
  227.0 3.9 convert_reduce_fusion
  230.9 0.9 add_convert_fusion.2
  231.9 0.2 convert_reduce_fusion.1
  232.1 2.7 all-reduce.1
  234.9 10.7 %all-gather.8.cloned.1.call-done = bf16[256,2048]{1,0:T(8,128)(2,1)} async-done(((bf16[128,2048]{1,0:T(8,128)(2,1)}), bf16[256,2048]{1,0:T(8,128)(2,1)}) %all-gather.8.cloned.1.call-update) | async-done | bytes 1048592 | tf_op jit(solution)/shard_map/all_gather | solution.py:128
  245.6 6.1 %fusion.61 = f32[2048,1024]{1,0:T(8,128)} fusion(bf16[256,2048]{1,0:T(8,128)(2,1)} %all-gather.8.cloned.1.call-done, bf16[256,1024]{1,0:T(8,128)(2,1)S(1)} %copy-done.3, f32[1024]{0:T(1024)S(1)} %copy-done.7, f32[256]{0:T(256)S(1)} %get-tuple-element.52, f32[256]{0:T(256)S(1)} %get-tuple-element.51), kind=kOutput, calls=%fused_computation.104 | convolution fusion | flops 1076101120 | bytes 9967616 | tf_op jit(solution)/shard_map/dot_general | solution.py:130
  251.7 0.9 copy-done.5
  252.6 0.3 copy-done.16
  252.9 6.7 %fusion.13 = f32[1,2048,512]{2,1,0:T(8,128)} fusion(bf16[32,1,32,2048]{3,2,1,0:T(8,128)(2,1)} %all-gather.4.cloned.1.call-done, bf16[32,1,32,512]{3,2,0,1:T(8,128)(2,1)S(1)} %copy-done.16), kind=kOutput, calls=%fused_computation.20 | convolution fusion | flops 2147483648 | bytes 9437184 | tf_op jit(solution)/shard_map/secd,secf->edf/dot_general | solution.py:54
  259.7 4.5 %fusion.19 = f32[1,512,2048]{2,1,0:T(8,128)} fusion(bf16[32,1,32,2048]{3,2,1,0:T(8,128)(2,1)S(1)} %copy-done.11, f32[32,32,512]{2,1,0:T(8,128)S(1)} %copy-done.18, f32[32,32,512]{2,1,0:T(8,128)S(1)} %copy-done.17), kind=kOutput, calls=%fused_computation.22 | convolution fusion | flops 2150629376 | bytes 12582912 | tf_op jit(solution)/shard_map/secf,secd->efd/dot_general | solution.py:50
  264.2 1.7 fusion.105
  265.9 2.5 all-reduce
  268.4 0.3 fusion.54
  268.8 3.6 collective-permute-start.1
  272.4 1.3 collective-permute-start
  273.7 7.0 %fusion.16 = f32[1,2048,512]{2,1,0:T(8,128)} fusion(bf16[32,32,512]{2,1,0:T(8,128)(2,1)} %copy-done.14, bf16[32,1,32,2048]{3,2,1,0:T(8,128)(2,1)} %all-gather.4.cloned.1.call-done), kind=kOutput, calls=%fused_computation.21 | convolution fusion | flops 2147483648 | bytes 9437184 | tf_op jit(solution)/shard_map/secd,secf->edf/dot_general | solution.py:55
  280.8 5.4 %add_convert_fusion.1 = bf16[256,1024]{1,0:T(8,128)(2,1)} fusion(bf16[256,1024]{1,0:T(8,128)(2,1)S(1)} %fusion.54, bf16[15,1024]{1,0:T(8,128)(2,1)S(1)} %collective-permute-done.1, bf16[15,1024]{1,0:T(8,128)(2,1)S(1)} %collective-permute-done, f32[1024]{0:T(1024)S(1)} %bitcast.200, f32[1024]{0:T(1024)S(1)} %bitcast.201, f32[1024]{0:T(1024)S(1)} %bitcast.203, ...), kind=kLoop, calls=%fused_computation.102 | loop fusion | flops 47972352 | bytes 1236992 | tf_op jit(solution)/shard_map/convert_element_type | solution.py:154
  286.2 146.1 %reduce-scatter.5.cloned.1.call-done = f32[128,1024]{1,0:T(8,128)} async-done(((f32[2048,1024]{1,0:T(8,128)}), f32[128,1024]{1,0:T(8,128)}) %reduce-scatter.5.cloned.1.call-update) | async-done | bytes 524304 | tf_op jit(solution)/shard_map/reduce_scatter | solution.py:129
  (70 shorter events, 1.2 us)
Async XLA Ops:
  7.2 126.2 %copy-start = (bf16[1,2048,512]{2,1,0:T(8,128)(2,1)S(1)}, bf16[1,2048,512]{2,1,0:T(8,128)(2,1)}, u32[]{:S(2)}) copy-start(bf16[1,2048,512]{2,1,0:T(8,128)(2,1)} %param.21) | copy-start | bytes 6291460
  21.2 8.6 %copy-start.2 = (bf16[128,2048]{1,0:T(8,128)(2,1)S(1)}, bf16[128,2048]{1,0:T(8,128)(2,1)}, u32[]{:S(2)}) copy-start(bf16[128,2048]{1,0:T(8,128)(2,1)} %param.14) | copy-start | bytes 1572868
  21.2 51.6 %all-to-all-start = ((bf16[16,1,32,2048]{3,2,1,0:T(8,128)(2,1)}), bf16[16,1,32,2048]{3,2,1,0:T(8,128)(2,1)}, u32[]{:S(2)}, u32[]{:S(2)}) async-start(bf16[16,1,32,2048]{3,2,1,0:T(8,128)(2,1)} %bitcast.187), calls=%async_computation | async-start | bytes 4194304 | tf_op jit(solution)/shard_map/all_to_all | solution.py:101
  29.7 3.4 copy-start.8
  29.7 103.7 %all-gather.4.cloned.1.call-start = ((), (), s32[]{:S(2)}) async-start(), calls=%async_computation.5 | async-start | bytes 6291456 | tf_op jit(solution)/shard_map/all_gather | solution.py:103
  72.8 72.5 %all-gather.6.cloned.1.call-start = ((), (), s32[]{:S(2)}) async-start(), calls=%async_computation.6 | async-start | bytes 6291456 | tf_op jit(solution)/shard_map/all_gather | solution.py:104
  133.1 39.4 %reduce-scatter.3.cloned.1.call-start = ((), (), s32[]{:S(2)}) async-start(), calls=%async_computation.7 | async-start | bytes 6291456 | tf_op jit(solution)/shard_map/reduce_scatter | solution.py:110
  133.4 6.0 %copy-start.10 = (bf16[32,1,32,2048]{3,2,1,0:T(8,128)(2,1)S(1)}, bf16[32,1,32,2048]{3,2,1,0:T(8,128)(2,1)}, u32[]{:S(2)}) copy-start(bf16[32,1,32,2048]{3,2,1,0:T(8,128)(2,1)} %all-gather.4.cloned.1.call-done) | copy-start | bytes 12582916
  133.4 6.0 %copy-start.12 = (bf16[1,2048,512]{2,1,0:T(8,128)(2,1)S(1)}, bf16[1,2048,512]{2,1,0:T(8,128)(2,1)}, u32[]{:S(2)}) copy-start(bf16[1,2048,512]{2,1,0:T(8,128)(2,1)} %param.22) | copy-start | bytes 6291460
  152.3 2.4 copy-start.15
  152.3 2.4 copy-start.14
  152.4 2.4 copy-start.13
  172.6 7.5 %copy-start.6 = (s32[128,2]{0,1:T(2,128)S(1)}, s32[128,2]{0,1:T(2,128)}, u32[]{:S(2)}) copy-start(s32[128,2]{0,1:T(2,128)} %param.15) | copy-start | bytes 3076
  172.6 50.3 %all-to-all-start.2 = ((bf16[16,1,32,2048]{3,2,1,0:T(8,128)(2,1)}), bf16[16,1,32,2048]{3,2,1,0:T(8,128)(2,1)S(1)}, u32[]{:S(2)}, u32[]{:S(2)}) async-start(bf16[16,1,32,2048]{3,2,1,0:T(8,128)(2,1)} %bitcast.189), calls=%async_computation.3 | async-start | bytes 4194304 | tf_op jit(solution)/shard_map/all_to_all | solution.py:114
  179.6 66.0 %all-gather.8.cloned.1.call-start = ((), (), s32[]{:S(2)}) async-start(), calls=%async_computation.8 | async-start | bytes 1572864 | tf_op jit(solution)/shard_map/all_gather | solution.py:128
  227.0 4.9 %copy-start.3 = (bf16[256,1024]{1,0:T(8,128)(2,1)S(1)}, bf16[256,1024]{1,0:T(8,128)(2,1)}, u32[]{:S(2)}) copy-start(bf16[256,1024]{1,0:T(8,128)(2,1)} %param.17) | copy-start | bytes 1572868
  230.9 14.7 %copy-start.7 = (f32[1024]{0:T(1024)S(1)}, f32[1024]{0:T(1024)}, u32[]{:S(2)}) copy-start(f32[1024]{0:T(1024)} %param.19) | copy-start | bytes 12292
  231.8 200.4 %reduce-scatter.5.cloned.1.call-start = ((), (), s32[]{:S(2)}) async-start(), calls=%async_computation.9 | async-start | bytes 8912896 | tf_op jit(solution)/shard_map/reduce_scatter | solution.py:129
  251.6 0.9 copy-start.5
  251.6 1.3 copy-start.16
  252.9 6.7 %copy-start.11 = (bf16[32,1,32,2048]{3,2,1,0:T(8,128)(2,1)S(1)}, bf16[32,1,32,2048]{3,2,1,0:T(8,128)(2,1)}, u32[]{:S(2)}) copy-start(bf16[32,1,32,2048]{3,2,1,0:T(8,128)(2,1)} %all-gather.6.cloned.1.call-done) | copy-start | bytes 12582916
  252.9 6.7 %copy-start.17 = (f32[32,32,512]{2,1,0:T(8,128)S(1)}, f32[32,32,512]{2,1,0:T(8,128)}, u32[]{:S(2)}) copy-start(f32[32,32,512]{2,1,0:T(8,128)} %fusion.9) | copy-start | bytes 6291460
  252.9 6.7 %copy-start.18 = (f32[32,32,512]{2,1,0:T(8,128)S(1)}, f32[32,32,512]{2,1,0:T(8,128)}, u32[]{:S(2)}) copy-start(f32[32,32,512]{2,1,0:T(8,128)} %fusion.11) | copy-start | bytes 6291460
  259.7 4.5 %copy-start.4 = (bf16[256,2048]{1,0:T(8,128)(2,1)S(1)}, bf16[256,2048]{1,0:T(8,128)(2,1)}, u32[]{:S(2)}) copy-start(bf16[256,2048]{1,0:T(8,128)(2,1)} %all-gather.8.cloned.1.call-done) | copy-start | bytes 3145732
  259.7 4.5 %copy-start.9 = (bf16[1024,2048]{1,0:T(8,128)(2,1)S(1)}, bf16[1024,2048]{1,0:T(8,128)(2,1)}, u32[]{:S(2)}) copy-start(bf16[1024,2048]{1,0:T(8,128)(2,1)} %param.20) | copy-start | bytes 12582916
  268.8 12.0 %collective-permute-start.1 = (bf16[15,1024]{1,0:T(8,128)(2,1)S(1)}, bf16[15,1024]{1,0:T(8,128)(2,1)S(1)}, u32[]{:S(2)}, u32[]{:S(2)}) collective-permute-start(bf16[15,1024]{1,0:T(8,128)(2,1)S(1)} %get-tuple-element.19), channel_id=1, source_target_pairs={{0,2},{2,4},{4,6},{6,8},{8,10},{10,12},{12,14},{14,16},{16,18},{18... | collective-permute-start | bytes 92168 | tf_op jit(solution)/shard_map/ppermute | solution.py:14
  272.4 8.3 %collective-permute-start = (bf16[15,1024]{1,0:T(8,128)(2,1)S(1)}, bf16[15,1024]{1,0:T(8,128)(2,1)S(1)}, u32[]{:S(2)}, u32[]{:S(2)}) collective-permute-start(bf16[15,1024]{1,0:T(8,128)(2,1)S(1)} %get-tuple-element.18), channel_id=1, source_target_pairs={{2,0},{4,2},{6,4},{8,6},{10,8},{12,10},{14,12},{16,14},{18,16},{20... | collective-permute-start | bytes 92168 | tf_op jit(solution)/shard_map/ppermute | solution.py:17
  273.7 158.6 %copy-start.1 = (bf16[1,2048,512]{2,1,0:T(8,128)(2,1)S(1)}, bf16[1,2048,512]{2,1,0:T(8,128)(2,1)}, u32[]{:S(2)}) copy-start(bf16[1,2048,512]{2,1,0:T(8,128)(2,1)} %param.21) | copy-start | bytes 6291460
Sparse Core Ops, SparseCore 0:
  72.9 18.0 all-gather.3
  133.3 11.9 all-gather.5
  159.3 13.2 reduce-scatter.2
  232.0 13.5 all-gather.7
  251.8 180.4 reduce-scatter.4
where the time goes:
time: 441 us; the launch traced here: 439 us
  waiting for transfers between devices  251 us (57%)
  blocking collectives  63.3 us (14%)
  matrix products  49.5 us (11%)
  local copies, waits for them, and re-layouts  22.1 us (5%)
  starting transfers between devices  21.1 us (5%)
  other arithmetic  17.8 us (4%)
  between operations  14.1 us (3%)
    reduce_scatter x1, waiting for transfers between devices, per_device(): lax.psum_scatter(lax.dot_general(grad_tokens, activated, (((0,), (0,)), (...  146 us
    all_to_all x1, blocking collectives, per_device(): lax.all_to_all(routed, 'sp', split_axis=0, concat_axis=0, tiled=True)  58.1 us
    all_to_all x1, waiting for transfers between devices, per_device(): lax.all_to_all(back_rows, 'sp', split_axis=0, concat_axis=0, tiled=True)  42.6 us
    all_to_all x1, waiting for transfers between devices, per_device(): lax.all_to_all(inputs, 'sp', split_axis=0, concat_axis=0, tiled=True)  35.9 us
    reduce_scatter x1, waiting for transfers between devices, per_device(): lax.psum_scatter(partial_rows, 'tp', scatter_dimension=0, tiled=True)  13.4 us
    all_gather x1, waiting for transfers between devices, per_device(): grad_tokens = lax.all_gather(mid_grad, 'tp', axis=0, tiled=True)  10.7 us
  transfers between devices with their start and end apart: 9, of which 6 were waited for; matrix products, arithmetic and copies ran while one was open for 10% of the time, Pallas kernels for 0%

commit v1 on v0

--- a/solution.py
+++ b/solution.py
@@ -24,22 +24,72 @@
     return logistic * (1.0 + pre_act * (1.0 - logistic))
 
 
-def assign_slots(routes, experts, capacity):
+def slot_targets(routes, experts, capacity):
     token_count, per_token = routes.shape
     flattened = routes.reshape(token_count * per_token)
-    one_hot = (flattened[:, None] == jnp.arange(experts, dtype=jnp.int32)[None, :]).astype(
-        jnp.int32
-    )
-    earlier = jnp.cumsum(one_hot, axis=0) - one_hot
-    positions = jnp.sum(earlier * one_hot, axis=1)
-    target = flattened * capacity + positions
+    one_hot = flattened[:, None] == jnp.arange(experts, dtype=jnp.int32)[None, :]
     route_ids = jnp.arange(token_count * per_token, dtype=jnp.int32)
-    slot_owner = (
-        jnp.full((experts * capacity,), token_count * per_token, jnp.int32)
-        .at[target]
-        .set(route_ids)
-    )
-    return (slot_owner, target)
+    before = (route_ids[None, :] < route_ids[:, None]).astype(jnp.bfloat16)
+    earlier = jnp.dot(before, one_hot.astype(jnp.bfloat16), preferred_element_type=jnp.float32)
+    positions = jnp.sum(jnp.where(one_hot, earlier, 0.0), axis=1).astype(jnp.int32)
+    return (flattened * capacity + positions).reshape(token_count, per_token)
+
+
+def halving_orders(count):
+    bits = count.bit_length() - 1
+    turned = min(bits, 3)
+    return [
+        [(start + step) % turned for step in range(turned)] + list(range(turned, bits))
+        for start in range(turned)
+    ]
+
+
+def column_groups(columns, groups):
+    lanes = 128
+    tiles = columns // lanes
+    sizes = [tiles // groups + (1 if g < tiles % groups else 0) for g in range(groups)]
+    starts = [sum(sizes[:g]) * lanes for g in range(groups)]
+    return [(start, size * lanes) for start, size in zip(starts, sizes) if size]
+
+
+def picked(block, place, dim):
+    return lax.dynamic_index_in_dim(block, place, dim, keepdims=False)
+
+
+def token_product(rows, columns):
+    flat = rows.reshape(rows.shape[0], -1)
+    return lax.dot_general(
+        flat, columns, (((0,), (0,)), ((), ())), preferred_element_type=jnp.float32
+    ).reshape(rows.shape[1:] + (columns.shape[1],))
+
+
+def reduced_products(rows, columns, axis):
+    count = lax.axis_size(axis)
+    tokens, width = rows.shape
+    bits = count.bit_length() - 1
+    own = lax.axis_index(axis)
+    cut = rows.reshape((tokens,) + (2,) * bits + (width // count,))
+    orders = halving_orders(count)
+    pieces = []
+    for order, (start, size) in zip(orders, column_groups(columns.shape[1], len(orders))):
+        group = lax.slice_in_dim(columns, start, start + size, axis=1)
+        left = list(range(bits - 1, -1, -1))
+        total = None
+        for bit in order:
+            mine = (own >> bit) & 1
+            dim = left.index(bit)
+            if total is None:
+                outgoing = token_product(picked(cut, 1 - mine, dim + 1), group)
+                kept = token_product(picked(cut, mine, dim + 1), group)
+            else:
+                outgoing = picked(total, 1 - mine, dim)
+                kept = picked(total, mine, dim)
+            pairs = [(i, i ^ (1 << bit)) for i in range(count)]
+            arrived = lax.ppermute(outgoing.astype(jnp.bfloat16), axis, pairs)
+            total = kept + arrived.astype(jnp.float32)
+            left.pop(dim)
+        pieces.append(total)
+    return jnp.concatenate(pieces, axis=1)
 
 
 def expert_backward(inputs, routed, gate_mat, up_mat, down_mat):
@@ -88,14 +138,14 @@
     channel_sum, squares = lax.psum(
         (jnp.sum(values, axis=1), jnp.sum(values * values, axis=1)), "tp"
     )
-    slot_owner, target = assign_slots(routes, experts, capacity)
-    token_of = slot_owner // per_token
-    inputs = jnp.take(mid_rows, token_of, axis=0, mode="fill", fill_value=0)
-    route_scale = jnp.take(
-        route_weight.reshape(token_count * per_token), slot_owner, mode="fill", fill_value=0.0
-    )
-    cot_rows = jnp.take(cotangent, token_of, axis=0, mode="fill", fill_value=0)
-    routed = (route_scale[:, None] * cot_rows.astype(jnp.float32)).astype(jnp.bfloat16)
+    target = slot_targets(routes, experts, capacity)
+    slot_ids = jnp.arange(experts * capacity, dtype=jnp.int32)
+    holds = slot_ids[:, None, None] == target[None, :, :]
+    chosen = jnp.any(holds, axis=2).astype(jnp.bfloat16)
+    route_scale = jnp.sum(jnp.where(holds, route_weight[None, :, :], 0.0), axis=(1, 2))
+    inputs = jnp.dot(chosen, mid_rows, preferred_element_type=jnp.float32).astype(jnp.bfloat16)
+    cot_rows = jnp.dot(chosen, cotangent, preferred_element_type=jnp.float32)
+    routed = (route_scale[:, None] * cot_rows).astype(jnp.bfloat16)
     inputs = inputs.reshape(sp_count, local_experts, capacity, model_width)
     routed = routed.reshape(sp_count, local_experts, capacity, model_width)
     got_in = lax.all_to_all(inputs, "sp", split_axis=0, concat_axis=0, tiled=True)
@@ -114,9 +164,8 @@
     returned = lax.all_to_all(back_rows, "sp", split_axis=0, concat_axis=0, tiled=True)
     gate_grad, up_grad, down_grad = (gate_part, up_part, down_part)
     back_all = returned.reshape(experts * capacity, model_width)
-    route_rows = jnp.take(back_all, target, axis=0)
-    route_sum = jnp.sum(
-        route_rows.astype(jnp.float32).reshape(token_count, per_token, model_width), axis=1
+    route_sum = lax.dot_general(
+        chosen, back_all, (((0,), (0,)), ((), ())), preferred_element_type=jnp.float32
     )
     mid_grad = (cotangent.astype(jnp.float32) + route_sum).astype(jnp.bfloat16)
     average = channel_sum / model_width
@@ -126,14 +175,7 @@
     scaled = normed * norm_gain
     activated = jax.nn.silu(scaled).astype(jnp.bfloat16)
     grad_tokens = lax.all_gather(mid_grad, "tp", axis=0, tiled=True)
-    proj_grad = lax.psum_scatter(
-        lax.dot_general(
-            grad_tokens, activated, (((0,), (0,)), ((), ())), preferred_element_type=jnp.float32
-        ),
-        "sp",
-        scatter_dimension=0,
-        tiled=True,
-    )
+    proj_grad = reduced_products(grad_tokens, activated, "sp")
     act_grad = lax.dot_general(
         grad_tokens, out_weight, (((1,), (1,)), ((), ())), preferred_element_type=jnp.float32
     )

time: 441 us -> 323 us (0.73)
  waiting for transfers between devices: 251 us -> 118 us
  starting transfers between devices: 21.1 us -> 37.7 us
  matrix products: 49.5 us -> 60.7 us
  other arithmetic: 17.8 us -> 10.4 us
    reduce_scatter x1 -> x0, waiting for transfers between devices: 146 us -> none  [per_device(): lax.psum_scatter(lax.dot_general(grad_tokens, activated, (((0,), (0,)), (...]
    ppermute x0 -> x12, starting transfers between devices: none -> 18 us  [reduced_products(): arrived = lax.ppermute(outgoing.astype(jnp.bfloat16), axis, pairs)]
    gather x5 -> x0, local copies, waits for them, and re-layouts: 17.2 us -> none  [the longest x1 6.34 us: per_device(): inputs = jnp.take(mid_rows, token_of, axis=0, mode='fill', fill_value=0)]
    ppermute x0 -> x12, waiting for transfers between devices: none -> 14.4 us  [reduced_products(): arrived = lax.ppermute(outgoing.astype(jnp.bfloat16), axis, pairs)]
    all_to_all x1, waiting for transfers between devices: 42.6 us -> 31.3 us  [per_device(): lax.all_to_all(back_rows, 'sp', split_axis=0, concat_axis=0, tiled=True)]
    ppermute x1, waiting for transfers between devices: 0.01 us -> 9.5 us  [extended(): lax.ppermute(lax.slice_in_dim(block, block.shape[dim] - width, None, axis...]
    dot_general x1 -> x10, matrix products: 6.05 us -> 13.6 us  [the longest x6 8.35 us: token_product(): lax.dot_general(flat, columns, (((0,), (0,)), ((), ())), preferred_elemen...]
    all_to_all x1, waiting for transfers between devices: 35.9 us -> 42.9 us  [per_device(): lax.all_to_all(inputs, 'sp', split_axis=0, concat_axis=0, tiled=True)]
  transfers between devices with their start and end apart: 9 -> 20, of which waited for: 6 -> 15; matrix products, arithmetic and copies ran while one was open for 10% -> 17% of each run, Pallas kernels for 0% -> 0%
where the time goes in v1:
time: 323 us
  waiting for transfers between devices  118 us (37%)
  blocking collectives  63.3 us (20%)
  matrix products  60.7 us (19%)
  starting transfers between devices  37.7 us (12%)
  local copies, waits for them, and re-layouts  18.5 us (6%)
  between operations  14.3 us (4%)
  other arithmetic  10.4 us (3%)
    all_to_all x1, blocking collectives, per_device(): lax.all_to_all(routed, 'sp', split_axis=0, concat_axis=0, tiled=True)  58.1 us
    all_to_all x1, waiting for transfers between devices, per_device(): lax.all_to_all(inputs, 'sp', split_axis=0, concat_axis=0, tiled=True)  42.9 us
    all_to_all x1, waiting for transfers between devices, per_device(): lax.all_to_all(back_rows, 'sp', split_axis=0, concat_axis=0, tiled=True)  31.3 us
    ppermute x12, starting transfers between devices, reduced_products(): arrived = lax.ppermute(outgoing.astype(jnp.bfloat16), axis, pairs)  18 us
    ppermute x12, waiting for transfers between devices, reduced_products(): arrived = lax.ppermute(outgoing.astype(jnp.bfloat16), axis, pairs)  14.4 us
    reduce_scatter x1, waiting for transfers between devices, per_device(): lax.psum_scatter(partial_rows, 'tp', scatter_dimension=0, tiled=True)  9.54 us
    ppermute x1, waiting for transfers between devices, extended(): lax.ppermute(lax.slice_in_dim(block, block.shape[dim] - width, None, axis...  9.5 us
    all_to_all x1, starting transfers between devices, per_device(): lax.all_to_all(inputs, 'sp', split_axis=0, concat_axis=0, tiled=True)  8.53 us
  transfers between devices with their start and end apart: 20, of which 15 were waited for; matrix products, arithmetic and copies ran while one was open for 17% of the time, Pallas kernels for 0%

profile of v1, /device:TPU:0, one launch (start us, length us, event | category | flops | bytes accessed | tf_op | source)
XLA Modules:
  0.0 322.6 jit_solution(7292771900348108206)
XLA Ops:
  9.4 3.1 convolution_convert_fusion
  12.5 8.5 %all-to-all-start = ((bf16[16,1,32,2048]{3,2,1,0:T(8,128)(2,1)}), bf16[16,1,32,2048]{3,2,1,0:T(8,128)(2,1)}, u32[]{:S(2)}, u32[]{:S(2)}) async-start(bf16[16,1,32,2048]{3,2,1,0:T(8,128)(2,1)} %bitcast.275), calls=%async_computation | async-start | bytes 4194304 | tf_op jit(solution)/shard_map/all_to_all | solution.py:151
  21.3 42.9 %all-to-all-done = bf16[16,1,32,2048]{3,2,1,0:T(8,128)(2,1)} async-done(((bf16[16,1,32,2048]{3,2,1,0:T(8,128)(2,1)}), bf16[16,1,32,2048]{3,2,1,0:T(8,128)(2,1)}, u32[]{:S(2)}, u32[]{:S(2)}) %all-to-all-start) | async-done | bytes 2097184 | tf_op jit(solution)/shard_map/all_to_all | solution.py:151
  64.9 58.1 %all_to_all.15 = bf16[16,1,32,2048]{3,2,1,0:T(8,128)(2,1)} all-to-all(bf16[16,1,32,2048]{3,2,1,0:T(8,128)(2,1)S(1)} %bitcast.276), channel_id=1, replica_groups=mesh['sp'=16,'tp'=2] {'sp'}, dimensions={0} | all-to-all | bytes 4194304 | tf_op jit(solution)/shard_map/all_to_all | solution.py:152
  123.3 6.0 %fusion.9 = f32[32,32,512]{2,1,0:T(8,128)} fusion(bf16[32,1,32,2048]{3,2,1,0:T(8,128)(2,1)} %all-gather.4.cloned.1.call-done, bf16[1,2048,512]{2,1,0:T(8,128)(2,1)S(1)} %copy-done), kind=kOutput, calls=%fused_computation.10 | convolution fusion | flops 2147483648 | bytes 8388608 | tf_op jit(solution)/shard_map/secd,edf->secf/dot_general | solution.py:96
  129.3 3.7 %fusion.11 = f32[32,32,512]{2,1,0:T(8,128)} fusion(bf16[32,1,32,2048]{3,2,1,0:T(8,128)(2,1)S(1)} %copy-done.11, bf16[1,2048,512]{2,1,0:T(8,128)(2,1)S(1)} %copy-done.13), kind=kOutput, calls=%fused_computation.12 | convolution fusion | flops 2147483648 | bytes 8388608 | tf_op jit(solution)/shard_map/secd,edf->secf/dot_general | solution.py:97
  133.0 2.2 all-gather.6.cloned.1.call-done
  135.2 7.1 %fusion.58 = (bf16[32,32,512]{2,1,0:T(8,128)(2,1)S(1)}, bf16[32,1,32,512]{3,2,0,1:T(8,128)(2,1)S(1)}) fusion(f32[32,32,512]{2,1,0:T(8,128)} %fusion.9, f32[32,32,512]{2,1,0:T(8,128)} %fusion.11, bf16[1,512,2048]{2,1,0:T(8,128)(2,1)} %param.21, bf16[32,1,32,2048]{3,2,1,0:T(8,128)(2,1)} %all-gather.6.cloned.1.call-done), kind=kOutput, calls=%fused_computation.100 | convolution fusion | flops 2154299392 | bytes 12582912 | tf_op jit(solution)/shard_map/secd,efd->secf/dot_general | solution.py:101
  142.3 2.4 fusion.32
  144.7 4.4 %fusion = bf16[32,1,32,2048]{3,2,0,1:T(8,128)(2,1)} fusion(f32[32,32,2048]{2,1,0:T(8,128)S(1)} %fusion.32, bf16[32,32,512]{2,1,0:T(8,128)(2,1)S(1)} %get-tuple-element.13, bf16[1,2048,512]{2,1,0:T(8,128)(2,1)S(1)} %copy-done.14), kind=kOutput, calls=%fused_computation.1 | convolution fusion | flops 2151677952 | bytes 15728640 | tf_op jit(solution)/shard_map/secf,edf->secd/dot_general | solution.py:113
  150.4 2.5 all-reduce.1
  152.9 9.5 %reduce-scatter.2.cloned.1.call-done = bf16[16,1,32,2048]{3,2,0,1:T(8,128)(2,1)} async-done(((bf16[32,1,32,2048]{3,2,0,1:T(8,128)(2,1)}), bf16[16,1,32,2048]{3,2,0,1:T(8,128)(2,1)}) %reduce-scatter.2.cloned.1.call-update) | async-done | bytes 2097168 | tf_op jit(solution)/shard_map/reduce_scatter | solution.py:160
  162.5 6.9 %all-to-all-start.2 = ((bf16[16,1,32,2048]{3,2,1,0:T(8,128)(2,1)}), bf16[16,1,32,2048]{3,2,1,0:T(8,128)(2,1)S(1)}, u32[]{:S(2)}, u32[]{:S(2)}) async-start(bf16[16,1,32,2048]{3,2,1,0:T(8,128)(2,1)} %bitcast.277), calls=%async_computation.3 | async-start | bytes 4194304 | tf_op jit(solution)/shard_map/all_to_all | solution.py:164
  169.7 7.0 %fusion.13 = f32[1,2048,512]{2,1,0:T(8,128)} fusion(bf16[32,1,32,2048]{3,2,1,0:T(8,128)(2,1)} %all-gather.4.cloned.1.call-done, bf16[32,1,32,512]{3,2,0,1:T(8,128)(2,1)} %copy-done.16), kind=kOutput, calls=%fused_computation.15 | convolution fusion | flops 2147483648 | bytes 9437184 | tf_op jit(solution)/shard_map/secd,secf->edf/dot_general | solution.py:104
  176.7 4.6 %fusion.19 = f32[1,512,2048]{2,1,0:T(8,128)} fusion(bf16[32,1,32,2048]{3,2,1,0:T(8,128)(2,1)S(1)} %copy-done.12, f32[32,32,512]{2,1,0:T(8,128)S(1)} %copy-done.18, f32[32,32,512]{2,1,0:T(8,128)S(1)} %copy-done.17), kind=kOutput, calls=%fused_computation.17 | convolution fusion | flops 2150629376 | bytes 12582912 | tf_op jit(solution)/shard_map/secf,secd->efd/dot_general | solution.py:100
  181.3 31.3 %all-to-all-done.2 = bf16[16,1,32,2048]{3,2,1,0:T(8,128)(2,1)S(1)} async-done(((bf16[16,1,32,2048]{3,2,1,0:T(8,128)(2,1)}), bf16[16,1,32,2048]{3,2,1,0:T(8,128)(2,1)S(1)}, u32[]{:S(2)}, u32[]{:S(2)}) %all-to-all-start.2) | async-done | bytes 2097184 | tf_op jit(solution)/shard_map/all_to_all | solution.py:164
  214.0 6.9 %fusion.16 = f32[1,2048,512]{2,1,0:T(8,128)} fusion(bf16[32,32,512]{2,1,0:T(8,128)(2,1)} %copy-done.15, bf16[32,1,32,2048]{3,2,1,0:T(8,128)(2,1)} %all-gather.4.cloned.1.call-done), kind=kOutput, calls=%fused_computation.16 | convolution fusion | flops 2147483648 | bytes 9437184 | tf_op jit(solution)/shard_map/secd,secf->edf/dot_general | solution.py:105
  220.8 6.9 %all-gather.8.cloned.1.call-done = bf16[256,2048]{1,0:T(8,128)(2,1)} async-done(((bf16[128,2048]{1,0:T(8,128)(2,1)}), bf16[256,2048]{1,0:T(8,128)(2,1)}) %all-gather.8.cloned.1.call-update) | async-done | bytes 1048592 | tf_op jit(solution)/shard_map/all_gather | solution.py:177
  227.7 1.8 reshape.137
  231.0 5.1 %fusion.118 = (f32[256]{0:T(256)S(1)}, f32[256]{0:T(256)S(1)}, f32[256,1024]{1,0:T(8,128)}) fusion(f32[256]{0:T(256)S(1)} %get-tuple-element.57, f32[256]{0:T(256)S(1)} %get-tuple-element.56, bf16[256,1024]{1,0:T(8,128)(2,1)S(1)} %copy-done.3, f32[1024]{0:T(1024)S(1)} %copy-done.9, bf16[256,2048]{1,0:T(8,128)(2,1)} %all-gather.8.cloned.1.call-done, ...), kind=kOutput, calls=%fused_computation.211 | convolution fusion | flops 1077935616 | bytes 6823936 | tf_op jit(solution)/shard_map/dot_general | solution.py:179
  236.1 2.7 all-reduce
  238.8 2.6 fusion.56
  242.5 1.8 collective-permute-start.8
  244.2 1.4 copy.115
  245.6 1.5 constant_dynamic-slice_fusion.3
  247.9 1.3 convolution_convert_fusion.1
  249.2 1.5 collective-permute-start.4
  250.7 3.1 constant_dynamic-slice_fusion.5
  253.8 1.4 copy.113
  255.2 2.3 copy.108
  257.6 1.3 convolution_convert_fusion.2
  258.9 1.5 collective-permute-start
  260.4 2.0 copy.107
  262.4 2.5 collective-permute-start.13
  264.8 1.3 collective-permute-start.12
  266.1 1.5 convert_add_fusion.2
  267.7 2.7 collective-permute-start.9
  270.4 9.5 %collective-permute-done.13 = bf16[15,1024]{1,0:T(8,128)(2,1)S(1)} collective-permute-done((bf16[15,1024]{1,0:T(8,128)(2,1)S(1)}, bf16[15,1024]{1,0:T(8,128)(2,1)S(1)}, u32[]{:S(2)}, u32[]{:S(2)}) %collective-permute-start.13) | collective-permute-done | bytes 30752 | tf_op jit(solution)/shard_map/ppermute | solution.py:14
  280.9 5.4 %add_convert_fusion.1 = bf16[256,1024]{1,0:T(8,128)(2,1)} fusion(bf16[256,1024]{1,0:T(8,128)(2,1)S(1)} %copy-done.2, bf16[15,1024]{1,0:T(8,128)(2,1)S(1)} %collective-permute-done.13, bf16[15,1024]{1,0:T(8,128)(2,1)S(1)} %collective-permute-done.12, f32[1024]{0:T(1024)S(1)} %bitcast.288, f32[1024]{0:T(1024)S(1)} %bitcast.289, f32[1024]{0:T(1024)S(1)} %bitcast.291, ...), kind=kLoop, calls=%fused_computation.104 | loop fusion | flops 47972352 | bytes 1236992 | tf_op jit(solution)/shard_map/convert_element_type | solution.py:196
  287.3 1.6 convert_add_fusion
  289.5 1.6 convert_add_fusion.1
  291.5 2.7 collective-permute-start.11
  295.0 2.3 collective-permute-done.11
  298.6 1.7 collective-permute-start.6
  300.4 1.8 collective-permute-done.1
  304.4 2.0 collective-permute-start.7
  306.4 2.7 collective-permute-done.2
  310.6 4.6 %collective-permute-done.3 = bf16[128,384]{1,0:T(8,128)(2,1)S(1)} collective-permute-done((bf16[128,384]{1,0:T(8,128)(2,1)S(1)}, bf16[128,384]{1,0:T(8,128)(2,1)S(1)}, u32[]{:S(2)}, u32[]{:S(2)}) %collective-permute-start.3) | collective-permute-done | bytes 98336 | tf_op jit(solution)/shard_map/ppermute | solution.py:88
  (101 shorter events, 19.4 us)
Async XLA Ops:
  7.2 116.1 %copy-start = (bf16[1,2048,512]{2,1,0:T(8,128)(2,1)S(1)}, bf16[1,2048,512]{2,1,0:T(8,128)(2,1)}, u32[]{:S(2)}) copy-start(bf16[1,2048,512]{2,1,0:T(8,128)(2,1)} %param.19) | copy-start | bytes 6291460
  12.5 8.6 %copy-start.10 = (f32[128,2]{0,1:T(2,128)S(1)}, f32[128,2]{0,1:T(2,128)}, u32[]{:S(2)}) copy-start(f32[128,2]{0,1:T(2,128)} %param.14) | copy-start | bytes 3076
  12.5 51.6 %all-to-all-start = ((bf16[16,1,32,2048]{3,2,1,0:T(8,128)(2,1)}), bf16[16,1,32,2048]{3,2,1,0:T(8,128)(2,1)}, u32[]{:S(2)}, u32[]{:S(2)}) async-start(bf16[16,1,32,2048]{3,2,1,0:T(8,128)(2,1)} %bitcast.275), calls=%async_computation | async-start | bytes 4194304 | tf_op jit(solution)/shard_map/all_to_all | solution.py:151
  21.0 43.2 %copy-start.4 = (bf16[128,2048]{1,0:T(8,128)(2,1)S(1)}, bf16[128,2048]{1,0:T(8,128)(2,1)}, u32[]{:S(2)}) copy-start(bf16[128,2048]{1,0:T(8,128)(2,1)} %param.12) | copy-start | bytes 1572868
  21.1 102.2 %all-gather.4.cloned.1.call-start = ((), (), s32[]{:S(2)}) async-start(), calls=%async_computation.4 | async-start | bytes 6291456 | tf_op jit(solution)/shard_map/all_gather | solution.py:153
  64.2 71.0 %all-gather.6.cloned.1.call-start = ((), (), s32[]{:S(2)}) async-start(), calls=%async_computation.5 | async-start | bytes 6291456 | tf_op jit(solution)/shard_map/all_gather | solution.py:154
  123.0 39.4 %reduce-scatter.2.cloned.1.call-start = ((), (), s32[]{:S(2)}) async-start(), calls=%async_computation.6 | async-start | bytes 6291456 | tf_op jit(solution)/shard_map/reduce_scatter | solution.py:160
  123.3 6.0 %copy-start.11 = (bf16[32,1,32,2048]{3,2,1,0:T(8,128)(2,1)S(1)}, bf16[32,1,32,2048]{3,2,1,0:T(8,128)(2,1)}, u32[]{:S(2)}) copy-start(bf16[32,1,32,2048]{3,2,1,0:T(8,128)(2,1)} %all-gather.4.cloned.1.call-done) | copy-start | bytes 12582916
  123.3 6.0 %copy-start.13 = (bf16[1,2048,512]{2,1,0:T(8,128)(2,1)S(1)}, bf16[1,2048,512]{2,1,0:T(8,128)(2,1)}, u32[]{:S(2)}) copy-start(bf16[1,2048,512]{2,1,0:T(8,128)(2,1)} %param.20) | copy-start | bytes 6291460
  142.2 2.4 copy-start.16
  142.2 2.4 copy-start.15
  142.3 2.4 copy-start.14
  149.1 1.0 copy-start.3
  149.1 3.8 %copy-start.8 = (f32[31,1024]{1,0:T(8,128)S(1)}, f32[31,1024]{1,0:T(8,128)}, u32[]{:S(2)}) copy-start(f32[31,1024]{1,0:T(8,128)} %param.16) | copy-start | bytes 380932
  162.5 50.2 %all-to-all-start.2 = ((bf16[16,1,32,2048]{3,2,1,0:T(8,128)(2,1)}), bf16[16,1,32,2048]{3,2,1,0:T(8,128)(2,1)S(1)}, u32[]{:S(2)}, u32[]{:S(2)}) async-start(bf16[16,1,32,2048]{3,2,1,0:T(8,128)(2,1)} %bitcast.277), calls=%async_computation.3 | async-start | bytes 4194304 | tf_op jit(solution)/shard_map/all_to_all | solution.py:164
  169.4 58.3 %all-gather.8.cloned.1.call-start = ((), (), s32[]{:S(2)}) async-start(), calls=%async_computation.7 | async-start | bytes 1572864 | tf_op jit(solution)/shard_map/all_gather | solution.py:177
  169.7 7.1 %copy-start.12 = (bf16[32,1,32,2048]{3,2,1,0:T(8,128)(2,1)S(1)}, bf16[32,1,32,2048]{3,2,1,0:T(8,128)(2,1)}, u32[]{:S(2)}) copy-start(bf16[32,1,32,2048]{3,2,1,0:T(8,128)(2,1)} %all-gather.6.cloned.1.call-done) | copy-start | bytes 12582916
  169.7 7.1 %copy-start.17 = (f32[32,32,512]{2,1,0:T(8,128)S(1)}, f32[32,32,512]{2,1,0:T(8,128)}, u32[]{:S(2)}) copy-start(f32[32,32,512]{2,1,0:T(8,128)} %fusion.9) | copy-start | bytes 6291460
  169.7 7.0 %copy-start.18 = (f32[32,32,512]{2,1,0:T(8,128)S(1)}, f32[32,32,512]{2,1,0:T(8,128)}, u32[]{:S(2)}) copy-start(f32[32,32,512]{2,1,0:T(8,128)} %fusion.11) | copy-start | bytes 6291460
  229.5 1.5 copy-start.9
  242.5 23.7 %collective-permute-start.8 = (bf16[2,2,2,128,256]{4,3,0,1,2:T(8,128)(2,1)}, bf16[2,2,2,128,256]{4,3,0,1,2:T(8,128)(2,1)}, u32[]{:S(2)}, u32[]{:S(2)}) collective-permute-start(bf16[2,2,2,128,256]{4,3,0,1,2:T(8,128)(2,1)} %convolution_convert_fusion.3), channel_id=1, source_target_pairs={{0,8},{2,10},{4,12},{6,14},{8,0},{10,2},{12,4},{14,6},{16,24},{18,... | collective-permute-start | bytes 1572872 | tf_op jit(solution)/shard_map/ppermute | solution.py:88
  249.2 4.6 %copy-start.7 = (bf16[256,2,2,1,2,128]{5,4,3,2,1,0:T(2,128)(2,1)S(1)}, bf16[256,2,2,1,2,128]{5,4,3,2,1,0:T(2,128)(2,1)}, u32[]{:S(2)}) copy-start(bf16[256,2,2,1,2,128]{5,4,3,2,1,0:T(2,128)(2,1)} %get-tuple-element.17) | copy-start | bytes 1572868
  249.2 38.1 %collective-permute-start.4 = (bf16[2,2,2,128,384]{4,3,0,2,1:T(8,128)(2,1)}, bf16[2,2,2,128,384]{4,3,0,2,1:T(8,128)(2,1)}, u32[]{:S(2)}, u32[]{:S(2)}) collective-permute-start(bf16[2,2,2,128,384]{4,3,0,2,1:T(8,128)(2,1)} %convolution_convert_fusion.1), channel_id=1, source_target_pairs={{0,4},{2,6},{4,0},{6,2},{8,12},{10,14},{12,8},{14,10},{16,20},{18,... | collective-permute-start | bytes 2359304 | tf_op jit(solution)/shard_map/ppermute | solution.py:88
  257.6 4.8 %copy-start.2 = (bf16[256,1024]{1,0:T(8,128)(2,1)S(1)}, bf16[256,1024]{1,0:T(8,128)(2,1)}, u32[]{:S(2)}) copy-start(bf16[256,1024]{1,0:T(8,128)(2,1)} %get-tuple-element.21) | copy-start | bytes 1572868
  258.9 30.6 %collective-permute-start = (bf16[2,2,2,128,384]{4,3,2,1,0:T(8,128)(2,1)}, bf16[2,2,2,128,384]{4,3,2,1,0:T(8,128)(2,1)}, u32[]{:S(2)}, u32[]{:S(2)}) collective-permute-start(bf16[2,2,2,128,384]{4,3,2,1,0:T(8,128)(2,1)} %convolution_convert_fusion.2), channel_id=1, source_target_pairs={{0,2},{2,0},{4,6},{6,4},{8,10},{10,8},{12,14},{14,12},{16,18},{18,... | collective-permute-start | bytes 2359304 | tf_op jit(solution)/shard_map/ppermute | solution.py:88
  262.4 17.5 %collective-permute-start.13 = (bf16[15,1024]{1,0:T(8,128)(2,1)S(1)}, bf16[15,1024]{1,0:T(8,128)(2,1)S(1)}, u32[]{:S(2)}, u32[]{:S(2)}) collective-permute-start(bf16[15,1024]{1,0:T(8,128)(2,1)S(1)} %get-tuple-element.24), channel_id=1, source_target_pairs={{0,2},{2,4},{4,6},{6,8},{8,10},{10,12},{12,14},{14,16},{16,18},{18... | collective-permute-start | bytes 92168 | tf_op jit(solution)/shard_map/ppermute | solution.py:14
  264.8 16.1 %collective-permute-start.12 = (bf16[15,1024]{1,0:T(8,128)(2,1)S(1)}, bf16[15,1024]{1,0:T(8,128)(2,1)S(1)}, u32[]{:S(2)}, u32[]{:S(2)}) collective-permute-start(bf16[15,1024]{1,0:T(8,128)(2,1)S(1)} %get-tuple-element.23), channel_id=1, source_target_pairs={{2,0},{4,2},{6,4},{8,6},{10,8},{12,10},{14,12},{16,14},{18,16},{20... | collective-permute-start | bytes 92168 | tf_op jit(solution)/shard_map/ppermute | solution.py:17
  267.6 19.6 %copy-start.6 = (bf16[256,2,2,1,2,128]{0,5,1,4,2,3:T(8,128)(2,1)S(1)}, bf16[256,2,2,1,2,128]{0,5,1,4,2,3:T(8,128)(2,1)}, u32[]{:S(2)}) copy-start(bf16[256,2,2,1,2,128]{0,5,1,4,2,3:T(8,128)(2,1)} %copy.113) | copy-start | bytes 1572868
  267.7 18.6 %collective-permute-start.9 = (bf16[2,2,128,256]{3,2,0,1:T(8,128)(2,1)S(1)}, bf16[2,2,128,256]{3,2,0,1:T(8,128)(2,1)S(1)}, u32[]{:S(2)}, u32[]{:S(2)}) collective-permute-start(bf16[2,2,128,256]{3,2,0,1:T(8,128)(2,1)S(1)} %fusion.109), channel_id=1, source_target_pairs={{0,2},{2,0},{4,6},{6,4},{8,10},{10,8},{12,14},{14,12},{16,18},{18,... | collective-permute-start | bytes 786440 | tf_op jit(solution)/shard_map/ppermute | solution.py:88
  286.4 3.1 copy-start.5
  286.4 5.0 %collective-permute-start.10 = (bf16[2,128,256]{2,1,0:T(8,128)(2,1)S(1)}, bf16[2,128,256]{2,1,0:T(8,128)(2,1)S(1)}, u32[]{:S(2)}, u32[]{:S(2)}) collective-permute-start(bf16[2,128,256]{2,1,0:T(8,128)(2,1)S(1)} %fusion.112), channel_id=1, source_target_pairs={{0,4},{2,6},{4,0},{6,2},{8,12},{10,14},{12,8},{14,10},{16,20},{18,... | collective-permute-start | bytes 393224 | tf_op jit(solution)/shard_map/ppermute | solution.py:88
  288.9 9.6 %collective-permute-start.5 = (bf16[2,2,128,384]{3,2,0,1:T(8,128)(2,1)S(1)}, bf16[2,2,128,384]{3,2,0,1:T(8,128)(2,1)S(1)}, u32[]{:S(2)}, u32[]{:S(2)}) collective-permute-start(bf16[2,2,128,384]{3,2,0,1:T(8,128)(2,1)S(1)} %fusion.108), channel_id=1, source_target_pairs={{0,8},{2,10},{4,12},{6,14},{8,0},{10,2},{12,4},{14,6},{16,24},{18,... | collective-permute-start | bytes 1179656 | tf_op jit(solution)/shard_map/ppermute | solution.py:88
  291.5 5.8 %collective-permute-start.11 = (bf16[128,256]{1,0:T(8,128)(2,1)S(1)}, bf16[128,256]{1,0:T(8,128)(2,1)S(1)}, u32[]{:S(2)}, u32[]{:S(2)}) collective-permute-start(bf16[128,256]{1,0:T(8,128)(2,1)S(1)} %fusion.115), channel_id=1, source_target_pairs={{0,16},{2,18},{4,20},{6,22},{8,24},{10,26},{12,28},{14,30},{16,0},... | collective-permute-start | bytes 196616 | tf_op jit(solution)/shard_map/ppermute | solution.py:88
  294.3 7.8 %collective-permute-start.1 = (bf16[2,2,128,384]{3,2,1,0:T(8,128)(2,1)S(1)}, bf16[2,2,128,384]{3,2,1,0:T(8,128)(2,1)S(1)}, u32[]{:S(2)}, u32[]{:S(2)}) collective-permute-start(bf16[2,2,128,384]{3,2,1,0:T(8,128)(2,1)S(1)} %fusion.107), channel_id=1, source_target_pairs={{0,4},{2,6},{4,0},{6,2},{8,12},{10,14},{12,8},{14,10},{16,20},{18,... | collective-permute-start | bytes 1179656 | tf_op jit(solution)/shard_map/ppermute | solution.py:88
  298.6 5.7 %collective-permute-start.6 = (bf16[2,128,384]{2,1,0:T(8,128)(2,1)S(1)}, bf16[2,128,384]{2,1,0:T(8,128)(2,1)S(1)}, u32[]{:S(2)}, u32[]{:S(2)}) collective-permute-start(bf16[2,128,384]{2,1,0:T(8,128)(2,1)S(1)} %fusion.111), channel_id=1, source_target_pairs={{0,2},{2,0},{4,6},{6,4},{8,10},{10,8},{12,14},{14,12},{16,18},{18,... | collective-permute-start | bytes 589832 | tf_op jit(solution)/shard_map/ppermute | solution.py:88
  302.2 13.8 %copy-start.1 = (bf16[1,2048,512]{2,1,0:T(8,128)(2,1)S(1)}, bf16[1,2048,512]{2,1,0:T(8,128)(2,1)}, u32[]{:S(2)}) copy-start(bf16[1,2048,512]{2,1,0:T(8,128)(2,1)} %param.19) | copy-start | bytes 6291460
  302.3 6.9 %collective-permute-start.2 = (bf16[2,128,384]{2,1,0:T(8,128)(2,1)S(1)}, bf16[2,128,384]{2,1,0:T(8,128)(2,1)S(1)}, u32[]{:S(2)}, u32[]{:S(2)}) collective-permute-start(bf16[2,128,384]{2,1,0:T(8,128)(2,1)S(1)} %fusion.110), channel_id=1, source_target_pairs={{0,8},{2,10},{4,12},{6,14},{8,0},{10,2},{12,4},{14,6},{16,24},{18,... | collective-permute-start | bytes 589832 | tf_op jit(solution)/shard_map/ppermute | solution.py:88
  304.4 6.1 %collective-permute-start.7 = (bf16[128,384]{1,0:T(8,128)(2,1)S(1)}, bf16[128,384]{1,0:T(8,128)(2,1)S(1)}, u32[]{:S(2)}, u32[]{:S(2)}) collective-permute-start(bf16[128,384]{1,0:T(8,128)(2,1)S(1)} %fusion.114), channel_id=1, source_target_pairs={{0,16},{2,18},{4,20},{6,22},{8,24},{10,26},{12,28},{14,30},{16,0},... | collective-permute-start | bytes 294920 | tf_op jit(solution)/shard_map/ppermute | solution.py:88
  309.2 6.0 %collective-permute-start.3 = (bf16[128,384]{1,0:T(8,128)(2,1)S(1)}, bf16[128,384]{1,0:T(8,128)(2,1)S(1)}, u32[]{:S(2)}, u32[]{:S(2)}) collective-permute-start(bf16[128,384]{1,0:T(8,128)(2,1)S(1)} %fusion.113), channel_id=1, source_target_pairs={{0,16},{2,18},{4,20},{6,22},{8,24},{10,26},{12,28},{14,30},{16,0},... | collective-permute-start | bytes 294920 | tf_op jit(solution)/shard_map/ppermute | solution.py:88
Sparse Core Ops, SparseCore 0:
  64.3 18.0 all-gather.3
  123.2 11.9 all-gather.5
  149.2 13.2 reduce-scatter.1
  214.1 13.5 all-gather.7

commit v2 on v1

--- a/solution.py
+++ b/solution.py
@@ -56,34 +56,23 @@
     return lax.dynamic_index_in_dim(block, place, dim, keepdims=False)
 
 
-def token_product(rows, columns):
-    flat = rows.reshape(rows.shape[0], -1)
-    return lax.dot_general(
-        flat, columns, (((0,), (0,)), ((), ())), preferred_element_type=jnp.float32
-    ).reshape(rows.shape[1:] + (columns.shape[1],))
-
-
 def reduced_products(rows, columns, axis):
     count = lax.axis_size(axis)
     tokens, width = rows.shape
     bits = count.bit_length() - 1
     own = lax.axis_index(axis)
-    cut = rows.reshape((tokens,) + (2,) * bits + (width // count,))
+    product = transposed_product(rows, columns).astype(jnp.bfloat16)
+    cut = product.reshape((2,) * bits + (width // count, columns.shape[1]))
     orders = halving_orders(count)
     pieces = []
     for order, (start, size) in zip(orders, column_groups(columns.shape[1], len(orders))):
-        group = lax.slice_in_dim(columns, start, start + size, axis=1)
+        total = lax.slice_in_dim(cut, start, start + size, axis=bits + 1)
         left = list(range(bits - 1, -1, -1))
-        total = None
         for bit in order:
             mine = (own >> bit) & 1
             dim = left.index(bit)
-            if total is None:
-                outgoing = token_product(picked(cut, 1 - mine, dim + 1), group)
-                kept = token_product(picked(cut, mine, dim + 1), group)
-            else:
-                outgoing = picked(total, 1 - mine, dim)
-                kept = picked(total, mine, dim)
+            outgoing = picked(total, 1 - mine, dim)
+            kept = picked(total, mine, dim).astype(jnp.float32)
             pairs = [(i, i ^ (1 << bit)) for i in range(count)]
             arrived = lax.ppermute(outgoing.astype(jnp.bfloat16), axis, pairs)
             total = kept + arrived.astype(jnp.float32)
@@ -92,27 +81,72 @@
     return jnp.concatenate(pieces, axis=1)
 
 
-def expert_backward(inputs, routed, gate_mat, up_mat, down_mat):
-    pre_gate = jnp.einsum("secd,edf->secf", inputs, gate_mat, preferred_element_type=jnp.float32)
-    pre_up = jnp.einsum("secd,edf->secf", inputs, up_mat, preferred_element_type=jnp.float32)
+def row_product(rows, matrix, dim=0):
+    return lax.dot_general(
+        rows, matrix, (((1,), (dim,)), ((), ())), preferred_element_type=jnp.float32
+    )
+
+
+def transposed_product(left, right):
+    return lax.dot_general(
+        left, right, (((0,), (0,)), ((), ())), preferred_element_type=jnp.float32
+    )
+
+
+def from_partner(block, axis):
+    count = lax.axis_size(axis)
+    return [
+        lax.ppermute(block, axis, [(i, (i + step) % count) for i in range(count)])
+        for step in range(1, count)
+    ]
+
+
+def hidden_gradients(pre_gate, pre_up, routed, down_mat):
     gate_act = jax.nn.silu(pre_gate)
     hidden = (gate_act * pre_up).astype(jnp.bfloat16)
-    down_part = jnp.einsum("secf,secd->efd", hidden, routed, preferred_element_type=jnp.float32)
-    hidden_grad = jnp.einsum("secd,efd->secf", routed, down_mat, preferred_element_type=jnp.float32)
+    hidden_grad = row_product(routed, down_mat, 1)
     gate_pre = (hidden_grad * pre_up * silu_grad(pre_gate)).astype(jnp.bfloat16)
     up_pre = (hidden_grad * gate_act).astype(jnp.bfloat16)
-    gate_part = jnp.einsum("secd,secf->edf", inputs, gate_pre, preferred_element_type=jnp.float32)
-    up_part = jnp.einsum("secd,secf->edf", inputs, up_pre, preferred_element_type=jnp.float32)
-    return (gate_pre, up_pre, gate_part, up_part, down_part)
+    return hidden, gate_pre, up_pre
 
 
 def input_part(gate_pre, up_pre, gate_mat, up_mat):
-    first_term = jnp.einsum(
-        "secf,edf->secd", gate_pre, gate_mat, preferred_element_type=jnp.float32
-    )
-    return first_term + jnp.einsum(
-        "secf,edf->secd", up_pre, up_mat, preferred_element_type=jnp.float32
-    )
+    return (row_product(gate_pre, gate_mat, 1) + row_product(up_pre, up_mat, 1)).astype(
+        jnp.bfloat16
+    )
+
+
+def expert_backward(got_in, got_cot, gate_mat, up_mat, down_mat, axis):
+    count = lax.axis_size(axis)
+    all_in = [got_in] + from_partner(got_in, axis)
+    pre = [(row_product(rows, gate_mat), row_product(rows, up_mat)) for rows in all_in]
+    all_cot = [got_cot] + from_partner(got_cot, axis)
+    grads = [hidden_gradients(g, u, c, down_mat) for (g, u), c in zip(pre, all_cot)]
+    back = None
+    for step in range(1, count):
+        part = input_part(grads[step][1], grads[step][2], gate_mat, up_mat)
+        arrived = lax.ppermute(part, axis, [(i, (i - step) % count) for i in range(count)])
+        back = (arrived,) if back is None else back + (arrived,)
+    back_rows = input_part(grads[0][1], grads[0][2], gate_mat, up_mat).astype(jnp.float32)
+    for arrived in back or ():
+        back_rows = back_rows + arrived.astype(jnp.float32)
+    gate_part = sum(transposed_product(x, g[1]) for x, g in zip(all_in, grads))
+    up_part = sum(transposed_product(x, g[2]) for x, g in zip(all_in, grads))
+    down_part = sum(transposed_product(g[0], c) for g, c in zip(grads, all_cot))
+    return gate_part, up_part, down_part, back_rows.astype(jnp.bfloat16)
+
+
+def gathered_rows(block, axis):
+    count = lax.axis_size(axis)
+    own = lax.axis_index(axis)
+    blocks = [block] + from_partner(block, axis)
+    turned = jnp.concatenate(blocks, axis=0)
+    result = turned
+    for place in range(1, count):
+        order = [blocks[(place - i) % count] for i in range(count)]
+        result = jnp.where(own == place, jnp.concatenate(order, axis=0), result)
+    first = [blocks[-i % count] for i in range(count)]
+    return jnp.where(own == 0, jnp.concatenate(first, axis=0), result)
 
 
 def per_device(
@@ -150,19 +184,25 @@
     routed = routed.reshape(sp_count, local_experts, capacity, model_width)
     got_in = lax.all_to_all(inputs, "sp", split_axis=0, concat_axis=0, tiled=True)
     got_cot = lax.all_to_all(routed, "sp", split_axis=0, concat_axis=0, tiled=True)
-    all_in = lax.all_gather(got_in, "tp", axis=0, tiled=True)
-    all_cot = lax.all_gather(got_cot, "tp", axis=0, tiled=True)
-    gate_pre, up_pre, gate_part, up_part, down_part = expert_backward(
-        all_in, all_cot, gate_weight, up_weight, down_weight
-    )
-    partial_rows = input_part(gate_pre, up_pre, gate_weight, up_weight).astype(jnp.bfloat16)
-    back_rows = (
-        lax.psum_scatter(partial_rows, "tp", scatter_dimension=0, tiled=True)
-        .astype(jnp.float32)
-        .astype(jnp.bfloat16)
-    )
+    by_expert = (sp_count, local_experts, capacity, model_width)
+    parts = [
+        expert_backward(
+            got_in[:, e].reshape(sp_count * capacity, model_width),
+            got_cot[:, e].reshape(sp_count * capacity, model_width),
+            gate_weight[e],
+            up_weight[e],
+            down_weight[e],
+            "tp",
+        )
+        for e in range(local_experts)
+    ]
+    gate_grad, up_grad, down_grad = (
+        jnp.stack([part[i] for part in parts], axis=0) for i in range(3)
+    )
+    back_rows = jnp.stack(
+        [part[3].reshape(sp_count, capacity, model_width) for part in parts], axis=1
+    ).reshape(by_expert)
     returned = lax.all_to_all(back_rows, "sp", split_axis=0, concat_axis=0, tiled=True)
-    gate_grad, up_grad, down_grad = (gate_part, up_part, down_part)
     back_all = returned.reshape(experts * capacity, model_width)
     route_sum = lax.dot_general(
         chosen, back_all, (((0,), (0,)), ((), ())), preferred_element_type=jnp.float32
@@ -174,7 +214,7 @@
     normed = (values - average[:, None]) * inv_scale
     scaled = normed * norm_gain
     activated = jax.nn.silu(scaled).astype(jnp.bfloat16)
-    grad_tokens = lax.all_gather(mid_grad, "tp", axis=0, tiled=True)
+    grad_tokens = gathered_rows(mid_grad, "tp")
     proj_grad = reduced_products(grad_tokens, activated, "sp")
     act_grad = lax.dot_general(
         grad_tokens, out_weight, (((1,), (1,)), ((), ())), preferred_element_type=jnp.float32

time: 323 us -> 281 us (0.87)
  blocking collectives: 63.3 us -> 5.29 us
  starting transfers between devices: 37.7 us -> 60.7 us
  waiting for transfers between devices: 118 us -> 137 us
  local copies, waits for them, and re-layouts: 18.5 us -> 2.92 us
  between operations: 14.3 us -> 1.36 us
    all_to_all x1 -> x0, blocking collectives: 58.1 us -> none  [per_device(): lax.all_to_all(routed, 'sp', split_axis=0, concat_axis=0, tiled=True)]
    all_to_all x0 -> x1, waiting for transfers between devices: none -> 42.5 us  [per_device(): lax.all_to_all(routed, 'sp', split_axis=0, concat_axis=0, tiled=True)]
    ppermute x12, waiting for transfers between devices: 14.4 us -> 31.6 us  [reduced_products(): arrived = lax.ppermute(outgoing.astype(jnp.bfloat16), axis, pairs)]
    all_to_all x0 -> x1, starting transfers between devices: none -> 10.1 us  [per_device(): lax.all_to_all(routed, 'sp', split_axis=0, concat_axis=0, tiled=True)]
    reduce_scatter x1 -> x0, waiting for transfers between devices: 9.54 us -> none  [per_device(): lax.psum_scatter(partial_rows, 'tp', scatter_dimension=0, tiled=True)]
    ppermute x1, waiting for transfers between devices: 9.5 us -> 0.01 us  [extended(): lax.ppermute(lax.slice_in_dim(block, block.shape[dim] - width, None, axis...]
    all_gather x3 -> x0, waiting for transfers between devices: 9.05 us -> none  [the longest x1 6.86 us: per_device(): grad_tokens = lax.all_gather(mid_grad, 'tp', axis=0, tiled=True)]
    all_to_all x1, waiting for transfers between devices: 31.3 us -> 22.5 us  [per_device(): lax.all_to_all(back_rows, 'sp', split_axis=0, concat_axis=0, tiled=True)]
  transfers between devices with their start and end apart: 20 -> 21, of which waited for: 15 -> 13; matrix products, arithmetic and copies ran while one was open for 17% -> 21% of each run, Pallas kernels for 0% -> 0%
where the time goes in v2:
time: 281 us; the launch traced here: 280 us
  waiting for transfers between devices  137 us (49%)
  matrix products  62.5 us (22%)
  starting transfers between devices  60.7 us (22%)
  other arithmetic  9.63 us (3%)
  blocking collectives  5.29 us (2%)
  local copies, waits for them, and re-layouts  2.92 us (1%)
    all_to_all x1, waiting for transfers between devices, per_device(): lax.all_to_all(routed, 'sp', split_axis=0, concat_axis=0, tiled=True)  42.5 us
    all_to_all x1, waiting for transfers between devices, per_device(): lax.all_to_all(inputs, 'sp', split_axis=0, concat_axis=0, tiled=True)  40.9 us
    ppermute x12, waiting for transfers between devices, reduced_products(): arrived = lax.ppermute(outgoing.astype(jnp.bfloat16), axis, pairs)  31.6 us
    dot_general x7, matrix products, transposed_product(): lax.dot_general(left, right, (((0,), (0,)), ((), ())), preferred_element_...  29.8 us
    ppermute x12, starting transfers between devices, reduced_products(): arrived = lax.ppermute(outgoing.astype(jnp.bfloat16), axis, pairs)  25.7 us
    dot_general x10, matrix products, row_product(): lax.dot_general(rows, matrix, (((1,), (dim,)), ((), ())), preferred_eleme...  24.2 us
    all_to_all x1, waiting for transfers between devices, per_device(): lax.all_to_all(back_rows, 'sp', split_axis=0, concat_axis=0, tiled=True)  22.5 us
    all_to_all x1, starting transfers between devices, per_device(): lax.all_to_all(routed, 'sp', split_axis=0, concat_axis=0, tiled=True)  10.1 us
  transfers between devices with their start and end apart: 21, of which 13 were waited for; matrix products, arithmetic and copies ran while one was open for 21% of the time, Pallas kernels for 0%

profile of v2, /device:TPU:0, one launch (start us, length us, event | category | flops | bytes accessed | tf_op | source)
XLA Modules:
  0.0 279.9 jit_solution(17925929641335688506)
XLA Ops:
  2.9 3.1 %convolution_convert_fusion.1 = bf16[512,2048]{1,0:T(8,128)(2,1)} fusion(pred[512,128]{1,0:T(8,128)(4,1)S(1)} %fusion.75, bf16[128,2048]{1,0:T(8,128)(2,1)} %param.11), kind=kOutput, calls=%fused_computation.36 | convolution fusion | flops 269484032 | bytes 2686976 | tf_op jit(solution)/shard_map/dot_general | solution.py:180
  6.0 8.5 %all-to-all-start = ((bf16[16,1,32,2048]{3,2,1,0:T(8,128)(2,1)}), bf16[16,1,32,2048]{3,2,1,0:T(8,128)(2,1)}, u32[]{:S(2)}, u32[]{:S(2)}) async-start(bf16[16,1,32,2048]{3,2,1,0:T(8,128)(2,1)} %bitcast.166), calls=%async_computation | async-start | bytes 4194304 | tf_op jit(solution)/shard_map/all_to_all | solution.py:185
  14.7 2.0 multiply_convert_fusion
  16.7 40.9 %all-to-all-done = bf16[16,1,32,2048]{3,2,1,0:T(8,128)(2,1)} async-done(((bf16[16,1,32,2048]{3,2,1,0:T(8,128)(2,1)}), bf16[16,1,32,2048]{3,2,1,0:T(8,128)(2,1)}, u32[]{:S(2)}, u32[]{:S(2)}) %all-to-all-start) | async-done | bytes 2097184 | tf_op jit(solution)/shard_map/all_to_all | solution.py:185
  57.6 10.1 %all-to-all-start.1 = ((bf16[16,1,32,2048]{3,2,1,0:T(8,128)(2,1)}), bf16[16,1,32,2048]{3,2,1,0:T(8,128)(2,1)}, u32[]{:S(2)}, u32[]{:S(2)}) async-start(bf16[16,1,32,2048]{3,2,1,0:T(8,128)(2,1)} %bitcast.165), calls=%async_computation.1 | async-start | bytes 4194304 | tf_op jit(solution)/shard_map/all_to_all | solution.py:186
  67.8 42.5 %all-to-all-done.1 = bf16[16,1,32,2048]{3,2,1,0:T(8,128)(2,1)} async-done(((bf16[16,1,32,2048]{3,2,1,0:T(8,128)(2,1)}), bf16[16,1,32,2048]{3,2,1,0:T(8,128)(2,1)}, u32[]{:S(2)}, u32[]{:S(2)}) %all-to-all-start.1) | async-done | bytes 2097184 | tf_op jit(solution)/shard_map/all_to_all | solution.py:186
  110.3 3.0 %fusion.5 = f32[512,512]{1,0:T(8,128)S(1)} fusion(bf16[512,2048]{1,0:T(8,128)(2,1)} %collective-permute-done, bf16[1,2048,512]{2,1,0:T(8,128)(2,1)S(1)} %copy-done), kind=kOutput, calls=%fused_computation.43 | convolution fusion | flops 1073741824 | bytes 5242880 | tf_op jit(solution)/shard_map/dot_general | solution.py:85
  113.3 3.3 %fusion.11 = f32[512,512]{1,0:T(8,128)S(1)} fusion(bf16[512,2048]{1,0:T(8,128)(2,1)} %collective-permute-done, bf16[1,2048,512]{2,1,0:T(8,128)(2,1)S(1)} %copy-done.3), kind=kOutput, calls=%fused_computation.49 | convolution fusion | flops 1073741824 | bytes 5242880 | tf_op jit(solution)/shard_map/dot_general | solution.py:85
  116.6 1.6 multiply_convert_fusion.3
  119.6 1.3 add_convert_fusion.1
  121.3 2.8 %fusion.7 = f32[512,512]{1,0:T(8,128)S(1)} fusion(bf16[512,2048]{1,0:T(8,128)(2,1)} %bitcast.2, bf16[1,2048,512]{2,1,0:T(8,128)(2,1)S(1)} %copy-done), kind=kOutput, calls=%fused_computation.45 | convolution fusion | flops 1073741824 | bytes 5242880 | tf_op jit(solution)/shard_map/dot_general | solution.py:85
  124.2 3.2 %fusion.13 = f32[512,512]{1,0:T(8,128)S(1)} fusion(bf16[512,2048]{1,0:T(8,128)(2,1)} %bitcast.2, bf16[1,2048,512]{2,1,0:T(8,128)(2,1)S(1)} %copy-done.3), kind=kOutput, calls=%fused_computation.51 | convolution fusion | flops 1073741824 | bytes 5242880 | tf_op jit(solution)/shard_map/dot_general | solution.py:85
  127.4 3.7 %multiply_convert_fusion.4 = (bf16[512,512]{1,0:T(8,128)(2,1)S(1)}, bf16[512,512]{1,0:T(8,128)(2,1)S(1)}) fusion(f32[512,512]{1,0:T(8,128)S(1)} %fusion.7, f32[512,512]{1,0:T(8,128)S(1)} %fusion.13, bf16[512,2048]{1,0:T(8,128)(2,1)} %bitcast.5, bf16[1,512,2048]{2,1,0:T(8,128)(2,1)S(1)} %copy-done.24), kind=kOutput, calls=%fused_computation.90 | convolution fusion | flops 1077149696 | bytes 7340032 | tf_op jit(solution)/shard_map/dot_general | solution.py:85
  132.4 2.7 add_convert_fusion
  135.1 9.8 %all-to-all-start.2 = ((bf16[16,1,32,2048]{3,2,1,0:T(8,128)(2,1)}), bf16[16,1,32,2048]{3,2,1,0:T(8,128)(2,1)S(1)}, u32[]{:S(2)}, u32[]{:S(2)}) async-start(bf16[16,1,32,2048]{3,2,1,0:T(8,128)(2,1)} %bitcast.167), calls=%async_computation.2 | async-start | bytes 4194304 | tf_op jit(solution)/shard_map/all_to_all | solution.py:205
  146.2 2.7 all-reduce.1
  149.0 5.0 %fusion.99 = f32[2048,512]{1,0:T(8,128)} fusion(bf16[512,2048]{1,0:T(8,128)(2,1)} %bitcast.2, bf16[512,512]{1,0:T(8,128)(2,1)} %copy-done.14), kind=kOutput, calls=%fused_computation.211 | convolution fusion | flops 1073741824 | bytes 6815744 | tf_op jit(solution)/shard_map/dot_general | solution.py:91
  154.0 5.0 %fusion.98 = f32[2048,512]{1,0:T(8,128)} fusion(bf16[512,2048]{1,0:T(8,128)(2,1)} %bitcast.2, bf16[512,512]{1,0:T(8,128)(2,1)S(1)} %get-tuple-element.18), kind=kOutput, calls=%fused_computation.210 | convolution fusion | flops 1073741824 | bytes 6815744 | tf_op jit(solution)/shard_map/dot_general | solution.py:91
  159.1 3.1 %fusion.42 = f32[512,2048]{1,0:T(8,128)S(1)} fusion(bf16[512,2048]{1,0:T(8,128)(2,1)} %bitcast.5, f32[512,512]{1,0:T(8,128)S(1)} %copy-done.18, f32[512,512]{1,0:T(8,128)S(1)} %copy-done.16), kind=kOutput, calls=%fused_computation.105 | convolution fusion | flops 1075314688 | bytes 8388608 | tf_op jit(solution)/shard_map/dot_general | solution.py:91
  162.2 3.5 %add_bitcast_fusion = f32[1,512,2048]{2,1,0:T(8,128)} fusion(f32[512,2048]{1,0:T(8,128)S(1)} %fusion.42, bf16[512,2048]{1,0:T(8,128)(2,1)S(1)} %copy-done.9, f32[512,512]{1,0:T(8,128)S(1)} %copy-done.7, f32[512,512]{1,0:T(8,128)S(1)} %copy-done.5), kind=kOutput, calls=%fused_computation.3 | convolution fusion | flops 1076363264 | bytes 12582912 | tf_op jit(solution)/shard_map/dot_general | solution.py:91
  165.7 22.5 %all-to-all-done.2 = bf16[16,1,32,2048]{3,2,1,0:T(8,128)(2,1)S(1)} async-done(((bf16[16,1,32,2048]{3,2,1,0:T(8,128)(2,1)}), bf16[16,1,32,2048]{3,2,1,0:T(8,128)(2,1)S(1)}, u32[]{:S(2)}, u32[]{:S(2)}) %all-to-all-start.2) | async-done | bytes 2097184 | tf_op jit(solution)/shard_map/all_to_all | solution.py:205
  188.1 1.5 fusion
  189.8 6.4 %add_bitcast_fusion.1 = f32[1,2048,512]{2,1,0:T(8,128)} fusion(f32[2048,512]{1,0:T(8,128)} %fusion.99, bf16[512,2048]{1,0:T(8,128)(2,1)} %collective-permute-done, bf16[512,512]{1,0:T(8,128)(2,1)S(1)} %copy-done.11), kind=kOutput, calls=%fused_computation.4 | convolution fusion | flops 1074790400 | bytes 11010048 | tf_op jit(solution)/shard_map/dot_general | solution.py:91
  196.2 5.2 %add_bitcast_fusion.2 = f32[1,2048,512]{2,1,0:T(8,128)} fusion(f32[2048,512]{1,0:T(8,128)S(1)} %copy-done.2, bf16[512,2048]{1,0:T(8,128)(2,1)} %collective-permute-done, bf16[512,512]{1,0:T(8,128)(2,1)S(1)} %get-tuple-element.16), kind=kOutput, calls=%fused_computation.5 | convolution fusion | flops 1074790400 | bytes 11010048 | tf_op jit(solution)/shard_map/dot_general | solution.py:91
  201.4 1.8 fusion.93
  203.2 2.6 all-reduce
  206.1 1.3 collective-permute-start.16
  207.4 4.8 %collective-permute-start.17 = (bf16[15,1024]{1,0:T(8,128)(2,1)S(1)}, bf16[15,1024]{1,0:T(8,128)(2,1)S(1)}, u32[]{:S(2)}, u32[]{:S(2)}) collective-permute-start(bf16[15,1024]{1,0:T(8,128)(2,1)S(1)} %get-tuple-element.26), channel_id=1, source_target_pairs={{0,2},{2,4},{4,6},{6,8},{8,10},{10,12},{12,14},{14,16},{16,18},{18... | collective-permute-start | bytes 92168 | tf_op jit(solution)/shard_map/ppermute | solution.py:14
  212.3 1.6 convolution_convert_fusion
  214.2 6.2 %collective-permute-start.12 = (bf16[2,2,2,128,256]{4,3,0,1,2:T(8,128)(2,1)S(1)}, bf16[2,2,2,128,256]{4,3,0,1,2:T(8,128)(2,1)S(1)}, u32[]{:S(2)}, u32[]{:S(2)}) collective-permute-start(bf16[2,2,2,128,256]{4,3,0,1,2:T(8,128)(2,1)S(1)} %bitcast.172), channel_id=1, source_target_pairs={{0,8},{2,10},{4,12},{6,14},{8,0},{10,2},{12,4},{14,6},{16,24},{18,... | collective-permute-start | bytes 1572872 | tf_op jit(solution)/shard_map/ppermute | solution.py:77
  221.3 2.4 collective-permute-start.4
  223.7 3.3 %collective-permute-start.8 = (bf16[2,2,2,128,384]{4,3,0,2,1:T(8,128)(2,1)S(1)}, bf16[2,2,2,128,384]{4,3,0,2,1:T(8,128)(2,1)S(1)}, u32[]{:S(2)}, u32[]{:S(2)}) collective-permute-start(bf16[2,2,2,128,384]{4,3,0,2,1:T(8,128)(2,1)S(1)} %bitcast.170), channel_id=1, source_target_pairs={{0,4},{2,6},{4,0},{6,2},{8,12},{10,14},{12,8},{14,10},{16,20},{18,... | collective-permute-start | bytes 2359304 | tf_op jit(solution)/shard_map/ppermute | solution.py:77
  227.0 5.2 %collective-permute-done.12 = bf16[2,2,2,128,256]{4,3,0,1,2:T(8,128)(2,1)S(1)} collective-permute-done((bf16[2,2,2,128,256]{4,3,0,1,2:T(8,128)(2,1)S(1)}, bf16[2,2,2,128,256]{4,3,0,1,2:T(8,128)(2,1)S(1)}, u32[]{:S(2)}, u32[]{:S(2)}) %collective-permute-start.12) | collective-permute-done | bytes 524320 | tf_op jit(solution)/shard_map/ppermute | solution.py:77
  232.4 2.4 collective-permute-start.13
  234.7 5.4 %add_convert_fusion.3 = bf16[256,1024]{1,0:T(8,128)(2,1)} fusion(bf16[256,1024]{1,0:T(8,128)(2,1)S(1)} %fusion.37, bf16[15,1024]{1,0:T(8,128)(2,1)S(1)} %collective-permute-done.17, bf16[15,1024]{1,0:T(8,128)(2,1)S(1)} %collective-permute-done.16, f32[1024]{0:T(1024)S(1)} %bitcast.183, f32[1024]{0:T(1024)S(1)} %bitcast.184, f32[1024]{0:T(1024)S(1)} %bitcast.186, ...), kind=kLoop, calls=%fused_computation.86 | loop fusion | flops 47972352 | bytes 1236992 | tf_op jit(solution)/shard_map/convert_element_type | solution.py:236
  240.1 6.3 %collective-permute-done.13 = bf16[2,2,128,256]{3,2,0,1:T(8,128)(2,1)S(1)} collective-permute-done((bf16[2,2,128,256]{3,2,0,1:T(8,128)(2,1)S(1)}, bf16[2,2,128,256]{3,2,0,1:T(8,128)(2,1)S(1)}, u32[]{:S(2)}, u32[]{:S(2)}) %collective-permute-start.13) | collective-permute-done | bytes 262176 | tf_op jit(solution)/shard_map/ppermute | solution.py:77
  246.5 3.4 %collective-permute-start.14 = (bf16[2,128,256]{2,1,0:T(8,128)(2,1)S(1)}, bf16[2,128,256]{2,1,0:T(8,128)(2,1)S(1)}, u32[]{:S(2)}, u32[]{:S(2)}) collective-permute-start(bf16[2,128,256]{2,1,0:T(8,128)(2,1)S(1)} %fusion.83), channel_id=1, source_target_pairs={{0,4},{2,6},{4,0},{6,2},{8,12},{10,14},{12,8},{14,10},{16,20},{18,... | collective-permute-start | bytes 393224 | tf_op jit(solution)/shard_map/ppermute | solution.py:77
  250.4 3.9 %collective-permute-done.14 = bf16[2,128,256]{2,1,0:T(8,128)(2,1)S(1)} collective-permute-done((bf16[2,128,256]{2,1,0:T(8,128)(2,1)S(1)}, bf16[2,128,256]{2,1,0:T(8,128)(2,1)S(1)}, u32[]{:S(2)}, u32[]{:S(2)}) %collective-permute-start.14) | collective-permute-done | bytes 131104 | tf_op jit(solution)/shard_map/ppermute | solution.py:77
  255.3 1.8 collective-permute-start.9
  257.1 3.0 %collective-permute-done.15 = bf16[128,256]{1,0:T(8,128)(2,1)S(1)} collective-permute-done((bf16[128,256]{1,0:T(8,128)(2,1)S(1)}, bf16[128,256]{1,0:T(8,128)(2,1)S(1)}, u32[]{:S(2)}, u32[]{:S(2)}) %collective-permute-start.15) | collective-permute-done | bytes 65568 | tf_op jit(solution)/shard_map/ppermute | solution.py:77
  261.8 3.7 %collective-permute-done.9 = bf16[2,2,128,384]{3,2,0,1:T(8,128)(2,1)S(1)} collective-permute-done((bf16[2,2,128,384]{3,2,0,1:T(8,128)(2,1)S(1)}, bf16[2,2,128,384]{3,2,0,1:T(8,128)(2,1)S(1)}, u32[]{:S(2)}, u32[]{:S(2)}) %collective-permute-start.9) | collective-permute-done | bytes 393248 | tf_op jit(solution)/shard_map/ppermute | solution.py:77
  265.6 1.3 collective-permute-start.10
  267.0 1.3 collective-permute-done.6
  268.4 1.4 collective-permute-start.7
  269.8 1.6 collective-permute-done.10
  271.5 2.1 collective-permute-start.11
  273.6 2.5 collective-permute-done.7
  276.1 2.9 %collective-permute-done.11 = bf16[128,384]{1,0:T(8,128)(2,1)S(1)} collective-permute-done((bf16[128,384]{1,0:T(8,128)(2,1)S(1)}, bf16[128,384]{1,0:T(8,128)(2,1)S(1)}, u32[]{:S(2)}, u32[]{:S(2)}) %collective-permute-start.11) | collective-permute-done | bytes 98336 | tf_op jit(solution)/shard_map/ppermute | solution.py:77
  (120 shorter events, 13.0 us)
Async XLA Ops:
  0.6 109.7 %copy-start = (bf16[1,2048,512]{2,1,0:T(8,128)(2,1)S(1)}, bf16[1,2048,512]{2,1,0:T(8,128)(2,1)}, u32[]{:S(2)}) copy-start(bf16[1,2048,512]{2,1,0:T(8,128)(2,1)} %param.19) | copy-start | bytes 6291460
  6.0 8.5 %copy-start.22 = (f32[128,2]{0,1:T(2,128)S(1)}, f32[128,2]{0,1:T(2,128)}, u32[]{:S(2)}) copy-start(f32[128,2]{0,1:T(2,128)} %param.14) | copy-start | bytes 3076
  6.0 8.7 %copy-start.12 = (bf16[128,2048]{1,0:T(8,128)(2,1)S(1)}, bf16[128,2048]{1,0:T(8,128)(2,1)}, u32[]{:S(2)}) copy-start(bf16[128,2048]{1,0:T(8,128)(2,1)} %param.12) | copy-start | bytes 1572868
  6.0 51.6 %all-to-all-start = ((bf16[16,1,32,2048]{3,2,1,0:T(8,128)(2,1)}), bf16[16,1,32,2048]{3,2,1,0:T(8,128)(2,1)}, u32[]{:S(2)}, u32[]{:S(2)}) async-start(bf16[16,1,32,2048]{3,2,1,0:T(8,128)(2,1)} %bitcast.166), calls=%async_computation | async-start | bytes 4194304 | tf_op jit(solution)/shard_map/all_to_all | solution.py:185
  57.6 52.7 %all-to-all-start.1 = ((bf16[16,1,32,2048]{3,2,1,0:T(8,128)(2,1)}), bf16[16,1,32,2048]{3,2,1,0:T(8,128)(2,1)}, u32[]{:S(2)}, u32[]{:S(2)}) async-start(bf16[16,1,32,2048]{3,2,1,0:T(8,128)(2,1)} %bitcast.165), calls=%async_computation.1 | async-start | bytes 4194304 | tf_op jit(solution)/shard_map/all_to_all | solution.py:186
  67.7 42.6 %collective-permute-start = (bf16[512,2048]{1,0:T(8,128)(2,1)}, bf16[512,2048]{1,0:T(8,128)(2,1)}, u32[]{:S(2)}, u32[]{:S(2)}) collective-permute-start(bf16[512,2048]{1,0:T(8,128)(2,1)} %bitcast.2), channel_id=1, source_target_pairs={{0,1},{1,0},{2,3},{3,2},{4,5},{5,4},{6,7},{7,6},{8,9},{9,8},{10,11... | collective-permute-start | bytes 6291464 | tf_op jit(solution)/shard_map/ppermute | solution.py:99
  110.3 3.0 %copy-start.3 = (bf16[1,2048,512]{2,1,0:T(8,128)(2,1)S(1)}, bf16[1,2048,512]{2,1,0:T(8,128)(2,1)}, u32[]{:S(2)}) copy-start(bf16[1,2048,512]{2,1,0:T(8,128)(2,1)} %param.20) | copy-start | bytes 6291460
  110.3 6.3 %collective-permute-start.1 = (bf16[512,2048]{1,0:T(8,128)(2,1)}, bf16[512,2048]{1,0:T(8,128)(2,1)S(1)}, u32[]{:S(2)}, u32[]{:S(2)}) collective-permute-start(bf16[512,2048]{1,0:T(8,128)(2,1)} %bitcast.5), channel_id=1, source_target_pairs={{0,1},{1,0},{2,3},{3,2},{4,5},{5,4},{6,7},{7,6},{8,9},{9,8},{10,11... | collective-permute-start | bytes 6291464 | tf_op jit(solution)/shard_map/ppermute | solution.py:99
  113.3 3.3 %copy-start.4 = (f32[512,512]{1,0:T(8,128)}, f32[512,512]{1,0:T(8,128)S(1)}, u32[]{:S(2)}) copy-start(f32[512,512]{1,0:T(8,128)S(1)} %fusion.5) | copy-start | bytes 3145732
  113.3 3.3 %copy-start.24 = (bf16[1,512,2048]{2,1,0:T(8,128)(2,1)S(1)}, bf16[1,512,2048]{2,1,0:T(8,128)(2,1)}, u32[]{:S(2)}) copy-start(bf16[1,512,2048]{2,1,0:T(8,128)(2,1)} %param.21) | copy-start | bytes 6291460
  116.6 1.7 copy-start.6
  116.6 1.6 copy-start.8
  120.9 11.5 %collective-permute-start.2 = (bf16[512,2048]{1,0:T(8,128)(2,1)S(1)}, bf16[512,2048]{1,0:T(8,128)(2,1)S(1)}, u32[]{:S(2)}, u32[]{:S(2)}) collective-permute-start(bf16[512,2048]{1,0:T(8,128)(2,1)S(1)} %add_convert_fusion.1), channel_id=1, source_target_pairs={{0,1},{1,0},{2,3},{3,2},{4,5},{5,4},{6,7},{7,6},{8,9},{9,8},{10,11... | collective-permute-start | bytes 6291464 | tf_op jit(solution)/shard_map/ppermute | solution.py:128
  124.2 3.2 %copy-start.15 = (f32[512,512]{1,0:T(8,128)}, f32[512,512]{1,0:T(8,128)S(1)}, u32[]{:S(2)}) copy-start(f32[512,512]{1,0:T(8,128)S(1)} %fusion.7) | copy-start | bytes 3145732
  127.4 3.7 %copy-start.17 = (f32[512,512]{1,0:T(8,128)}, f32[512,512]{1,0:T(8,128)S(1)}, u32[]{:S(2)}) copy-start(f32[512,512]{1,0:T(8,128)S(1)} %fusion.13) | copy-start | bytes 3145732
  131.1 1.3 copy-start.14
  135.1 13.8 %copy-start.21 = (f32[31,1024]{1,0:T(8,128)S(1)}, f32[31,1024]{1,0:T(8,128)}, u32[]{:S(2)}) copy-start(f32[31,1024]{1,0:T(8,128)} %param.16) | copy-start | bytes 380932
  135.1 53.0 %all-to-all-start.2 = ((bf16[16,1,32,2048]{3,2,1,0:T(8,128)(2,1)}), bf16[16,1,32,2048]{3,2,1,0:T(8,128)(2,1)S(1)}, u32[]{:S(2)}, u32[]{:S(2)}) async-start(bf16[16,1,32,2048]{3,2,1,0:T(8,128)(2,1)} %bitcast.167), calls=%async_computation.2 | async-start | bytes 4194304 | tf_op jit(solution)/shard_map/all_to_all | solution.py:205
  154.0 5.1 %copy-start.16 = (f32[512,512]{1,0:T(8,128)S(1)}, f32[512,512]{1,0:T(8,128)}, u32[]{:S(2)}) copy-start(f32[512,512]{1,0:T(8,128)} %copy-done.15) | copy-start | bytes 3145732
  154.0 5.1 %copy-start.18 = (f32[512,512]{1,0:T(8,128)S(1)}, f32[512,512]{1,0:T(8,128)}, u32[]{:S(2)}) copy-start(f32[512,512]{1,0:T(8,128)} %copy-done.17) | copy-start | bytes 3145732
  159.0 3.2 %copy-start.5 = (f32[512,512]{1,0:T(8,128)S(1)}, f32[512,512]{1,0:T(8,128)}, u32[]{:S(2)}) copy-start(f32[512,512]{1,0:T(8,128)} %copy-done.4) | copy-start | bytes 3145732
  159.1 3.2 %copy-start.7 = (f32[512,512]{1,0:T(8,128)S(1)}, f32[512,512]{1,0:T(8,128)}, u32[]{:S(2)}) copy-start(f32[512,512]{1,0:T(8,128)} %copy-done.6) | copy-start | bytes 3145732
  159.1 3.2 %copy-start.9 = (bf16[512,2048]{1,0:T(8,128)(2,1)S(1)}, bf16[512,2048]{1,0:T(8,128)(2,1)}, u32[]{:S(2)}) copy-start(bf16[512,2048]{1,0:T(8,128)(2,1)} %copy-done.8) | copy-start | bytes 6291460
  165.7 24.1 %copy-start.11 = (bf16[512,512]{1,0:T(8,128)(2,1)S(1)}, bf16[512,512]{1,0:T(8,128)(2,1)}, u32[]{:S(2)}) copy-start(bf16[512,512]{1,0:T(8,128)(2,1)} %copy-done.10) | copy-start | bytes 1572868
  189.7 11.7 %copy-start.19 = (bf16[128,2048]{1,0:T(8,128)(2,1)}, bf16[128,2048]{1,0:T(8,128)(2,1)S(1)}, u32[]{:S(2)}) copy-start(bf16[128,2048]{1,0:T(8,128)(2,1)S(1)} %fusion) | copy-start | bytes 1572868
  189.7 6.5 %copy-start.2 = (f32[2048,512]{1,0:T(8,128)S(1)}, f32[2048,512]{1,0:T(8,128)}, u32[]{:S(2)}) copy-start(f32[2048,512]{1,0:T(8,128)} %fusion.98) | copy-start | bytes 12582916
  189.7 11.6 %collective-permute-start.3 = (bf16[128,2048]{1,0:T(8,128)(2,1)S(1)}, bf16[128,2048]{1,0:T(8,128)(2,1)S(1)}, u32[]{:S(2)}, u32[]{:S(2)}) collective-permute-start(bf16[128,2048]{1,0:T(8,128)(2,1)S(1)} %fusion), channel_id=1, source_target_pairs={{0,1},{1,0},{2,3},{3,2},{4,5},{5,4},{6,7},{7,6},{8,9},{9,8},{10,11... | collective-permute-start | bytes 1572872 | tf_op jit(solution)/shard_map/ppermute | solution.py:99
  196.2 5.2 %copy-start.13 = (bf16[256,1024]{1,0:T(8,128)(2,1)S(1)}, bf16[256,1024]{1,0:T(8,128)(2,1)}, u32[]{:S(2)}) copy-start(bf16[256,1024]{1,0:T(8,128)(2,1)} %param.15) | copy-start | bytes 1572868
  196.2 5.2 %copy-start.23 = (bf16[1024,2048]{1,0:T(8,128)(2,1)S(1)}, bf16[1024,2048]{1,0:T(8,128)(2,1)}, u32[]{:S(2)}) copy-start(bf16[1024,2048]{1,0:T(8,128)(2,1)} %param.18) | copy-start | bytes 12582916
  196.2 5.2 %copy-start.27 = (f32[1024]{0:T(1024)S(1)}, f32[1024]{0:T(1024)}, u32[]{:S(2)}) copy-start(f32[1024]{0:T(1024)} %param.17) | copy-start | bytes 12292
  201.3 1.8 copy-start.25
  203.2 9.1 %copy-start.20 = (bf16[128,2048]{1,0:T(8,128)(2,1)S(1)}, bf16[128,2048]{1,0:T(8,128)(2,1)}, u32[]{:S(2)}) copy-start(bf16[128,2048]{1,0:T(8,128)(2,1)} %copy-done.19) | copy-start | bytes 1572868
  203.2 9.1 %copy-start.26 = (bf16[128,2048]{1,0:T(8,128)(2,1)S(1)}, bf16[128,2048]{1,0:T(8,128)(2,1)}, u32[]{:S(2)}) copy-start(bf16[128,2048]{1,0:T(8,128)(2,1)} %copy-done.25) | copy-start | bytes 1572868
  206.1 28.6 %collective-permute-start.16 = (bf16[15,1024]{1,0:T(8,128)(2,1)S(1)}, bf16[15,1024]{1,0:T(8,128)(2,1)S(1)}, u32[]{:S(2)}, u32[]{:S(2)}) collective-permute-start(bf16[15,1024]{1,0:T(8,128)(2,1)S(1)} %get-tuple-element.25), channel_id=1, source_target_pairs={{2,0},{4,2},{6,4},{8,6},{10,8},{12,10},{14,12},{16,14},{18,16},{20... | collective-permute-start | bytes 92168 | tf_op jit(solution)/shard_map/ppermute | solution.py:17
  207.4 27.3 %collective-permute-start.17 = (bf16[15,1024]{1,0:T(8,128)(2,1)S(1)}, bf16[15,1024]{1,0:T(8,128)(2,1)S(1)}, u32[]{:S(2)}, u32[]{:S(2)}) collective-permute-start(bf16[15,1024]{1,0:T(8,128)(2,1)S(1)} %get-tuple-element.26), channel_id=1, source_target_pairs={{0,2},{2,4},{4,6},{6,8},{8,10},{10,12},{12,14},{14,16},{16,18},{18... | collective-permute-start | bytes 92168 | tf_op jit(solution)/shard_map/ppermute | solution.py:14
  214.2 18.0 %collective-permute-start.12 = (bf16[2,2,2,128,256]{4,3,0,1,2:T(8,128)(2,1)S(1)}, bf16[2,2,2,128,256]{4,3,0,1,2:T(8,128)(2,1)S(1)}, u32[]{:S(2)}, u32[]{:S(2)}) collective-permute-start(bf16[2,2,2,128,256]{4,3,0,1,2:T(8,128)(2,1)S(1)} %bitcast.172), channel_id=1, source_target_pairs={{0,8},{2,10},{4,12},{6,14},{8,0},{10,2},{12,4},{14,6},{16,24},{18,... | collective-permute-start | bytes 1572872 | tf_op jit(solution)/shard_map/ppermute | solution.py:77
  221.3 28.6 %collective-permute-start.4 = (bf16[2,2,2,128,384]{4,3,0,1,2:T(8,128)(2,1)S(1)}, bf16[2,2,2,128,384]{4,3,0,1,2:T(8,128)(2,1)S(1)}, u32[]{:S(2)}, u32[]{:S(2)}) collective-permute-start(bf16[2,2,2,128,384]{4,3,0,1,2:T(8,128)(2,1)S(1)} %bitcast.171), channel_id=1, source_target_pairs={{0,2},{2,0},{4,6},{6,4},{8,10},{10,8},{12,14},{14,12},{16,18},{18,... | collective-permute-start | bytes 2359304 | tf_op jit(solution)/shard_map/ppermute | solution.py:77
  223.7 26.6 %collective-permute-start.8 = (bf16[2,2,2,128,384]{4,3,0,2,1:T(8,128)(2,1)S(1)}, bf16[2,2,2,128,384]{4,3,0,2,1:T(8,128)(2,1)S(1)}, u32[]{:S(2)}, u32[]{:S(2)}) collective-permute-start(bf16[2,2,2,128,384]{4,3,0,2,1:T(8,128)(2,1)S(1)} %bitcast.170), channel_id=1, source_target_pairs={{0,4},{2,6},{4,0},{6,2},{8,12},{10,14},{12,8},{14,10},{16,20},{18,... | collective-permute-start | bytes 2359304 | tf_op jit(solution)/shard_map/ppermute | solution.py:77
  232.4 14.0 %collective-permute-start.13 = (bf16[2,2,128,256]{3,2,0,1:T(8,128)(2,1)S(1)}, bf16[2,2,128,256]{3,2,0,1:T(8,128)(2,1)S(1)}, u32[]{:S(2)}, u32[]{:S(2)}) collective-permute-start(bf16[2,2,128,256]{3,2,0,1:T(8,128)(2,1)S(1)} %fusion.78), channel_id=1, source_target_pairs={{0,2},{2,0},{4,6},{6,4},{8,10},{10,8},{12,14},{14,12},{16,18},{18,... | collective-permute-start | bytes 786440 | tf_op jit(solution)/shard_map/ppermute | solution.py:77
  246.5 7.8 %collective-permute-start.14 = (bf16[2,128,256]{2,1,0:T(8,128)(2,1)S(1)}, bf16[2,128,256]{2,1,0:T(8,128)(2,1)S(1)}, u32[]{:S(2)}, u32[]{:S(2)}) collective-permute-start(bf16[2,128,256]{2,1,0:T(8,128)(2,1)S(1)} %fusion.83), channel_id=1, source_target_pairs={{0,4},{2,6},{4,0},{6,2},{8,12},{10,14},{12,8},{14,10},{16,20},{18,... | collective-permute-start | bytes 393224 | tf_op jit(solution)/shard_map/ppermute | solution.py:77
  250.1 11.1 %collective-permute-start.5 = (bf16[2,2,128,384]{3,2,0,1:T(8,128)(2,1)S(1)}, bf16[2,2,128,384]{3,2,0,1:T(8,128)(2,1)S(1)}, u32[]{:S(2)}, u32[]{:S(2)}) collective-permute-start(bf16[2,2,128,384]{3,2,0,1:T(8,128)(2,1)S(1)} %fusion.76), channel_id=1, source_target_pairs={{0,4},{2,6},{4,0},{6,2},{8,12},{10,14},{12,8},{14,10},{16,20},{18,... | collective-permute-start | bytes 1179656 | tf_op jit(solution)/shard_map/ppermute | solution.py:77
  254.3 5.8 %collective-permute-start.15 = (bf16[128,256]{1,0:T(8,128)(2,1)S(1)}, bf16[128,256]{1,0:T(8,128)(2,1)S(1)}, u32[]{:S(2)}, u32[]{:S(2)}) collective-permute-start(bf16[128,256]{1,0:T(8,128)(2,1)S(1)} %fusion.86), channel_id=1, source_target_pairs={{0,16},{2,18},{4,20},{6,22},{8,24},{10,26},{12,28},{14,30},{16,0},... | collective-permute-start | bytes 196616 | tf_op jit(solution)/shard_map/ppermute | solution.py:77
  255.3 10.2 %collective-permute-start.9 = (bf16[2,2,128,384]{3,2,0,1:T(8,128)(2,1)S(1)}, bf16[2,2,128,384]{3,2,0,1:T(8,128)(2,1)S(1)}, u32[]{:S(2)}, u32[]{:S(2)}) collective-permute-start(bf16[2,2,128,384]{3,2,0,1:T(8,128)(2,1)S(1)} %fusion.77), channel_id=1, source_target_pairs={{0,8},{2,10},{4,12},{6,14},{8,0},{10,2},{12,4},{14,6},{16,24},{18,... | collective-permute-start | bytes 1179656 | tf_op jit(solution)/shard_map/ppermute | solution.py:77
  261.3 7.0 %collective-permute-start.6 = (bf16[2,128,384]{2,1,0:T(8,128)(2,1)S(1)}, bf16[2,128,384]{2,1,0:T(8,128)(2,1)S(1)}, u32[]{:S(2)}, u32[]{:S(2)}) collective-permute-start(bf16[2,128,384]{2,1,0:T(8,128)(2,1)S(1)} %fusion.79), channel_id=1, source_target_pairs={{0,8},{2,10},{4,12},{6,14},{8,0},{10,2},{12,4},{14,6},{16,24},{18,... | collective-permute-start | bytes 589832 | tf_op jit(solution)/shard_map/ppermute | solution.py:77
  265.6 14.3 %copy-start.1 = (bf16[1,2048,512]{2,1,0:T(8,128)(2,1)S(1)}, bf16[1,2048,512]{2,1,0:T(8,128)(2,1)}, u32[]{:S(2)}) copy-start(bf16[1,2048,512]{2,1,0:T(8,128)(2,1)} %param.19) | copy-start | bytes 6291460
  265.6 5.7 %collective-permute-start.10 = (bf16[2,128,384]{2,1,0:T(8,128)(2,1)S(1)}, bf16[2,128,384]{2,1,0:T(8,128)(2,1)S(1)}, u32[]{:S(2)}, u32[]{:S(2)}) collective-permute-start(bf16[2,128,384]{2,1,0:T(8,128)(2,1)S(1)} %fusion.80), channel_id=1, source_target_pairs={{0,2},{2,0},{4,6},{6,4},{8,10},{10,8},{12,14},{14,12},{16,18},{18,... | collective-permute-start | bytes 589832 | tf_op jit(solution)/shard_map/ppermute | solution.py:77
  268.4 7.7 %collective-permute-start.7 = (bf16[128,384]{1,0:T(8,128)(2,1)S(1)}, bf16[128,384]{1,0:T(8,128)(2,1)S(1)}, u32[]{:S(2)}, u32[]{:S(2)}) collective-permute-start(bf16[128,384]{1,0:T(8,128)(2,1)S(1)} %fusion.84), channel_id=1, source_target_pairs={{0,16},{2,18},{4,20},{6,22},{8,24},{10,26},{12,28},{14,30},{16,0},... | collective-permute-start | bytes 294920 | tf_op jit(solution)/shard_map/ppermute | solution.py:77
  271.5 7.6 %collective-permute-start.11 = (bf16[128,384]{1,0:T(8,128)(2,1)S(1)}, bf16[128,384]{1,0:T(8,128)(2,1)S(1)}, u32[]{:S(2)}, u32[]{:S(2)}) collective-permute-start(bf16[128,384]{1,0:T(8,128)(2,1)S(1)} %fusion.85), channel_id=1, source_target_pairs={{0,16},{2,18},{4,20},{6,22},{8,24},{10,26},{12,28},{14,30},{16,0},... | collective-permute-start | bytes 294920 | tf_op jit(solution)/shard_map/ppermute | solution.py:77
  (1 other events, 1.3 us)

commit v3 on v2

--- a/solution.py
+++ b/solution.py
@@ -64,21 +64,27 @@
     product = transposed_product(rows, columns).astype(jnp.bfloat16)
     cut = product.reshape((2,) * bits + (width // count, columns.shape[1]))
     orders = halving_orders(count)
-    pieces = []
-    for order, (start, size) in zip(orders, column_groups(columns.shape[1], len(orders))):
-        total = lax.slice_in_dim(cut, start, start + size, axis=bits + 1)
-        left = list(range(bits - 1, -1, -1))
-        for bit in order:
-            mine = (own >> bit) & 1
-            dim = left.index(bit)
-            outgoing = picked(total, 1 - mine, dim)
-            kept = picked(total, mine, dim).astype(jnp.float32)
-            pairs = [(i, i ^ (1 << bit)) for i in range(count)]
-            arrived = lax.ppermute(outgoing.astype(jnp.bfloat16), axis, pairs)
-            total = kept + arrived.astype(jnp.float32)
-            left.pop(dim)
-        pieces.append(total)
-    return jnp.concatenate(pieces, axis=1)
+    groups = column_groups(columns.shape[1], len(orders))
+    orders = orders[: len(groups)]
+    totals = [lax.slice_in_dim(cut, start, start + size, axis=bits + 1) for start, size in groups]
+    left = [list(range(bits - 1, -1, -1)) for _ in groups]
+    for step in range(bits):
+        outgoing, kept = [], []
+        for total, order, dims in zip(totals, orders, left):
+            mine = (own >> order[step]) & 1
+            dim = dims.index(order[step])
+            dims.pop(dim)
+            outgoing.append(picked(total, 1 - mine, dim).astype(jnp.bfloat16))
+            kept.append(picked(total, mine, dim).astype(jnp.float32))
+        if step == 0:
+            outgoing, rows = lax.optimization_barrier((outgoing, rows))
+        arrived = [
+            lax.ppermute(block, axis, [(i, i ^ (1 << order[step])) for i in range(count)])
+            for block, order in zip(outgoing, orders)
+        ]
+        arrived = lax.optimization_barrier(arrived)
+        totals = [own_part + got.astype(jnp.float32) for own_part, got in zip(kept, arrived)]
+    return jnp.concatenate(totals, axis=1), rows
 
 
 def row_product(rows, matrix, dim=0):
@@ -120,6 +126,7 @@
     count = lax.axis_size(axis)
     all_in = [got_in] + from_partner(got_in, axis)
     pre = [(row_product(rows, gate_mat), row_product(rows, up_mat)) for rows in all_in]
+    pre, got_cot = lax.optimization_barrier((pre, got_cot))
     all_cot = [got_cot] + from_partner(got_cot, axis)
     grads = [hidden_gradients(g, u, c, down_mat) for (g, u), c in zip(pre, all_cot)]
     back = None
@@ -203,6 +210,9 @@
         [part[3].reshape(sp_count, capacity, model_width) for part in parts], axis=1
     ).reshape(by_expert)
     returned = lax.all_to_all(back_rows, "sp", split_axis=0, concat_axis=0, tiled=True)
+    returned, gate_grad, up_grad, down_grad, channel_sum, squares = lax.optimization_barrier(
+        (returned, gate_grad, up_grad, down_grad, channel_sum, squares)
+    )
     back_all = returned.reshape(experts * capacity, model_width)
     route_sum = lax.dot_general(
         chosen, back_all, (((0,), (0,)), ((), ())), preferred_element_type=jnp.float32
@@ -215,7 +225,7 @@
     scaled = normed * norm_gain
     activated = jax.nn.silu(scaled).astype(jnp.bfloat16)
     grad_tokens = gathered_rows(mid_grad, "tp")
-    proj_grad = reduced_products(grad_tokens, activated, "sp")
+    proj_grad, grad_tokens = reduced_products(grad_tokens, activated, "sp")
     act_grad = lax.dot_general(
         grad_tokens, out_weight, (((1,), (1,)), ((), ())), preferred_element_type=jnp.float32
     )

time: 281 us -> 256 us (0.911)
  waiting for transfers between devices: 137 us -> 117 us
  starting transfers between devices: 60.7 us -> 54.9 us
  local copies, waits for them, and re-layouts: 2.92 us -> 6.81 us
  matrix products: 62.5 us -> 58.7 us
    all_to_all x1, waiting for transfers between devices: 42.5 us -> 29.6 us  [per_device(): lax.all_to_all(routed, 'sp', split_axis=0, concat_axis=0, tiled=True)]
    ppermute x12, waiting for transfers between devices: 31.6 us -> 19.1 us  [reduced_products(): lax.ppermute(block, axis, [(i, i ^ 1 << order[step]) for i in range(count)])]
    dot_general x7, matrix products: 29.8 us -> 20.9 us  [transposed_product(): lax.dot_general(left, right, (((0,), (0,)), ((), ())), preferred_element_...]
    ppermute x3, waiting for transfers between devices: 0.01 us -> 6.11 us  [from_partner(): lax.ppermute(block, axis, [(i, (i + step) % count) for i in range(count)])]
    ppermute x12, starting transfers between devices: 25.7 us -> 20.3 us  [reduced_products(): lax.ppermute(block, axis, [(i, i ^ 1 << order[step]) for i in range(count)])]
    unnamed x60, local copies, waits for them, and re-layouts: 1.27 us -> 4.96 us
    dot_general x10, matrix products: 24.2 us -> 27.3 us  [row_product(): lax.dot_general(rows, matrix, (((1,), (dim,)), ((), ())), preferred_eleme...]
  transfers between devices with their start and end apart: 21 -> 21, of which waited for: 13 -> 12; matrix products, arithmetic and copies ran while one was open for 21% -> 20% of each run, Pallas kernels for 0% -> 0%
where the time goes in v3:
time: 256 us
  waiting for transfers between devices  117 us (46%)
  matrix products  58.7 us (23%)
  starting transfers between devices  54.9 us (21%)
  other arithmetic  11.7 us (5%)
  local copies, waits for them, and re-layouts  6.81 us (3%)
  blocking collectives  5.69 us (2%)
    all_to_all x1, waiting for transfers between devices, per_device(): lax.all_to_all(inputs, 'sp', split_axis=0, concat_axis=0, tiled=True)  40.9 us
    all_to_all x1, waiting for transfers between devices, per_device(): lax.all_to_all(routed, 'sp', split_axis=0, concat_axis=0, tiled=True)  29.6 us
    dot_general x10, matrix products, row_product(): lax.dot_general(rows, matrix, (((1,), (dim,)), ((), ())), preferred_eleme...  27.3 us
    dot_general x7, matrix products, transposed_product(): lax.dot_general(left, right, (((0,), (0,)), ((), ())), preferred_element_...  20.9 us
    all_to_all x1, waiting for transfers between devices, per_device(): lax.all_to_all(back_rows, 'sp', split_axis=0, concat_axis=0, tiled=True)  20.8 us
    ppermute x12, starting transfers between devices, reduced_products(): lax.ppermute(block, axis, [(i, i ^ 1 << order[step]) for i in range(count)])  20.3 us
    ppermute x12, waiting for transfers between devices, reduced_products(): lax.ppermute(block, axis, [(i, i ^ 1 << order[step]) for i in range(count)])  19.1 us
    all_to_all x1, starting transfers between devices, per_device(): lax.all_to_all(routed, 'sp', split_axis=0, concat_axis=0, tiled=True)  10.1 us
  transfers between devices with their start and end apart: 21, of which 12 were waited for; matrix products, arithmetic and copies ran while one was open for 20% of the time, Pallas kernels for 0%

profile of v3, /device:TPU:0, one launch (start us, length us, event | category | flops | bytes accessed | tf_op | source)
XLA Modules:
  0.0 255.6 jit_solution(15672044580082873999)
XLA Ops:
  2.9 3.1 %convolution_convert_fusion.1 = bf16[512,2048]{1,0:T(8,128)(2,1)} fusion(pred[512,128]{1,0:T(8,128)(4,1)S(1)} %fusion.75, bf16[128,2048]{1,0:T(8,128)(2,1)} %param.11), kind=kOutput, calls=%fused_computation.36 | convolution fusion | flops 269484032 | bytes 2686976 | tf_op jit(solution)/shard_map/dot_general | solution.py:187
  6.0 8.5 %all-to-all-start = ((bf16[16,1,32,2048]{3,2,1,0:T(8,128)(2,1)}), bf16[16,1,32,2048]{3,2,1,0:T(8,128)(2,1)}, u32[]{:S(2)}, u32[]{:S(2)}) async-start(bf16[16,1,32,2048]{3,2,1,0:T(8,128)(2,1)} %bitcast.167), calls=%async_computation | async-start | bytes 4194304 | tf_op jit(solution)/shard_map/all_to_all | solution.py:192
  14.7 2.0 multiply_convert_fusion
  16.7 40.9 %all-to-all-done = bf16[16,1,32,2048]{3,2,1,0:T(8,128)(2,1)} async-done(((bf16[16,1,32,2048]{3,2,1,0:T(8,128)(2,1)}), bf16[16,1,32,2048]{3,2,1,0:T(8,128)(2,1)}, u32[]{:S(2)}, u32[]{:S(2)}) %all-to-all-start) | async-done | bytes 2097184 | tf_op jit(solution)/shard_map/all_to_all | solution.py:192
  57.6 10.1 %all-to-all-start.1 = ((bf16[16,1,32,2048]{3,2,1,0:T(8,128)(2,1)}), bf16[16,1,32,2048]{3,2,1,0:T(8,128)(2,1)}, u32[]{:S(2)}, u32[]{:S(2)}) async-start(bf16[16,1,32,2048]{3,2,1,0:T(8,128)(2,1)} %bitcast.166), calls=%async_computation.1 | async-start | bytes 4194304 | tf_op jit(solution)/shard_map/all_to_all | solution.py:193
  67.7 4.4 %fusion.9 = f32[512,512]{1,0:T(8,128)} fusion(bf16[512,2048]{1,0:T(8,128)(2,1)} %bitcast.2, bf16[1,2048,512]{2,1,0:T(8,128)(2,1)} %param.20), kind=kOutput, calls=%fused_computation.47 | convolution fusion | flops 1073741824 | bytes 5242880 | tf_op jit(solution)/shard_map/dot_general | solution.py:91
  72.2 4.0 %fusion.17 = f32[512,512]{1,0:T(8,128)} fusion(bf16[512,2048]{1,0:T(8,128)(2,1)} %bitcast.2, bf16[1,2048,512]{2,1,0:T(8,128)(2,1)S(1)} %copy-done), kind=kOutput, calls=%fused_computation.55 | convolution fusion | flops 1073741824 | bytes 5242880 | tf_op jit(solution)/shard_map/dot_general | solution.py:91
  76.2 2.3 fusion.7
  78.4 2.2 fusion.15
  80.6 29.6 %all-to-all-done.1 = bf16[16,1,32,2048]{3,2,1,0:T(8,128)(2,1)} async-done(((bf16[16,1,32,2048]{3,2,1,0:T(8,128)(2,1)}), bf16[16,1,32,2048]{3,2,1,0:T(8,128)(2,1)}, u32[]{:S(2)}, u32[]{:S(2)}) %all-to-all-start.1) | async-done | bytes 2097184 | tf_op jit(solution)/shard_map/all_to_all | solution.py:193
  110.3 4.4 %collective-permute-done.1 = bf16[512,2048]{1,0:T(8,128)(2,1)S(1)} collective-permute-done((bf16[512,2048]{1,0:T(8,128)(2,1)}, bf16[512,2048]{1,0:T(8,128)(2,1)S(1)}, u32[]{:S(2)}, u32[]{:S(2)}) %collective-permute-start.1) | collective-permute-done | bytes 2097184 | tf_op jit(solution)/shard_map/ppermute | solution.py:105
  114.7 4.6 %multiply_convert_fusion.3 = (bf16[512,512]{1,0:T(8,128)(2,1)S(1)}, bf16[512,512]{1,0:T(8,128)(2,1)S(1)}) fusion(f32[512,512]{1,0:T(8,128)} %fusion.15, f32[512,512]{1,0:T(8,128)} %fusion.7, bf16[512,2048]{1,0:T(8,128)(2,1)S(1)} %collective-permute-done.1, bf16[1,512,2048]{2,1,0:T(8,128)(2,1)} %param.21), kind=kOutput, calls=%fused_computation.89 | convolution fusion | flops 1077149696 | bytes 7340032 | tf_op jit(solution)/shard_map/dot_general | solution.py:91
  119.3 1.3 fusion.11
  121.1 1.3 add_convert_fusion.1
  123.3 3.3 %multiply_convert_fusion.5 = (bf16[512,512]{1,0:T(8,128)(2,1)S(1)}, bf16[512,512]{1,0:T(8,128)(2,1)S(1)}) fusion(f32[512,512]{1,0:T(8,128)S(1)} %copy-done.21, f32[512,512]{1,0:T(8,128)S(1)} %copy-done.19, bf16[512,2048]{1,0:T(8,128)(2,1)} %bitcast.7, bf16[1,512,2048]{2,1,0:T(8,128)(2,1)S(1)} %copy-done.26), kind=kOutput, calls=%fused_computation.93 | convolution fusion | flops 1077149696 | bytes 7340032 | tf_op jit(solution)/shard_map/dot_general | solution.py:91
  126.6 1.3 fusion.13
  127.9 2.7 %add_convert_fusion = bf16[512,2048]{1,0:T(8,128)(2,1)} fusion(bf16[512,2048]{1,0:T(8,128)(2,1)S(1)} %collective-permute-done.2, f32[512,2048]{1,0:T(8,128)S(1)} %fusion.13, bf16[512,512]{1,0:T(8,128)(2,1)S(1)} %get-tuple-element.69, bf16[1,2048,512]{2,1,0:T(8,128)(2,1)S(1)} %copy-done.5), kind=kOutput, calls=%fused_computation.3 | convolution fusion | flops 1080033280 | bytes 11010048 | tf_op jit(solution)/shard_map/dot_general | solution.py:91
  130.6 9.8 %all-to-all-start.2 = ((bf16[16,1,32,2048]{3,2,1,0:T(8,128)(2,1)}), bf16[16,1,32,2048]{3,2,1,0:T(8,128)(2,1)}, u32[]{:S(2)}, u32[]{:S(2)}) async-start(bf16[16,1,32,2048]{3,2,1,0:T(8,128)(2,1)} %bitcast.10), calls=%async_computation.2 | async-start | bytes 4194304 | tf_op jit(solution)/shard_map/all_to_all | solution.py:212
  140.6 2.7 %all-reduce.1 = (f32[256]{0:T(256)S(1)}, f32[256]{0:T(256)S(1)}) all-reduce(f32[256]{0:T(256)S(1)} %get-tuple-element.62, f32[256]{0:T(256)S(1)} %get-tuple-element.61), channel_id=1, replica_groups=mesh['sp'=16,'tp'=2] {'tp'}, use_global_device_ids=true, to_apply=%region_4.5 | all-reduce | flops 512 | bytes 4096 | tf_op jit(solution)/shard_map/psum | solution.py:179
  143.3 2.9 %fusion.97 = f32[2048,512]{1,0:T(8,128)S(1)} fusion(bf16[512,2048]{1,0:T(8,128)(2,1)} %bitcast.2, bf16[512,512]{1,0:T(8,128)(2,1)S(1)} %copy-done.17), kind=kOutput, calls=%fused_computation.209 | convolution fusion | flops 1073741824 | bytes 6815744 | tf_op jit(solution)/shard_map/dot_general | solution.py:97
  146.2 3.0 %fusion.96 = f32[2048,512]{1,0:T(8,128)S(1)} fusion(bf16[512,2048]{1,0:T(8,128)(2,1)} %bitcast.2, bf16[512,512]{1,0:T(8,128)(2,1)S(1)} %get-tuple-element.70), kind=kOutput, calls=%fused_computation.208 | convolution fusion | flops 1073741824 | bytes 6815744 | tf_op jit(solution)/shard_map/dot_general | solution.py:97
  149.3 3.1 %fusion.42 = f32[512,2048]{1,0:T(8,128)S(1)} fusion(bf16[512,2048]{1,0:T(8,128)(2,1)} %bitcast.7, f32[512,512]{1,0:T(8,128)S(1)} %copy-done.20, f32[512,512]{1,0:T(8,128)S(1)} %copy-done.22), kind=kOutput, calls=%fused_computation.105 | convolution fusion | flops 1075314688 | bytes 8388608 | tf_op jit(solution)/shard_map/dot_general | solution.py:97
  152.5 3.4 %add_bitcast_fusion.1 = f32[1,2048,512]{2,1,0:T(8,128)} fusion(f32[2048,512]{1,0:T(8,128)S(1)} %fusion.97, bf16[512,2048]{1,0:T(8,128)(2,1)S(1)} %copy-done.3, bf16[512,512]{1,0:T(8,128)(2,1)S(1)} %copy-done.11), kind=kOutput, calls=%fused_computation.1 | convolution fusion | flops 1074790400 | bytes 11010048 | tf_op jit(solution)/shard_map/dot_general | solution.py:97
  155.9 3.4 %add_bitcast_fusion.2 = f32[1,2048,512]{2,1,0:T(8,128)} fusion(f32[2048,512]{1,0:T(8,128)S(1)} %fusion.96, bf16[512,2048]{1,0:T(8,128)(2,1)S(1)} %copy-done.3, bf16[512,512]{1,0:T(8,128)(2,1)S(1)} %get-tuple-element.72), kind=kOutput, calls=%fused_computation.2 | convolution fusion | flops 1074790400 | bytes 11010048 | tf_op jit(solution)/shard_map/dot_general | solution.py:97
  159.3 3.4 %add_bitcast_fusion = f32[1,512,2048]{2,1,0:T(8,128)} fusion(f32[512,2048]{1,0:T(8,128)S(1)} %fusion.42, bf16[512,2048]{1,0:T(8,128)(2,1)S(1)} %copy-done.9, f32[512,512]{1,0:T(8,128)S(1)} %copy-done.6, f32[512,512]{1,0:T(8,128)S(1)} %copy-done.7), kind=kOutput, calls=%fused_computation | convolution fusion | flops 1076363264 | bytes 12582912 | tf_op jit(solution)/shard_map/dot_general | solution.py:97
  162.7 20.8 %all-to-all-done.2 = bf16[16,1,32,2048]{3,2,1,0:T(8,128)(2,1)} async-done(((bf16[16,1,32,2048]{3,2,1,0:T(8,128)(2,1)}), bf16[16,1,32,2048]{3,2,1,0:T(8,128)(2,1)}, u32[]{:S(2)}, u32[]{:S(2)}) %all-to-all-start.2) | async-done | bytes 2097184 | tf_op jit(solution)/shard_map/all_to_all | solution.py:212
  183.5 2.1 fusion
  185.9 1.7 collective-permute-done.3
  188.0 1.6 convolution_convert_fusion
  193.5 6.1 %collective-permute-start.6 = (bf16[2,2,2,128,256]{4,3,0,1,2:T(8,128)(2,1)}, bf16[2,2,2,128,256]{4,3,0,1,2:T(8,128)(2,1)}, u32[]{:S(2)}, u32[]{:S(2)}) collective-permute-start(bf16[2,2,2,128,256]{4,3,0,1,2:T(8,128)(2,1)} %bitcast.165), channel_id=1, source_target_pairs={{0,8},{2,10},{4,12},{6,14},{8,0},{10,2},{12,4},{14,6},{16,24},{18,... | collective-permute-start | bytes 1572872 | tf_op jit(solution)/shard_map/ppermute | solution.py:82
  199.7 1.4 collective-permute-start.4
  201.1 2.4 collective-permute-start.5
  203.5 3.0 %fusion.91 = (f32[256]{0:T(256)S(1)}, f32[256]{0:T(256)S(1)}, f32[256,1024]{1,0:T(8,128)}) fusion(f32[256]{0:T(256)S(1)} %get-tuple-element.113, f32[256]{0:T(256)S(1)} %get-tuple-element.112, bf16[256,1024]{1,0:T(8,128)(2,1)S(1)} %copy-done.15, f32[1024]{0:T(1024)S(1)} %copy-done.27, bf16[256,2048]{1,0:T(8,128)(2,1)S(1)} %select_select_fusion, ...), kind=kOutput, calls=%fused_computation.203 | convolution fusion | flops 1077935616 | bytes 6823936 | tf_op jit(solution)/shard_map/dot_general | solution.py:229
  206.5 3.0 %all-reduce = (f32[256]{0:T(256)S(1)}, f32[256]{0:T(256)}) all-reduce(f32[256]{0:T(256)S(1)} %get-tuple-element.60, f32[256]{0:T(256)S(1)} %get-tuple-element.59), channel_id=1, replica_groups=mesh['sp'=16,'tp'=2] {'tp'}, use_global_device_ids=true, to_apply=%region_10.11 | all-reduce | flops 512 | bytes 4096 | tf_op jit(solution)/shard_map/psum | solution.py:233
  210.2 2.0 collective-permute-done.6
  212.2 7.1 %collective-permute-done.4 = bf16[2,2,2,128,384]{4,3,0,1,2:T(8,128)(2,1)} collective-permute-done((bf16[2,2,2,128,384]{4,3,0,1,2:T(8,128)(2,1)}, bf16[2,2,2,128,384]{4,3,0,1,2:T(8,128)(2,1)}, u32[]{:S(2)}, u32[]{:S(2)}) %collective-permute-start.4) | collective-permute-done | bytes 786464 | tf_op jit(solution)/shard_map/ppermute | solution.py:82
  219.3 1.7 collective-permute-done.5
  221.0 1.3 convert_add_fusion.1
  222.3 1.8 collective-permute-start.7
  224.7 1.1 convert_add_fusion.2
  226.9 5.8 %collective-permute-done.9 = bf16[2,2,128,256]{3,2,0,1:T(8,128)(2,1)S(1)} collective-permute-done((bf16[2,2,128,256]{3,2,0,1:T(8,128)(2,1)S(1)}, bf16[2,2,128,256]{3,2,0,1:T(8,128)(2,1)S(1)}, u32[]{:S(2)}, u32[]{:S(2)}) %collective-permute-start.9) | collective-permute-done | bytes 262176 | tf_op jit(solution)/shard_map/ppermute | solution.py:82
  232.7 1.3 collective-permute-done.8
  236.1 1.3 collective-permute-start.16
  237.4 4.5 %collective-permute-start.17 = (bf16[15,1024]{1,0:T(8,128)(2,1)S(1)}, bf16[15,1024]{1,0:T(8,128)(2,1)S(1)}, u32[]{:S(2)}, u32[]{:S(2)}) collective-permute-start(bf16[15,1024]{1,0:T(8,128)(2,1)S(1)} %get-tuple-element.80), channel_id=1, source_target_pairs={{0,2},{2,4},{4,6},{6,8},{8,10},{10,12},{12,14},{14,16},{16,18},{18... | collective-permute-start | bytes 92168 | tf_op jit(solution)/shard_map/ppermute | solution.py:14
  242.1 2.8 %collective-permute-start.15 = (bf16[128,256]{1,0:T(8,128)(2,1)S(1)}, bf16[128,256]{1,0:T(8,128)(2,1)S(1)}, u32[]{:S(2)}, u32[]{:S(2)}) collective-permute-start(bf16[128,256]{1,0:T(8,128)(2,1)S(1)} %fusion.86), channel_id=1, source_target_pairs={{0,16},{2,18},{4,20},{6,22},{8,24},{10,26},{12,28},{14,30},{16,0},... | collective-permute-start | bytes 196616 | tf_op jit(solution)/shard_map/ppermute | solution.py:82
  245.2 2.8 %collective-permute-start.13 = (bf16[128,384]{1,0:T(8,128)(2,1)S(1)}, bf16[128,384]{1,0:T(8,128)(2,1)S(1)}, u32[]{:S(2)}, u32[]{:S(2)}) collective-permute-start(bf16[128,384]{1,0:T(8,128)(2,1)S(1)} %fusion.84), channel_id=1, source_target_pairs={{0,16},{2,18},{4,20},{6,22},{8,24},{10,26},{12,28},{14,30},{16,0},... | collective-permute-start | bytes 294920 | tf_op jit(solution)/shard_map/ppermute | solution.py:82
  248.0 5.4 %add_convert_fusion.3 = bf16[256,1024]{1,0:T(8,128)(2,1)} fusion(bf16[256,1024]{1,0:T(8,128)(2,1)S(1)} %fusion.38, bf16[15,1024]{1,0:T(8,128)(2,1)S(1)} %collective-permute-done.17, bf16[15,1024]{1,0:T(8,128)(2,1)S(1)} %collective-permute-done.16, f32[1024]{0:T(1024)S(1)} %bitcast.180, f32[1024]{0:T(1024)S(1)} %bitcast.181, f32[1024]{0:T(1024)S(1)} %bitcast.183, ...), kind=kLoop, calls=%fused_computation.86 | loop fusion | flops 47972352 | bytes 1236992 | tf_op jit(solution)/shard_map/convert_element_type | solution.py:246
  253.6 1.1 collective-permute-done.13
  (120 shorter events, 14.4 us)
Async XLA Ops:
  0.6 71.6 %copy-start = (bf16[1,2048,512]{2,1,0:T(8,128)(2,1)S(1)}, bf16[1,2048,512]{2,1,0:T(8,128)(2,1)}, u32[]{:S(2)}) copy-start(bf16[1,2048,512]{2,1,0:T(8,128)(2,1)} %param.19) | copy-start | bytes 6291460
  6.0 8.5 %copy-start.24 = (f32[128,2]{0,1:T(2,128)S(1)}, f32[128,2]{0,1:T(2,128)}, u32[]{:S(2)}) copy-start(f32[128,2]{0,1:T(2,128)} %param.14) | copy-start | bytes 3076
  6.0 8.7 %copy-start.12 = (bf16[128,2048]{1,0:T(8,128)(2,1)S(1)}, bf16[128,2048]{1,0:T(8,128)(2,1)}, u32[]{:S(2)}) copy-start(bf16[128,2048]{1,0:T(8,128)(2,1)} %param.12) | copy-start | bytes 1572868
  6.0 51.6 %all-to-all-start = ((bf16[16,1,32,2048]{3,2,1,0:T(8,128)(2,1)}), bf16[16,1,32,2048]{3,2,1,0:T(8,128)(2,1)}, u32[]{:S(2)}, u32[]{:S(2)}) async-start(bf16[16,1,32,2048]{3,2,1,0:T(8,128)(2,1)} %bitcast.167), calls=%async_computation | async-start | bytes 4194304 | tf_op jit(solution)/shard_map/all_to_all | solution.py:192
  57.6 52.7 %all-to-all-start.1 = ((bf16[16,1,32,2048]{3,2,1,0:T(8,128)(2,1)}), bf16[16,1,32,2048]{3,2,1,0:T(8,128)(2,1)}, u32[]{:S(2)}, u32[]{:S(2)}) async-start(bf16[16,1,32,2048]{3,2,1,0:T(8,128)(2,1)} %bitcast.166), calls=%async_computation.1 | async-start | bytes 4194304 | tf_op jit(solution)/shard_map/all_to_all | solution.py:193
  67.7 8.5 %collective-permute-start = (bf16[512,2048]{1,0:T(8,128)(2,1)}, bf16[512,2048]{1,0:T(8,128)(2,1)S(1)}, u32[]{:S(2)}, u32[]{:S(2)}) collective-permute-start(bf16[512,2048]{1,0:T(8,128)(2,1)} %bitcast.2), channel_id=1, source_target_pairs={{0,1},{1,0},{2,3},{3,2},{4,5},{5,4},{6,7},{7,6},{8,9},{9,8},{10,11... | collective-permute-start | bytes 6291464 | tf_op jit(solution)/shard_map/ppermute | solution.py:105
  72.2 4.0 %copy-start.4 = (bf16[1,2048,512]{2,1,0:T(8,128)(2,1)S(1)}, bf16[1,2048,512]{2,1,0:T(8,128)(2,1)}, u32[]{:S(2)}) copy-start(bf16[1,2048,512]{2,1,0:T(8,128)(2,1)} %param.20) | copy-start | bytes 6291460
  76.2 2.3 copy-start.2
  110.3 4.4 %collective-permute-start.1 = (bf16[512,2048]{1,0:T(8,128)(2,1)}, bf16[512,2048]{1,0:T(8,128)(2,1)S(1)}, u32[]{:S(2)}, u32[]{:S(2)}) collective-permute-start(bf16[512,2048]{1,0:T(8,128)(2,1)} %bitcast.7), channel_id=1, source_target_pairs={{0,1},{1,0},{2,3},{3,2},{4,5},{5,4},{6,7},{7,6},{8,9},{9,8},{10,11... | collective-permute-start | bytes 6291464 | tf_op jit(solution)/shard_map/ppermute | solution.py:105
  114.7 4.6 %copy-start.8 = (bf16[512,2048]{1,0:T(8,128)(2,1)}, bf16[512,2048]{1,0:T(8,128)(2,1)S(1)}, u32[]{:S(2)}) copy-start(bf16[512,2048]{1,0:T(8,128)(2,1)S(1)} %collective-permute-done.1) | copy-start | bytes 6291460
  119.3 1.8 copy-start.5
  121.1 1.6 copy-start.19
  121.1 1.6 copy-start.21
  121.1 2.2 copy-start.26
  122.4 5.5 %collective-permute-start.2 = (bf16[512,2048]{1,0:T(8,128)(2,1)S(1)}, bf16[512,2048]{1,0:T(8,128)(2,1)S(1)}, u32[]{:S(2)}, u32[]{:S(2)}) collective-permute-start(bf16[512,2048]{1,0:T(8,128)(2,1)S(1)} %add_convert_fusion.1), channel_id=1, source_target_pairs={{0,1},{1,0},{2,3},{3,2},{4,5},{5,4},{6,7},{7,6},{8,9},{9,8},{10,11... | collective-permute-start | bytes 6291464 | tf_op jit(solution)/shard_map/ppermute | solution.py:135
  126.6 1.3 copy-start.16
  130.6 9.8 %copy-start.14 = (bf16[256,1024]{1,0:T(8,128)(2,1)S(1)}, bf16[256,1024]{1,0:T(8,128)(2,1)}, u32[]{:S(2)}) copy-start(bf16[256,1024]{1,0:T(8,128)(2,1)} %param.15) | copy-start | bytes 1572868
  130.6 12.7 %copy-start.17 = (bf16[512,512]{1,0:T(8,128)(2,1)S(1)}, bf16[512,512]{1,0:T(8,128)(2,1)}, u32[]{:S(2)}) copy-start(bf16[512,512]{1,0:T(8,128)(2,1)} %copy-done.16) | copy-start | bytes 1572868
  130.6 53.0 %all-to-all-start.2 = ((bf16[16,1,32,2048]{3,2,1,0:T(8,128)(2,1)}), bf16[16,1,32,2048]{3,2,1,0:T(8,128)(2,1)}, u32[]{:S(2)}, u32[]{:S(2)}) async-start(bf16[16,1,32,2048]{3,2,1,0:T(8,128)(2,1)} %bitcast.10), calls=%async_computation.2 | async-start | bytes 4194304 | tf_op jit(solution)/shard_map/all_to_all | solution.py:212
  146.2 3.1 %copy-start.20 = (f32[512,512]{1,0:T(8,128)S(1)}, f32[512,512]{1,0:T(8,128)}, u32[]{:S(2)}) copy-start(f32[512,512]{1,0:T(8,128)} %fusion.9) | copy-start | bytes 3145732
  146.2 3.1 %copy-start.22 = (f32[512,512]{1,0:T(8,128)S(1)}, f32[512,512]{1,0:T(8,128)}, u32[]{:S(2)}) copy-start(f32[512,512]{1,0:T(8,128)} %fusion.17) | copy-start | bytes 3145732
  149.3 3.2 %copy-start.3 = (bf16[512,2048]{1,0:T(8,128)(2,1)S(1)}, bf16[512,2048]{1,0:T(8,128)(2,1)}, u32[]{:S(2)}) copy-start(bf16[512,2048]{1,0:T(8,128)(2,1)} %copy-done.2) | copy-start | bytes 6291460
  149.3 3.2 %copy-start.11 = (bf16[512,512]{1,0:T(8,128)(2,1)S(1)}, bf16[512,512]{1,0:T(8,128)(2,1)}, u32[]{:S(2)}) copy-start(bf16[512,512]{1,0:T(8,128)(2,1)} %copy-done.10) | copy-start | bytes 1572868
  155.9 3.4 %copy-start.6 = (f32[512,512]{1,0:T(8,128)S(1)}, f32[512,512]{1,0:T(8,128)}, u32[]{:S(2)}) copy-start(f32[512,512]{1,0:T(8,128)} %fusion.7) | copy-start | bytes 3145732
  155.9 3.4 %copy-start.7 = (f32[512,512]{1,0:T(8,128)S(1)}, f32[512,512]{1,0:T(8,128)}, u32[]{:S(2)}) copy-start(f32[512,512]{1,0:T(8,128)} %fusion.15) | copy-start | bytes 3145732
  155.9 3.4 %copy-start.9 = (bf16[512,2048]{1,0:T(8,128)(2,1)S(1)}, bf16[512,2048]{1,0:T(8,128)(2,1)}, u32[]{:S(2)}) copy-start(bf16[512,2048]{1,0:T(8,128)(2,1)} %copy-done.8) | copy-start | bytes 6291460
  159.3 24.2 %copy-start.13 = (bf16[128,2048]{1,0:T(8,128)(2,1)S(1)}, bf16[128,2048]{1,0:T(8,128)(2,1)}, u32[]{:S(2)}) copy-start(bf16[128,2048]{1,0:T(8,128)(2,1)} %param.12) | copy-start | bytes 1572868
  162.7 23.0 %copy-start.23 = (f32[31,1024]{1,0:T(8,128)S(1)}, f32[31,1024]{1,0:T(8,128)}, u32[]{:S(2)}) copy-start(f32[31,1024]{1,0:T(8,128)} %param.16) | copy-start | bytes 380932
  183.5 4.5 %copy-start.15 = (bf16[256,1024]{1,0:T(8,128)(2,1)S(1)}, bf16[256,1024]{1,0:T(8,128)(2,1)}, u32[]{:S(2)}) copy-start(bf16[256,1024]{1,0:T(8,128)(2,1)} %param.15) | copy-start | bytes 1572868
  183.5 4.5 %copy-start.27 = (f32[1024]{0:T(1024)S(1)}, f32[1024]{0:T(1024)}, u32[]{:S(2)}) copy-start(f32[1024]{0:T(1024)} %param.17) | copy-start | bytes 12292
  185.7 2.0 collective-permute-start.3
  192.4 11.1 %copy-start.25 = (bf16[1024,2048]{1,0:T(8,128)(2,1)S(1)}, bf16[1024,2048]{1,0:T(8,128)(2,1)}, u32[]{:S(2)}) copy-start(bf16[1024,2048]{1,0:T(8,128)(2,1)} %param.18) | copy-start | bytes 12582916
  193.5 18.7 %collective-permute-start.6 = (bf16[2,2,2,128,256]{4,3,0,1,2:T(8,128)(2,1)}, bf16[2,2,2,128,256]{4,3,0,1,2:T(8,128)(2,1)}, u32[]{:S(2)}, u32[]{:S(2)}) collective-permute-start(bf16[2,2,2,128,256]{4,3,0,1,2:T(8,128)(2,1)} %bitcast.165), channel_id=1, source_target_pairs={{0,8},{2,10},{4,12},{6,14},{8,0},{10,2},{12,4},{14,6},{16,24},{18,... | collective-permute-start | bytes 1572872 | tf_op jit(solution)/shard_map/ppermute | solution.py:82
  199.7 19.6 %collective-permute-start.4 = (bf16[2,2,2,128,384]{4,3,0,1,2:T(8,128)(2,1)}, bf16[2,2,2,128,384]{4,3,0,1,2:T(8,128)(2,1)}, u32[]{:S(2)}, u32[]{:S(2)}) collective-permute-start(bf16[2,2,2,128,384]{4,3,0,1,2:T(8,128)(2,1)} %bitcast.164), channel_id=1, source_target_pairs={{0,2},{2,0},{4,6},{6,4},{8,10},{10,8},{12,14},{14,12},{16,18},{18,... | collective-permute-start | bytes 2359304 | tf_op jit(solution)/shard_map/ppermute | solution.py:82
  201.1 19.9 %collective-permute-start.5 = (bf16[2,2,2,128,384]{4,3,0,2,1:T(8,128)(2,1)}, bf16[2,2,2,128,384]{4,3,0,2,1:T(8,128)(2,1)S(1)}, u32[]{:S(2)}, u32[]{:S(2)}) collective-permute-start(bf16[2,2,2,128,384]{4,3,0,2,1:T(8,128)(2,1)} %bitcast.163), channel_id=1, source_target_pairs={{0,4},{2,6},{4,0},{6,2},{8,12},{10,14},{12,8},{14,10},{16,20},{18,... | collective-permute-start | bytes 2359304 | tf_op jit(solution)/shard_map/ppermute | solution.py:82
  222.3 10.4 %collective-permute-start.7 = (bf16[2,2,128,384]{3,2,0,1:T(8,128)(2,1)S(1)}, bf16[2,2,128,384]{3,2,0,1:T(8,128)(2,1)S(1)}, u32[]{:S(2)}, u32[]{:S(2)}) collective-permute-start(bf16[2,2,128,384]{3,2,0,1:T(8,128)(2,1)S(1)} %fusion.76), channel_id=1, source_target_pairs={{0,4},{2,6},{4,0},{6,2},{8,12},{10,14},{12,8},{14,10},{16,20},{18,... | collective-permute-start | bytes 1179656 | tf_op jit(solution)/shard_map/ppermute | solution.py:82
  224.3 2.3 copy-start.18
  224.4 9.6 %collective-permute-start.8 = (bf16[2,2,128,384]{3,2,0,1:T(8,128)(2,1)S(1)}, bf16[2,2,128,384]{3,2,0,1:T(8,128)(2,1)S(1)}, u32[]{:S(2)}, u32[]{:S(2)}) collective-permute-start(bf16[2,2,128,384]{3,2,0,1:T(8,128)(2,1)S(1)} %fusion.77), channel_id=1, source_target_pairs={{0,8},{2,10},{4,12},{6,14},{8,0},{10,2},{12,4},{14,6},{16,24},{18,... | collective-permute-start | bytes 1179656 | tf_op jit(solution)/shard_map/ppermute | solution.py:82
  225.9 6.8 %collective-permute-start.9 = (bf16[2,2,128,256]{3,2,0,1:T(8,128)(2,1)S(1)}, bf16[2,2,128,256]{3,2,0,1:T(8,128)(2,1)S(1)}, u32[]{:S(2)}, u32[]{:S(2)}) collective-permute-start(bf16[2,2,128,256]{3,2,0,1:T(8,128)(2,1)S(1)} %fusion.78), channel_id=1, source_target_pairs={{0,2},{2,0},{4,6},{6,4},{8,10},{10,8},{12,14},{14,12},{16,18},{18,... | collective-permute-start | bytes 786440 | tf_op jit(solution)/shard_map/ppermute | solution.py:82
  234.2 7.7 %collective-permute-start.12 = (bf16[2,128,256]{2,1,0:T(8,128)(2,1)S(1)}, bf16[2,128,256]{2,1,0:T(8,128)(2,1)S(1)}, u32[]{:S(2)}, u32[]{:S(2)}) collective-permute-start(bf16[2,128,256]{2,1,0:T(8,128)(2,1)S(1)} %fusion.83), channel_id=1, source_target_pairs={{0,4},{2,6},{4,0},{6,2},{8,12},{10,14},{12,8},{14,10},{16,20},{18,... | collective-permute-start | bytes 393224 | tf_op jit(solution)/shard_map/ppermute | solution.py:82
  234.8 7.1 %collective-permute-start.11 = (bf16[2,128,384]{2,1,0:T(8,128)(2,1)S(1)}, bf16[2,128,384]{2,1,0:T(8,128)(2,1)S(1)}, u32[]{:S(2)}, u32[]{:S(2)}) collective-permute-start(bf16[2,128,384]{2,1,0:T(8,128)(2,1)S(1)} %fusion.80), channel_id=1, source_target_pairs={{0,2},{2,0},{4,6},{6,4},{8,10},{10,8},{12,14},{14,12},{16,18},{18,... | collective-permute-start | bytes 589832 | tf_op jit(solution)/shard_map/ppermute | solution.py:82
  235.6 6.4 %collective-permute-start.10 = (bf16[2,128,384]{2,1,0:T(8,128)(2,1)S(1)}, bf16[2,128,384]{2,1,0:T(8,128)(2,1)S(1)}, u32[]{:S(2)}, u32[]{:S(2)}) collective-permute-start(bf16[2,128,384]{2,1,0:T(8,128)(2,1)S(1)} %fusion.79), channel_id=1, source_target_pairs={{0,8},{2,10},{4,12},{6,14},{8,0},{10,2},{12,4},{14,6},{16,24},{18,... | collective-permute-start | bytes 589832 | tf_op jit(solution)/shard_map/ppermute | solution.py:82
  236.1 11.9 %collective-permute-start.16 = (bf16[15,1024]{1,0:T(8,128)(2,1)S(1)}, bf16[15,1024]{1,0:T(8,128)(2,1)S(1)}, u32[]{:S(2)}, u32[]{:S(2)}) collective-permute-start(bf16[15,1024]{1,0:T(8,128)(2,1)S(1)} %get-tuple-element.79), channel_id=1, source_target_pairs={{2,0},{4,2},{6,4},{8,6},{10,8},{12,10},{14,12},{16,14},{18,16},{20... | collective-permute-start | bytes 92168 | tf_op jit(solution)/shard_map/ppermute | solution.py:17
  237.4 10.6 %collective-permute-start.17 = (bf16[15,1024]{1,0:T(8,128)(2,1)S(1)}, bf16[15,1024]{1,0:T(8,128)(2,1)S(1)}, u32[]{:S(2)}, u32[]{:S(2)}) collective-permute-start(bf16[15,1024]{1,0:T(8,128)(2,1)S(1)} %get-tuple-element.80), channel_id=1, source_target_pairs={{0,2},{2,4},{4,6},{6,8},{8,10},{10,12},{12,14},{14,16},{16,18},{18... | collective-permute-start | bytes 92168 | tf_op jit(solution)/shard_map/ppermute | solution.py:14
  242.1 13.6 %copy-start.1 = (bf16[1,2048,512]{2,1,0:T(8,128)(2,1)S(1)}, bf16[1,2048,512]{2,1,0:T(8,128)(2,1)}, u32[]{:S(2)}) copy-start(bf16[1,2048,512]{2,1,0:T(8,128)(2,1)} %param.19) | copy-start | bytes 6291460
  242.1 11.3 %collective-permute-start.15 = (bf16[128,256]{1,0:T(8,128)(2,1)S(1)}, bf16[128,256]{1,0:T(8,128)(2,1)S(1)}, u32[]{:S(2)}, u32[]{:S(2)}) collective-permute-start(bf16[128,256]{1,0:T(8,128)(2,1)S(1)} %fusion.86), channel_id=1, source_target_pairs={{0,16},{2,18},{4,20},{6,22},{8,24},{10,26},{12,28},{14,30},{16,0},... | collective-permute-start | bytes 196616 | tf_op jit(solution)/shard_map/ppermute | solution.py:82
  245.0 8.6 %collective-permute-start.14 = (bf16[128,384]{1,0:T(8,128)(2,1)S(1)}, bf16[128,384]{1,0:T(8,128)(2,1)S(1)}, u32[]{:S(2)}, u32[]{:S(2)}) collective-permute-start(bf16[128,384]{1,0:T(8,128)(2,1)S(1)} %fusion.85), channel_id=1, source_target_pairs={{0,16},{2,18},{4,20},{6,22},{8,24},{10,26},{12,28},{14,30},{16,0},... | collective-permute-start | bytes 294920 | tf_op jit(solution)/shard_map/ppermute | solution.py:82
  245.2 9.5 %collective-permute-start.13 = (bf16[128,384]{1,0:T(8,128)(2,1)S(1)}, bf16[128,384]{1,0:T(8,128)(2,1)S(1)}, u32[]{:S(2)}, u32[]{:S(2)}) collective-permute-start(bf16[128,384]{1,0:T(8,128)(2,1)S(1)} %fusion.84), channel_id=1, source_target_pairs={{0,16},{2,18},{4,20},{6,22},{8,24},{10,26},{12,28},{14,30},{16,0},... | collective-permute-start | bytes 294920 | tf_op jit(solution)/shard_map/ppermute | solution.py:82
  (1 other events, 1.3 us)

commit v4 on v3

--- a/solution.py
+++ b/solution.py
@@ -179,23 +179,51 @@
     channel_sum, squares = lax.psum(
         (jnp.sum(values, axis=1), jnp.sum(values * values, axis=1)), "tp"
     )
+    half = sp_count // 2
+    side = lax.axis_index("sp") // half
     target = slot_targets(routes, experts, capacity)
     slot_ids = jnp.arange(experts * capacity, dtype=jnp.int32)
-    holds = slot_ids[:, None, None] == target[None, :, :]
-    chosen = jnp.any(holds, axis=2).astype(jnp.bfloat16)
-    route_scale = jnp.sum(jnp.where(holds, route_weight[None, :, :], 0.0), axis=(1, 2))
-    inputs = jnp.dot(chosen, mid_rows, preferred_element_type=jnp.float32).astype(jnp.bfloat16)
-    cot_rows = jnp.dot(chosen, cotangent, preferred_element_type=jnp.float32)
+    chosen = jnp.any(slot_ids[:, None, None] == target[None, :, :], axis=2).astype(jnp.bfloat16)
+
+    def with_far(block):
+        far = lax.ppermute(block, "sp", [(i, (i + half) % sp_count) for i in range(sp_count)])
+        return jnp.concatenate([block, far], axis=0)
+
+    both_target, both_weight = with_far(target), with_far(route_weight)
+    expert = both_target // capacity - side * half * local_experts
+    origin = jnp.concatenate(
+        [jnp.full((token_count, 1), side), jnp.full((token_count, 1), 1 - side)], axis=0
+    )
+    place = (expert // local_experts * 2 + origin) * local_experts + expert % local_experts
+    place = place * capacity + both_target % capacity
+    place = jnp.where((expert >= 0) & (expert < half * local_experts), place, -1)
+    holds = slot_ids[:, None, None] == place[None, :, :]
+    sent = jnp.any(holds, axis=2).astype(jnp.bfloat16)
+    route_scale = jnp.sum(jnp.where(holds, both_weight[None, :, :], 0.0), axis=(1, 2))
+
+    def within_half(block):
+        return lax.all_to_all(
+            block.reshape(half, 2, local_experts, capacity, model_width),
+            "sp",
+            split_axis=0,
+            concat_axis=0,
+            axis_index_groups=[[s * half + i for i in range(half)] for s in range(2)],
+            tiled=True,
+        )
+
+    both_mid = with_far(mid_rows)
+    both_mid, near_cot = lax.optimization_barrier((both_mid, cotangent))
+    both_cot = with_far(near_cot)
+    inputs = jnp.dot(sent, both_mid, preferred_element_type=jnp.float32).astype(jnp.bfloat16)
+    got_in = within_half(inputs)
+    cot_rows = jnp.dot(sent, both_cot, preferred_element_type=jnp.float32)
     routed = (route_scale[:, None] * cot_rows).astype(jnp.bfloat16)
-    inputs = inputs.reshape(sp_count, local_experts, capacity, model_width)
-    routed = routed.reshape(sp_count, local_experts, capacity, model_width)
-    got_in = lax.all_to_all(inputs, "sp", split_axis=0, concat_axis=0, tiled=True)
-    got_cot = lax.all_to_all(routed, "sp", split_axis=0, concat_axis=0, tiled=True)
+    got_cot = within_half(routed)
     by_expert = (sp_count, local_experts, capacity, model_width)
     parts = [
         expert_backward(
-            got_in[:, e].reshape(sp_count * capacity, model_width),
-            got_cot[:, e].reshape(sp_count * capacity, model_width),
+            got_in[:, :, e].reshape(sp_count * capacity, model_width),
+            got_cot[:, :, e].reshape(sp_count * capacity, model_width),
             gate_weight[e],
             up_weight[e],
             down_weight[e],
@@ -207,7 +235,11 @@
         jnp.stack([part[i] for part in parts], axis=0) for i in range(3)
     )
     back_rows = jnp.stack(
-        [part[3].reshape(sp_count, capacity, model_width) for part in parts], axis=1
+        [
+            part[3].reshape(half, 2, capacity, model_width).transpose(1, 0, 2, 3)
+            for part in parts
+        ],
+        axis=2,
     ).reshape(by_expert)
     returned = lax.all_to_all(back_rows, "sp", split_axis=0, concat_axis=0, tiled=True)
     returned, gate_grad, up_grad, down_grad, channel_sum, squares = lax.optimization_barrier(

time: 256 us -> 251 us (0.980)
  waiting for transfers between devices: 117 us -> 111 us
    all_to_all x2, waiting for transfers between devices: 70.5 us -> 12.6 us  [within_half(): lax.all_to_all(block.reshape(half, 2, local_experts, capacity, model_widt...]
    ppermute x0 -> x4, waiting for transfers between devices: none -> 52 us  [with_far(): lax.ppermute(block, 'sp', [(i, (i + half) % sp_count) for i in range(sp_c...]
    ppermute x0 -> x4, starting transfers between devices: none -> 7.34 us  [with_far(): lax.ppermute(block, 'sp', [(i, (i + half) % sp_count) for i in range(sp_c...]
    all_to_all x1, starting transfers between devices: 9.81 us -> 4.57 us  [per_device(): lax.all_to_all(back_rows, 'sp', split_axis=0, concat_axis=0, tiled=True)]
    all_to_all x2, starting transfers between devices: 18.6 us -> 15.9 us  [within_half(): lax.all_to_all(block.reshape(half, 2, local_experts, capacity, model_widt...]
  transfers between devices with their start and end apart: 21 -> 25, of which waited for: 12 -> 13; matrix products, arithmetic and copies ran while one was open for 20% -> 22% of each run, Pallas kernels for 0% -> 0%
where the time goes in v4:
time: 251 us; the launch traced here: 250 us
  waiting for transfers between devices  111 us (44%)
  matrix products  56.3 us (22%)
  starting transfers between devices  54.5 us (22%)
  other arithmetic  14.2 us (6%)
  local copies, waits for them, and re-layouts  7.4 us (3%)
  blocking collectives  5.69 us (2%)
    ppermute x4, waiting for transfers between devices, with_far(): lax.ppermute(block, 'sp', [(i, (i + half) % sp_count) for i in range(sp_c...  52 us
    dot_general x10, matrix products, row_product(): lax.dot_general(rows, matrix, (((1,), (dim,)), ((), ())), preferred_eleme...  25.9 us
    dot_general x7, matrix products, transposed_product(): lax.dot_general(left, right, (((0,), (0,)), ((), ())), preferred_element_...  20.9 us
    all_to_all x1, waiting for transfers between devices, per_device(): lax.all_to_all(back_rows, 'sp', split_axis=0, concat_axis=0, tiled=True)  20.8 us
    ppermute x12, starting transfers between devices, reduced_products(): lax.ppermute(block, axis, [(i, i ^ 1 << order[step]) for i in range(count)])  20.6 us
    ppermute x12, waiting for transfers between devices, reduced_products(): lax.ppermute(block, axis, [(i, i ^ 1 << order[step]) for i in range(count)])  19 us
    all_to_all x2, starting transfers between devices, within_half(): lax.all_to_all(block.reshape(half, 2, local_experts, capacity, model_widt...  15.9 us
    all_to_all x2, waiting for transfers between devices, within_half(): lax.all_to_all(block.reshape(half, 2, local_experts, capacity, model_widt...  12.6 us
  transfers between devices with their start and end apart: 25, of which 13 were waited for; matrix products, arithmetic and copies ran while one was open for 22% of the time, Pallas kernels for 0%

profile of v4, /device:TPU:0, one launch (start us, length us, event | category | flops | bytes accessed | tf_op | source)
XLA Modules:
  0.0 249.9 jit_solution(11022024559254988577)
XLA Ops:
  0.6 4.1 %collective-permute-start.1 = (bf16[128,2048]{1,0:T(8,128)(2,1)}, bf16[128,2048]{1,0:T(8,128)(2,1)S(1)}, u32[]{:S(2)}, u32[]{:S(2)}) collective-permute-start(bf16[128,2048]{1,0:T(8,128)(2,1)} %param.11), channel_id=1, source_target_pairs={{0,16},{2,18},{4,20},{6,22},{8,24},{10,26},{12,28},{14,30},{16,0},... | collective-permute-start | bytes 1572872 | tf_op jit(solution)/shard_map/ppermute | solution.py:189
  7.0 21.2 %collective-permute-done = s32[128,2]{0,1:T(2,128)S(1)} collective-permute-done((s32[128,2]{0,1:T(2,128)S(1)}, s32[128,2]{0,1:T(2,128)S(1)}, u32[]{:S(2)}, u32[]{:S(2)}) %collective-permute-start) | collective-permute-done | bytes 1056 | tf_op jit(solution)/shard_map/ppermute | solution.py:189
  29.6 2.0 convolution_convert_fusion.1
  31.6 4.5 %all-to-all-start = ((bf16[8,2,1,32,2048]{4,3,1,2,0:T(8,128)(2,1)}), bf16[8,2,1,32,2048]{4,3,1,2,0:T(8,128)(2,1)}, u32[]{:S(2)}, u32[]{:S(2)}) async-start(bf16[8,2,1,32,2048]{4,3,1,2,0:T(8,128)(2,1)} %bitcast.168), calls=%async_computation | async-start | bytes 4194304 | tf_op jit(solution)/shard_map/all_to_all | solution.py:205
  36.1 3.0 %collective-permute-start.4 = (bf16[128,2048]{1,0:T(8,128)(2,1)S(1)}, bf16[128,2048]{1,0:T(8,128)(2,1)S(1)}, u32[]{:S(2)}, u32[]{:S(2)}) collective-permute-start(bf16[128,2048]{1,0:T(8,128)(2,1)S(1)} %copy-done.21), channel_id=1, source_target_pairs={{0,16},{2,18},{4,20},{6,22},{8,24},{10,26},{12,28},{14,30},{16,0},... | collective-permute-start | bytes 1572872 | tf_op jit(solution)/shard_map/ppermute | solution.py:189
  39.2 30.7 %collective-permute-done.3 = f32[128,2]{0,1:T(2,128)S(1)} collective-permute-done((f32[128,2]{0,1:T(2,128)S(1)}, f32[128,2]{0,1:T(2,128)S(1)}, u32[]{:S(2)}, u32[]{:S(2)}) %collective-permute-start.3) | collective-permute-done | bytes 1056 | tf_op jit(solution)/shard_map/ppermute | solution.py:189
  70.1 2.0 multiply_convert_fusion
  72.1 11.4 %all-to-all-start.1 = ((bf16[8,2,1,32,2048]{4,3,1,2,0:T(8,128)(2,1)}), bf16[8,2,1,32,2048]{4,3,1,2,0:T(8,128)(2,1)}, u32[]{:S(2)}, u32[]{:S(2)}) async-start(bf16[8,2,1,32,2048]{4,3,1,2,0:T(8,128)(2,1)} %bitcast.172), calls=%async_computation.1 | async-start | bytes 4194304 | tf_op jit(solution)/shard_map/all_to_all | solution.py:205
  83.5 4.4 %fusion.9 = f32[512,512]{1,0:T(8,128)} fusion(bf16[512,2048]{1,0:T(8,128)(2,1)} %bitcast.2, bf16[1,2048,512]{2,1,0:T(8,128)(2,1)} %param.20), kind=kOutput, calls=%fused_computation.47 | convolution fusion | flops 1073741824 | bytes 5242880 | tf_op jit(solution)/shard_map/dot_general | solution.py:91
  88.0 4.0 %fusion.17 = f32[512,512]{1,0:T(8,128)} fusion(bf16[512,2048]{1,0:T(8,128)(2,1)} %bitcast.2, bf16[1,2048,512]{2,1,0:T(8,128)(2,1)S(1)} %copy-done), kind=kOutput, calls=%fused_computation.55 | convolution fusion | flops 1073741824 | bytes 5242880 | tf_op jit(solution)/shard_map/dot_general | solution.py:91
  92.0 2.3 fusion.7
  94.2 2.2 fusion.15
  96.4 12.6 %all-to-all-done.1 = bf16[8,2,1,32,2048]{4,3,1,2,0:T(8,128)(2,1)} async-done(((bf16[8,2,1,32,2048]{4,3,1,2,0:T(8,128)(2,1)}), bf16[8,2,1,32,2048]{4,3,1,2,0:T(8,128)(2,1)}, u32[]{:S(2)}, u32[]{:S(2)}) %all-to-all-start.1) | async-done | bytes 2097184 | tf_op jit(solution)/shard_map/all_to_all | solution.py:205
  109.1 4.4 %collective-permute-done.5 = bf16[512,2048]{1,0:T(8,128)(2,1)S(1)} collective-permute-done((bf16[512,2048]{1,0:T(8,128)(2,1)}, bf16[512,2048]{1,0:T(8,128)(2,1)S(1)}, u32[]{:S(2)}, u32[]{:S(2)}) %collective-permute-start.5) | collective-permute-done | bytes 2097184 | tf_op jit(solution)/shard_map/ppermute | solution.py:105
  113.5 4.6 %multiply_convert_fusion.3 = (bf16[512,512]{1,0:T(8,128)(2,1)S(1)}, bf16[512,512]{1,0:T(8,128)(2,1)S(1)}) fusion(f32[512,512]{1,0:T(8,128)} %fusion.15, f32[512,512]{1,0:T(8,128)} %fusion.7, bf16[512,2048]{1,0:T(8,128)(2,1)S(1)} %collective-permute-done.5, bf16[1,512,2048]{2,1,0:T(8,128)(2,1)} %param.21), kind=kOutput, calls=%fused_computation.93 | convolution fusion | flops 1077149696 | bytes 7340032 | tf_op jit(solution)/shard_map/dot_general | solution.py:91
  119.9 1.3 add_convert_fusion.1
  122.1 3.3 %multiply_convert_fusion.5 = (bf16[512,512]{1,0:T(8,128)(2,1)S(1)}, bf16[512,512]{1,0:T(8,128)(2,1)S(1)}) fusion(f32[512,512]{1,0:T(8,128)S(1)} %copy-done.19, f32[512,512]{1,0:T(8,128)S(1)} %copy-done.17, bf16[512,2048]{1,0:T(8,128)(2,1)} %bitcast.7, bf16[1,512,2048]{2,1,0:T(8,128)(2,1)S(1)} %copy-done.26), kind=kOutput, calls=%fused_computation.97 | convolution fusion | flops 1077149696 | bytes 7340032 | tf_op jit(solution)/shard_map/dot_general | solution.py:91
  126.7 1.3 add_convert_fusion
  128.0 1.6 copy.61
  129.6 4.6 %all-to-all-start.2 = ((bf16[16,1,32,2048]{3,2,1,0:T(8,128)(2,1)}), bf16[16,1,32,2048]{3,2,1,0:T(8,128)(2,1)}, u32[]{:S(2)}, u32[]{:S(2)}) async-start(bf16[16,1,32,2048]{3,2,1,0:T(8,128)(2,1)} %bitcast.12), calls=%async_computation.2 | async-start | bytes 4194304 | tf_op jit(solution)/shard_map/all_to_all | solution.py:244
  134.4 2.7 %all-reduce.2 = (f32[256]{0:T(256)S(1)}, f32[256]{0:T(256)S(1)}) all-reduce(f32[256]{0:T(256)S(1)} %get-tuple-element.66, f32[256]{0:T(256)S(1)} %get-tuple-element.65), channel_id=1, replica_groups=mesh['sp'=16,'tp'=2] {'tp'}, use_global_device_ids=true, to_apply=%region_4.5 | all-reduce | flops 512 | bytes 4096 | tf_op jit(solution)/shard_map/psum | solution.py:179
  137.2 2.9 %fusion.103 = f32[2048,512]{1,0:T(8,128)S(1)} fusion(bf16[512,2048]{1,0:T(8,128)(2,1)} %bitcast.2, bf16[512,512]{1,0:T(8,128)(2,1)S(1)} %copy-done.15), kind=kOutput, calls=%fused_computation.225 | convolution fusion | flops 1073741824 | bytes 6815744 | tf_op jit(solution)/shard_map/dot_general | solution.py:97
  140.1 3.0 %fusion.102 = f32[2048,512]{1,0:T(8,128)S(1)} fusion(bf16[512,2048]{1,0:T(8,128)(2,1)} %bitcast.2, bf16[512,512]{1,0:T(8,128)(2,1)S(1)} %get-tuple-element.74), kind=kOutput, calls=%fused_computation.224 | convolution fusion | flops 1073741824 | bytes 6815744 | tf_op jit(solution)/shard_map/dot_general | solution.py:97
  143.2 3.1 %fusion.46 = f32[512,2048]{1,0:T(8,128)S(1)} fusion(bf16[512,2048]{1,0:T(8,128)(2,1)} %bitcast.7, f32[512,512]{1,0:T(8,128)S(1)} %copy-done.18, f32[512,512]{1,0:T(8,128)S(1)} %copy-done.20), kind=kOutput, calls=%fused_computation.112 | convolution fusion | flops 1075314688 | bytes 8388608 | tf_op jit(solution)/shard_map/dot_general | solution.py:97
  146.3 3.4 %add_bitcast_fusion.1 = f32[1,2048,512]{2,1,0:T(8,128)} fusion(f32[2048,512]{1,0:T(8,128)S(1)} %fusion.103, bf16[512,2048]{1,0:T(8,128)(2,1)S(1)} %copy-done.3, bf16[512,512]{1,0:T(8,128)(2,1)S(1)} %copy-done.11), kind=kOutput, calls=%fused_computation.1 | convolution fusion | flops 1074790400 | bytes 11010048 | tf_op jit(solution)/shard_map/dot_general | solution.py:97
  149.7 3.4 %add_bitcast_fusion.2 = f32[1,2048,512]{2,1,0:T(8,128)} fusion(f32[2048,512]{1,0:T(8,128)S(1)} %fusion.102, bf16[512,2048]{1,0:T(8,128)(2,1)S(1)} %copy-done.3, bf16[512,512]{1,0:T(8,128)(2,1)S(1)} %get-tuple-element.76), kind=kOutput, calls=%fused_computation.2 | convolution fusion | flops 1074790400 | bytes 11010048 | tf_op jit(solution)/shard_map/dot_general | solution.py:97
  153.2 3.4 %add_bitcast_fusion = f32[1,512,2048]{2,1,0:T(8,128)} fusion(f32[512,2048]{1,0:T(8,128)S(1)} %fusion.46, bf16[512,2048]{1,0:T(8,128)(2,1)S(1)} %copy-done.9, f32[512,512]{1,0:T(8,128)S(1)} %copy-done.6, f32[512,512]{1,0:T(8,128)S(1)} %copy-done.7), kind=kOutput, calls=%fused_computation | convolution fusion | flops 1076363264 | bytes 12582912 | tf_op jit(solution)/shard_map/dot_general | solution.py:97
  156.6 20.8 %all-to-all-done.2 = bf16[16,1,32,2048]{3,2,1,0:T(8,128)(2,1)} async-done(((bf16[16,1,32,2048]{3,2,1,0:T(8,128)(2,1)}), bf16[16,1,32,2048]{3,2,1,0:T(8,128)(2,1)}, u32[]{:S(2)}, u32[]{:S(2)}) %all-to-all-start.2) | async-done | bytes 2097184 | tf_op jit(solution)/shard_map/all_to_all | solution.py:244
  177.4 2.1 fusion
  179.8 1.7 collective-permute-done.7
  181.8 1.6 convolution_convert_fusion
  186.5 6.1 %collective-permute-start.10 = (bf16[2,2,2,128,256]{4,3,0,1,2:T(8,128)(2,1)}, bf16[2,2,2,128,256]{4,3,0,1,2:T(8,128)(2,1)}, u32[]{:S(2)}, u32[]{:S(2)}) collective-permute-start(bf16[2,2,2,128,256]{4,3,0,1,2:T(8,128)(2,1)} %bitcast.167), channel_id=1, source_target_pairs={{0,8},{2,10},{4,12},{6,14},{8,0},{10,2},{12,4},{14,6},{16,24},{18,... | collective-permute-start | bytes 1572872 | tf_op jit(solution)/shard_map/ppermute | solution.py:82
  192.6 1.6 collective-permute-start.8
  194.3 2.5 %collective-permute-start.9 = (bf16[2,2,2,128,384]{4,3,0,2,1:T(8,128)(2,1)S(1)}, bf16[2,2,2,128,384]{4,3,0,2,1:T(8,128)(2,1)}, u32[]{:S(2)}, u32[]{:S(2)}) collective-permute-start(bf16[2,2,2,128,384]{4,3,0,2,1:T(8,128)(2,1)S(1)} %bitcast.173), channel_id=1, source_target_pairs={{0,4},{2,6},{4,0},{6,2},{8,12},{10,14},{12,8},{14,10},{16,20},{18,... | collective-permute-start | bytes 2359304 | tf_op jit(solution)/shard_map/ppermute | solution.py:82
  196.8 3.0 %fusion.97 = (f32[256]{0:T(256)S(1)}, f32[256]{0:T(256)S(1)}, f32[256,1024]{1,0:T(8,128)}) fusion(f32[256]{0:T(256)S(1)} %get-tuple-element.117, f32[256]{0:T(256)S(1)} %get-tuple-element.116, bf16[256,1024]{1,0:T(8,128)(2,1)S(1)} %copy-done.13, f32[1024]{0:T(1024)S(1)} %copy-done.27, bf16[256,2048]{1,0:T(8,128)(2,1)S(1)} %select_select_fusion, ...), kind=kOutput, calls=%fused_computation.219 | convolution fusion | flops 1077935616 | bytes 6823936 | tf_op jit(solution)/shard_map/dot_general | solution.py:261
  199.8 3.0 %all-reduce.1 = (f32[256]{0:T(256)S(1)}, f32[256]{0:T(256)}) all-reduce(f32[256]{0:T(256)S(1)} %get-tuple-element.64, f32[256]{0:T(256)S(1)} %get-tuple-element.63), channel_id=1, replica_groups=mesh['sp'=16,'tp'=2] {'tp'}, use_global_device_ids=true, to_apply=%region_11.12 | all-reduce | flops 512 | bytes 4096 | tf_op jit(solution)/shard_map/psum | solution.py:265
  203.5 1.7 collective-permute-done.10
  205.2 7.1 %collective-permute-done.8 = bf16[2,2,2,128,384]{4,3,0,1,2:T(8,128)(2,1)} collective-permute-done((bf16[2,2,2,128,384]{4,3,0,1,2:T(8,128)(2,1)}, bf16[2,2,2,128,384]{4,3,0,1,2:T(8,128)(2,1)}, u32[]{:S(2)}, u32[]{:S(2)}) %collective-permute-start.8) | collective-permute-done | bytes 786464 | tf_op jit(solution)/shard_map/ppermute | solution.py:82
  212.3 1.9 collective-permute-done.9
  214.2 1.3 convert_add_fusion.1
  215.5 1.8 collective-permute-start.11
  217.3 1.3 convert_add_fusion
  221.2 5.8 %collective-permute-done.13 = bf16[2,2,128,256]{3,2,0,1:T(8,128)(2,1)S(1)} collective-permute-done((bf16[2,2,128,256]{3,2,0,1:T(8,128)(2,1)S(1)}, bf16[2,2,128,256]{3,2,0,1:T(8,128)(2,1)S(1)}, u32[]{:S(2)}, u32[]{:S(2)}) %collective-permute-start.13) | collective-permute-done | bytes 262176 | tf_op jit(solution)/shard_map/ppermute | solution.py:82
  230.3 1.3 collective-permute-start.20
  231.6 4.5 %collective-permute-start.21 = (bf16[15,1024]{1,0:T(8,128)(2,1)S(1)}, bf16[15,1024]{1,0:T(8,128)(2,1)S(1)}, u32[]{:S(2)}, u32[]{:S(2)}) collective-permute-start(bf16[15,1024]{1,0:T(8,128)(2,1)S(1)} %get-tuple-element.84), channel_id=1, source_target_pairs={{0,2},{2,4},{4,6},{6,8},{8,10},{10,12},{12,14},{14,16},{16,18},{18... | collective-permute-start | bytes 92168 | tf_op jit(solution)/shard_map/ppermute | solution.py:14
  236.4 2.8 %collective-permute-start.19 = (bf16[128,256]{1,0:T(8,128)(2,1)S(1)}, bf16[128,256]{1,0:T(8,128)(2,1)S(1)}, u32[]{:S(2)}, u32[]{:S(2)}) collective-permute-start(bf16[128,256]{1,0:T(8,128)(2,1)S(1)} %fusion.90), channel_id=1, source_target_pairs={{0,16},{2,18},{4,20},{6,22},{8,24},{10,26},{12,28},{14,30},{16,0},... | collective-permute-start | bytes 196616 | tf_op jit(solution)/shard_map/ppermute | solution.py:82
  239.5 2.8 %collective-permute-start.17 = (bf16[128,384]{1,0:T(8,128)(2,1)S(1)}, bf16[128,384]{1,0:T(8,128)(2,1)S(1)}, u32[]{:S(2)}, u32[]{:S(2)}) collective-permute-start(bf16[128,384]{1,0:T(8,128)(2,1)S(1)} %fusion.88), channel_id=1, source_target_pairs={{0,16},{2,18},{4,20},{6,22},{8,24},{10,26},{12,28},{14,30},{16,0},... | collective-permute-start | bytes 294920 | tf_op jit(solution)/shard_map/ppermute | solution.py:82
  242.3 5.4 %add_convert_fusion.3 = bf16[256,1024]{1,0:T(8,128)(2,1)} fusion(bf16[256,1024]{1,0:T(8,128)(2,1)S(1)} %fusion.38, bf16[15,1024]{1,0:T(8,128)(2,1)S(1)} %collective-permute-done.21, bf16[15,1024]{1,0:T(8,128)(2,1)S(1)} %collective-permute-done.20, f32[1024]{0:T(1024)S(1)} %bitcast.184, f32[1024]{0:T(1024)S(1)} %bitcast.185, f32[1024]{0:T(1024)S(1)} %bitcast.187, ...), kind=kLoop, calls=%fused_computation.90 | loop fusion | flops 47972352 | bytes 1236992 | tf_op jit(solution)/shard_map/convert_element_type | solution.py:278
  (135 shorter events, 20.7 us)
Async XLA Ops:
  0.6 87.4 %copy-start = (bf16[1,2048,512]{2,1,0:T(8,128)(2,1)S(1)}, bf16[1,2048,512]{2,1,0:T(8,128)(2,1)}, u32[]{:S(2)}) copy-start(bf16[1,2048,512]{2,1,0:T(8,128)(2,1)} %param.19) | copy-start | bytes 6291460
  0.6 27.8 %collective-permute-start.1 = (bf16[128,2048]{1,0:T(8,128)(2,1)}, bf16[128,2048]{1,0:T(8,128)(2,1)S(1)}, u32[]{:S(2)}, u32[]{:S(2)}) collective-permute-start(bf16[128,2048]{1,0:T(8,128)(2,1)} %param.11), channel_id=1, source_target_pairs={{0,16},{2,18},{4,20},{6,22},{8,24},{10,26},{12,28},{14,30},{16,0},... | collective-permute-start | bytes 1572872 | tf_op jit(solution)/shard_map/ppermute | solution.py:189
  6.8 21.4 %collective-permute-start = (s32[128,2]{0,1:T(2,128)S(1)}, s32[128,2]{0,1:T(2,128)S(1)}, u32[]{:S(2)}, u32[]{:S(2)}) collective-permute-start(s32[128,2]{0,1:T(2,128)S(1)} %multiply_add_fusion), channel_id=1, source_target_pairs={{0,16},{2,18},{4,20},{6,22},{8,24},{10,26},{12,28},{14,30},{16,0},... | collective-permute-start | bytes 3080 | tf_op jit(solution)/shard_map/ppermute | solution.py:189
  31.6 4.5 %copy-start.21 = (bf16[128,2048]{1,0:T(8,128)(2,1)S(1)}, bf16[128,2048]{1,0:T(8,128)(2,1)}, u32[]{:S(2)}) copy-start(bf16[128,2048]{1,0:T(8,128)(2,1)} %param.12) | copy-start | bytes 1572868
  31.6 7.5 %copy-start.24 = (f32[128,2]{0,1:T(2,128)S(1)}, f32[128,2]{0,1:T(2,128)}, u32[]{:S(2)}) copy-start(f32[128,2]{0,1:T(2,128)} %param.14) | copy-start | bytes 3076
  31.6 40.5 %all-to-all-start = ((bf16[8,2,1,32,2048]{4,3,1,2,0:T(8,128)(2,1)}), bf16[8,2,1,32,2048]{4,3,1,2,0:T(8,128)(2,1)}, u32[]{:S(2)}, u32[]{:S(2)}) async-start(bf16[8,2,1,32,2048]{4,3,1,2,0:T(8,128)(2,1)} %bitcast.168), calls=%async_computation | async-start | bytes 4194304 | tf_op jit(solution)/shard_map/all_to_all | solution.py:205
  36.1 34.0 %collective-permute-start.4 = (bf16[128,2048]{1,0:T(8,128)(2,1)S(1)}, bf16[128,2048]{1,0:T(8,128)(2,1)S(1)}, u32[]{:S(2)}, u32[]{:S(2)}) collective-permute-start(bf16[128,2048]{1,0:T(8,128)(2,1)S(1)} %copy-done.21), channel_id=1, source_target_pairs={{0,16},{2,18},{4,20},{6,22},{8,24},{10,26},{12,28},{14,30},{16,0},... | collective-permute-start | bytes 1572872 | tf_op jit(solution)/shard_map/ppermute | solution.py:189
  39.1 30.8 %collective-permute-start.3 = (f32[128,2]{0,1:T(2,128)S(1)}, f32[128,2]{0,1:T(2,128)S(1)}, u32[]{:S(2)}, u32[]{:S(2)}) collective-permute-start(f32[128,2]{0,1:T(2,128)S(1)} %copy-done.24), channel_id=1, source_target_pairs={{0,16},{2,18},{4,20},{6,22},{8,24},{10,26},{12,28},{14,30},{16,0},... | collective-permute-start | bytes 3080 | tf_op jit(solution)/shard_map/ppermute | solution.py:189
  72.1 36.9 %all-to-all-start.1 = ((bf16[8,2,1,32,2048]{4,3,1,2,0:T(8,128)(2,1)}), bf16[8,2,1,32,2048]{4,3,1,2,0:T(8,128)(2,1)}, u32[]{:S(2)}, u32[]{:S(2)}) async-start(bf16[8,2,1,32,2048]{4,3,1,2,0:T(8,128)(2,1)} %bitcast.172), calls=%async_computation.1 | async-start | bytes 4194304 | tf_op jit(solution)/shard_map/all_to_all | solution.py:205
  83.5 8.4 %collective-permute-start.2 = (bf16[512,2048]{1,0:T(8,128)(2,1)}, bf16[512,2048]{1,0:T(8,128)(2,1)S(1)}, u32[]{:S(2)}, u32[]{:S(2)}) collective-permute-start(bf16[512,2048]{1,0:T(8,128)(2,1)} %bitcast.2), channel_id=1, source_target_pairs={{0,1},{1,0},{2,3},{3,2},{4,5},{5,4},{6,7},{7,6},{8,9},{9,8},{10,11... | collective-permute-start | bytes 6291464 | tf_op jit(solution)/shard_map/ppermute | solution.py:105
  88.0 4.0 %copy-start.4 = (bf16[1,2048,512]{2,1,0:T(8,128)(2,1)S(1)}, bf16[1,2048,512]{2,1,0:T(8,128)(2,1)}, u32[]{:S(2)}) copy-start(bf16[1,2048,512]{2,1,0:T(8,128)(2,1)} %param.20) | copy-start | bytes 6291460
  92.0 2.3 copy-start.2
  109.1 4.4 %collective-permute-start.5 = (bf16[512,2048]{1,0:T(8,128)(2,1)}, bf16[512,2048]{1,0:T(8,128)(2,1)S(1)}, u32[]{:S(2)}, u32[]{:S(2)}) collective-permute-start(bf16[512,2048]{1,0:T(8,128)(2,1)} %bitcast.7), channel_id=1, source_target_pairs={{0,1},{1,0},{2,3},{3,2},{4,5},{5,4},{6,7},{7,6},{8,9},{9,8},{10,11... | collective-permute-start | bytes 6291464 | tf_op jit(solution)/shard_map/ppermute | solution.py:105
  113.4 4.6 %copy-start.8 = (bf16[512,2048]{1,0:T(8,128)(2,1)}, bf16[512,2048]{1,0:T(8,128)(2,1)S(1)}, u32[]{:S(2)}) copy-start(bf16[512,2048]{1,0:T(8,128)(2,1)S(1)} %collective-permute-done.5) | copy-start | bytes 6291460
  119.9 2.2 copy-start.26
  121.2 5.5 %collective-permute-start.6 = (bf16[512,2048]{1,0:T(8,128)(2,1)S(1)}, bf16[512,2048]{1,0:T(8,128)(2,1)S(1)}, u32[]{:S(2)}, u32[]{:S(2)}) collective-permute-start(bf16[512,2048]{1,0:T(8,128)(2,1)S(1)} %add_convert_fusion.1), channel_id=1, source_target_pairs={{0,1},{1,0},{2,3},{3,2},{4,5},{5,4},{6,7},{7,6},{8,9},{9,8},{10,11... | collective-permute-start | bytes 6291464 | tf_op jit(solution)/shard_map/ppermute | solution.py:135
  129.6 4.6 %copy-start.12 = (bf16[256,1024]{1,0:T(8,128)(2,1)S(1)}, bf16[256,1024]{1,0:T(8,128)(2,1)}, u32[]{:S(2)}) copy-start(bf16[256,1024]{1,0:T(8,128)(2,1)} %param.15) | copy-start | bytes 1572868
  129.6 7.6 %copy-start.15 = (bf16[512,512]{1,0:T(8,128)(2,1)S(1)}, bf16[512,512]{1,0:T(8,128)(2,1)}, u32[]{:S(2)}) copy-start(bf16[512,512]{1,0:T(8,128)(2,1)} %copy-done.14) | copy-start | bytes 1572868
  129.6 47.8 %all-to-all-start.2 = ((bf16[16,1,32,2048]{3,2,1,0:T(8,128)(2,1)}), bf16[16,1,32,2048]{3,2,1,0:T(8,128)(2,1)}, u32[]{:S(2)}, u32[]{:S(2)}) async-start(bf16[16,1,32,2048]{3,2,1,0:T(8,128)(2,1)} %bitcast.12), calls=%async_computation.2 | async-start | bytes 4194304 | tf_op jit(solution)/shard_map/all_to_all | solution.py:244
  140.0 3.1 %copy-start.18 = (f32[512,512]{1,0:T(8,128)S(1)}, f32[512,512]{1,0:T(8,128)}, u32[]{:S(2)}) copy-start(f32[512,512]{1,0:T(8,128)} %fusion.9) | copy-start | bytes 3145732
  140.1 3.1 %copy-start.20 = (f32[512,512]{1,0:T(8,128)S(1)}, f32[512,512]{1,0:T(8,128)}, u32[]{:S(2)}) copy-start(f32[512,512]{1,0:T(8,128)} %fusion.17) | copy-start | bytes 3145732
  143.1 3.2 %copy-start.3 = (bf16[512,2048]{1,0:T(8,128)(2,1)S(1)}, bf16[512,2048]{1,0:T(8,128)(2,1)}, u32[]{:S(2)}) copy-start(bf16[512,2048]{1,0:T(8,128)(2,1)} %copy-done.2) | copy-start | bytes 6291460
  143.1 3.2 %copy-start.11 = (bf16[512,512]{1,0:T(8,128)(2,1)S(1)}, bf16[512,512]{1,0:T(8,128)(2,1)}, u32[]{:S(2)}) copy-start(bf16[512,512]{1,0:T(8,128)(2,1)} %copy-done.10) | copy-start | bytes 1572868
  149.7 3.4 %copy-start.6 = (f32[512,512]{1,0:T(8,128)S(1)}, f32[512,512]{1,0:T(8,128)}, u32[]{:S(2)}) copy-start(f32[512,512]{1,0:T(8,128)} %fusion.7) | copy-start | bytes 3145732
  149.7 3.4 %copy-start.7 = (f32[512,512]{1,0:T(8,128)S(1)}, f32[512,512]{1,0:T(8,128)}, u32[]{:S(2)}) copy-start(f32[512,512]{1,0:T(8,128)} %fusion.15) | copy-start | bytes 3145732
  149.7 3.4 %copy-start.9 = (bf16[512,2048]{1,0:T(8,128)(2,1)S(1)}, bf16[512,2048]{1,0:T(8,128)(2,1)}, u32[]{:S(2)}) copy-start(bf16[512,2048]{1,0:T(8,128)(2,1)} %copy-done.8) | copy-start | bytes 6291460
  153.2 24.2 %copy-start.22 = (bf16[128,2048]{1,0:T(8,128)(2,1)S(1)}, bf16[128,2048]{1,0:T(8,128)(2,1)}, u32[]{:S(2)}) copy-start(bf16[128,2048]{1,0:T(8,128)(2,1)} %param.12) | copy-start | bytes 1572868
  156.6 23.0 %copy-start.23 = (f32[31,1024]{1,0:T(8,128)S(1)}, f32[31,1024]{1,0:T(8,128)}, u32[]{:S(2)}) copy-start(f32[31,1024]{1,0:T(8,128)} %param.16) | copy-start | bytes 380932
  177.4 4.5 %copy-start.13 = (bf16[256,1024]{1,0:T(8,128)(2,1)S(1)}, bf16[256,1024]{1,0:T(8,128)(2,1)}, u32[]{:S(2)}) copy-start(bf16[256,1024]{1,0:T(8,128)(2,1)} %param.15) | copy-start | bytes 1572868
  177.4 4.5 %copy-start.27 = (f32[1024]{0:T(1024)S(1)}, f32[1024]{0:T(1024)}, u32[]{:S(2)}) copy-start(f32[1024]{0:T(1024)} %param.17) | copy-start | bytes 12292
  179.5 2.0 collective-permute-start.7
  185.4 11.4 %copy-start.25 = (bf16[1024,2048]{1,0:T(8,128)(2,1)S(1)}, bf16[1024,2048]{1,0:T(8,128)(2,1)}, u32[]{:S(2)}) copy-start(bf16[1024,2048]{1,0:T(8,128)(2,1)} %param.18) | copy-start | bytes 12582916
  186.5 18.7 %collective-permute-start.10 = (bf16[2,2,2,128,256]{4,3,0,1,2:T(8,128)(2,1)}, bf16[2,2,2,128,256]{4,3,0,1,2:T(8,128)(2,1)}, u32[]{:S(2)}, u32[]{:S(2)}) collective-permute-start(bf16[2,2,2,128,256]{4,3,0,1,2:T(8,128)(2,1)} %bitcast.167), channel_id=1, source_target_pairs={{0,8},{2,10},{4,12},{6,14},{8,0},{10,2},{12,4},{14,6},{16,24},{18,... | collective-permute-start | bytes 1572872 | tf_op jit(solution)/shard_map/ppermute | solution.py:82
  192.6 19.6 %collective-permute-start.8 = (bf16[2,2,2,128,384]{4,3,0,1,2:T(8,128)(2,1)}, bf16[2,2,2,128,384]{4,3,0,1,2:T(8,128)(2,1)}, u32[]{:S(2)}, u32[]{:S(2)}) collective-permute-start(bf16[2,2,2,128,384]{4,3,0,1,2:T(8,128)(2,1)} %bitcast.166), channel_id=1, source_target_pairs={{0,2},{2,0},{4,6},{6,4},{8,10},{10,8},{12,14},{14,12},{16,18},{18,... | collective-permute-start | bytes 2359304 | tf_op jit(solution)/shard_map/ppermute | solution.py:82
  194.3 19.9 %collective-permute-start.9 = (bf16[2,2,2,128,384]{4,3,0,2,1:T(8,128)(2,1)S(1)}, bf16[2,2,2,128,384]{4,3,0,2,1:T(8,128)(2,1)}, u32[]{:S(2)}, u32[]{:S(2)}) collective-permute-start(bf16[2,2,2,128,384]{4,3,0,2,1:T(8,128)(2,1)S(1)} %bitcast.173), channel_id=1, source_target_pairs={{0,4},{2,6},{4,0},{6,2},{8,12},{10,14},{12,8},{14,10},{16,20},{18,... | collective-permute-start | bytes 2359304 | tf_op jit(solution)/shard_map/ppermute | solution.py:82
  215.5 11.4 %collective-permute-start.11 = (bf16[2,2,128,384]{3,2,0,1:T(8,128)(2,1)S(1)}, bf16[2,2,128,384]{3,2,0,1:T(8,128)(2,1)S(1)}, u32[]{:S(2)}, u32[]{:S(2)}) collective-permute-start(bf16[2,2,128,384]{3,2,0,1:T(8,128)(2,1)S(1)} %fusion.80), channel_id=1, source_target_pairs={{0,4},{2,6},{4,0},{6,2},{8,12},{10,14},{12,8},{14,10},{16,20},{18,... | collective-permute-start | bytes 1179656 | tf_op jit(solution)/shard_map/ppermute | solution.py:82
  218.6 2.2 copy-start.16
  218.7 9.5 %collective-permute-start.12 = (bf16[2,2,128,384]{3,2,0,1:T(8,128)(2,1)S(1)}, bf16[2,2,128,384]{3,2,0,1:T(8,128)(2,1)S(1)}, u32[]{:S(2)}, u32[]{:S(2)}) collective-permute-start(bf16[2,2,128,384]{3,2,0,1:T(8,128)(2,1)S(1)} %fusion.81), channel_id=1, source_target_pairs={{0,8},{2,10},{4,12},{6,14},{8,0},{10,2},{12,4},{14,6},{16,24},{18,... | collective-permute-start | bytes 1179656 | tf_op jit(solution)/shard_map/ppermute | solution.py:82
  220.3 6.7 %collective-permute-start.13 = (bf16[2,2,128,256]{3,2,0,1:T(8,128)(2,1)S(1)}, bf16[2,2,128,256]{3,2,0,1:T(8,128)(2,1)S(1)}, u32[]{:S(2)}, u32[]{:S(2)}) collective-permute-start(bf16[2,2,128,256]{3,2,0,1:T(8,128)(2,1)S(1)} %fusion.82), channel_id=1, source_target_pairs={{0,2},{2,0},{4,6},{6,4},{8,10},{10,8},{12,14},{14,12},{16,18},{18,... | collective-permute-start | bytes 786440 | tf_op jit(solution)/shard_map/ppermute | solution.py:82
  228.5 7.7 %collective-permute-start.16 = (bf16[2,128,256]{2,1,0:T(8,128)(2,1)S(1)}, bf16[2,128,256]{2,1,0:T(8,128)(2,1)S(1)}, u32[]{:S(2)}, u32[]{:S(2)}) collective-permute-start(bf16[2,128,256]{2,1,0:T(8,128)(2,1)S(1)} %fusion.87), channel_id=1, source_target_pairs={{0,4},{2,6},{4,0},{6,2},{8,12},{10,14},{12,8},{14,10},{16,20},{18,... | collective-permute-start | bytes 393224 | tf_op jit(solution)/shard_map/ppermute | solution.py:82
  229.2 7.0 %collective-permute-start.15 = (bf16[2,128,384]{2,1,0:T(8,128)(2,1)S(1)}, bf16[2,128,384]{2,1,0:T(8,128)(2,1)S(1)}, u32[]{:S(2)}, u32[]{:S(2)}) collective-permute-start(bf16[2,128,384]{2,1,0:T(8,128)(2,1)S(1)} %fusion.84), channel_id=1, source_target_pairs={{0,2},{2,0},{4,6},{6,4},{8,10},{10,8},{12,14},{14,12},{16,18},{18,... | collective-permute-start | bytes 589832 | tf_op jit(solution)/shard_map/ppermute | solution.py:82
  229.8 6.5 %collective-permute-start.14 = (bf16[2,128,384]{2,1,0:T(8,128)(2,1)S(1)}, bf16[2,128,384]{2,1,0:T(8,128)(2,1)S(1)}, u32[]{:S(2)}, u32[]{:S(2)}) collective-permute-start(bf16[2,128,384]{2,1,0:T(8,128)(2,1)S(1)} %fusion.83), channel_id=1, source_target_pairs={{0,8},{2,10},{4,12},{6,14},{8,0},{10,2},{12,4},{14,6},{16,24},{18,... | collective-permute-start | bytes 589832 | tf_op jit(solution)/shard_map/ppermute | solution.py:82
  230.3 11.9 %collective-permute-start.20 = (bf16[15,1024]{1,0:T(8,128)(2,1)S(1)}, bf16[15,1024]{1,0:T(8,128)(2,1)S(1)}, u32[]{:S(2)}, u32[]{:S(2)}) collective-permute-start(bf16[15,1024]{1,0:T(8,128)(2,1)S(1)} %get-tuple-element.83), channel_id=1, source_target_pairs={{2,0},{4,2},{6,4},{8,6},{10,8},{12,10},{14,12},{16,14},{18,16},{20... | collective-permute-start | bytes 92168 | tf_op jit(solution)/shard_map/ppermute | solution.py:17
  231.6 10.6 %collective-permute-start.21 = (bf16[15,1024]{1,0:T(8,128)(2,1)S(1)}, bf16[15,1024]{1,0:T(8,128)(2,1)S(1)}, u32[]{:S(2)}, u32[]{:S(2)}) collective-permute-start(bf16[15,1024]{1,0:T(8,128)(2,1)S(1)} %get-tuple-element.84), channel_id=1, source_target_pairs={{0,2},{2,4},{4,6},{6,8},{8,10},{10,12},{12,14},{14,16},{16,18},{18... | collective-permute-start | bytes 92168 | tf_op jit(solution)/shard_map/ppermute | solution.py:14
  236.3 13.6 %copy-start.1 = (bf16[1,2048,512]{2,1,0:T(8,128)(2,1)S(1)}, bf16[1,2048,512]{2,1,0:T(8,128)(2,1)}, u32[]{:S(2)}) copy-start(bf16[1,2048,512]{2,1,0:T(8,128)(2,1)} %param.19) | copy-start | bytes 6291460
  236.4 11.3 %collective-permute-start.19 = (bf16[128,256]{1,0:T(8,128)(2,1)S(1)}, bf16[128,256]{1,0:T(8,128)(2,1)S(1)}, u32[]{:S(2)}, u32[]{:S(2)}) collective-permute-start(bf16[128,256]{1,0:T(8,128)(2,1)S(1)} %fusion.90), channel_id=1, source_target_pairs={{0,16},{2,18},{4,20},{6,22},{8,24},{10,26},{12,28},{14,30},{16,0},... | collective-permute-start | bytes 196616 | tf_op jit(solution)/shard_map/ppermute | solution.py:82
  239.3 8.6 %collective-permute-start.18 = (bf16[128,384]{1,0:T(8,128)(2,1)S(1)}, bf16[128,384]{1,0:T(8,128)(2,1)S(1)}, u32[]{:S(2)}, u32[]{:S(2)}) collective-permute-start(bf16[128,384]{1,0:T(8,128)(2,1)S(1)} %fusion.89), channel_id=1, source_target_pairs={{0,16},{2,18},{4,20},{6,22},{8,24},{10,26},{12,28},{14,30},{16,0},... | collective-permute-start | bytes 294920 | tf_op jit(solution)/shard_map/ppermute | solution.py:82
  239.5 9.5 %collective-permute-start.17 = (bf16[128,384]{1,0:T(8,128)(2,1)S(1)}, bf16[128,384]{1,0:T(8,128)(2,1)S(1)}, u32[]{:S(2)}, u32[]{:S(2)}) collective-permute-start(bf16[128,384]{1,0:T(8,128)(2,1)S(1)} %fusion.88), channel_id=1, source_target_pairs={{0,16},{2,18},{4,20},{6,22},{8,24},{10,26},{12,28},{14,30},{16,0},... | collective-permute-start | bytes 294920 | tf_op jit(solution)/shard_map/ppermute | solution.py:82
  (5 other events, 7.5 us)
